TPU v7x, 32 devices: a whole 2x2x4 slice. The times are simulated.
32 devices in a mesh: sp: 8 (over z, core), tp: 4 (over y, x).
Axes of the slice: x: 2, y: 2, z: 4, core: 2. Of those that a mesh axis runs over, the one named last changes fastest.
Arguments:
- pool_in: bfloat16 [512, 3072], P('tp', 'sp'), may hold values from -8 to 8
- doc_ids: int32 [3072], P('sp'), may hold values from 0 to 3, never falling along the last dimension, each value on 1 to 1536 neighbouring positions
- pool_map: bfloat16 [8, 64, 64], replicated, may hold values from -0.75 to 0.75
- pool_scale: float32 [512], replicated, may hold values from 0.1 to 1.9
- w_out: bfloat16 [512, 2048], P(None, 'tp'), may hold values from -0.25 to 0.25
- gate_logit: bfloat16 [3072, 2048], P('sp', 'tp'), may hold values from -8 to 8
- residual: bfloat16 [3072, 2048], P('sp', 'tp'), may hold values from -4 to 4
- first_gain: float32 [2048], P('tp'), may hold values from 0.1 to 1.9
- first_bias: float32 [2048], P('tp'), may hold values from -1.5 to 1.5
- routes: int32 [3072, 2], P('sp'), may hold values from 0 to 7, all different within a row; in each aligned block of 384 rows (0 to 383, 384 to 767, ...) at most 192 rows name the same one
- route_weight: float32 [3072, 2], P('sp'), may hold values from 0.25 to 1
- w_gate: bfloat16 [8, 2048, 1024], P('sp', None, 'tp'), may hold values from -0.125 to 0.125
- w_up: bfloat16 [8, 2048, 1024], P('sp', None, 'tp'), may hold values from -0.125 to 0.125
- w_down: bfloat16 [8, 1024, 2048], P('sp', None, 'tp'), may hold values from -0.375 to 0.375
- second_gain: float32 [2048], P('tp'), may hold values from 0.1 to 1.9
- second_bias: float32 [2048], P('tp'), may hold values from -1.5 to 1.5
Outputs:
- layer_out: bfloat16 [3072, 2048], P('sp', 'tp')
Inputs may be any that keep to these rules, and one draw needn't show every extreme that they name: `doc_ids`: never falling; each document spans 1 to 1536 positions. `routes`: each row names 2 different experts; in each aligned block of 384 rows (the rows of one index of sp) no expert is named by more than 192 rows, a bound that some block reaches.
All inputs are finite; a program needn't handle non-finite values.
Results may differ from a plain program's by a relative error of at most 0.008.
Values may be sent and summed in bfloat16 or wider, within the bound.
No kernel may reach another device: no remote copies, remote signals or barrier semaphores. Data moves between devices by JAX's collectives and lax.ppermute only.
A program may use at most 64 MiB of HBM per device.

v0:
```python
import jax
import jax.numpy as jnp
from jax import lax
from jax.sharding import PartitionSpec as P

GROUP_W = 64


EPS = 1e-05
ALPHA = 8.0**0.25
halo_len = 16


def shifted(shard, axis, by):
    size = lax.axis_size(axis)
    pairs = [(i, i + by) for i in range(size) if 0 <= i + by < size]
    return lax.ppermute(shard, axis, pairs)


def entering(shard, axis, combine, identity):
    size, place = (lax.axis_size(axis), lax.axis_index(axis))
    everything = jax.tree.map(lambda part: lax.all_gather(part, axis), shard)
    start = jax.tree.map(
        lambda part, zero: jnp.broadcast_to(jnp.asarray(zero, part.dtype), part.shape),
        shard,
        identity,
    )

    def turn(k, before):
        reached = k < place
        new = combine(before, jax.tree.map(lambda part: part[k], everything))
        return jax.tree.map(lambda a, b: jnp.where(reached, a, b), new, before)

    return lax.fori_loop(0, size, turn, start)


def carry_join(earlier, later):
    keeping = 1.0 - later[2]
    return (
        later[0] + keeping * earlier[0],
        later[1] + keeping * earlier[1],
        jnp.maximum(earlier[2], later[2]),
    )


def apply_norm(row_data, totals, gain_vec, bias_vec, features):
    row_mean = totals[0][:, None] / features
    row_var = totals[1][:, None] / features - row_mean * row_mean
    return (row_data - row_mean) * lax.rsqrt(row_var + EPS) * gain_vec + bias_vec


def pool_scales(pool_in, doc_ids):
    channels_dev, positions = pool_in.shape
    edge_block = jnp.concatenate(
        [
            pool_in[:, positions - halo_len :],
            doc_ids[None, positions - halo_len :].astype(jnp.bfloat16),
        ],
        axis=0,
    )
    previous = shifted(edge_block, "sp", 1)
    prior_ids = jnp.where(
        lax.axis_index("sp") == 0, -1.0, previous[channels_dev].astype(jnp.float32)
    )
    ids_ext = jnp.concatenate([prior_ids, doc_ids.astype(jnp.float32)])
    inputs_ext = jnp.concatenate([previous[:channels_dev], pool_in], axis=1).astype(jnp.float32)
    length = positions + halo_len
    opening = jnp.concatenate([jnp.zeros((1,), bool), ids_ext[1:] != ids_ext[:-1]])
    places = jnp.arange(length, dtype=jnp.int32)
    doc_start = lax.cummax(jnp.where(opening, places, 0), axis=0)
    prefix = jnp.concatenate(
        [jnp.zeros((channels_dev, 1), jnp.float32), jnp.cumsum(inputs_ext, axis=1)], axis=1
    )
    start_here = doc_start[halo_len:]
    upper_at = places[halo_len:] + 1
    at_start = jnp.take(prefix, start_here, axis=1)
    current = prefix[:, halo_len + 1 :]
    group_id = (
        lax.axis_index("tp") * channels_dev + jnp.arange(channels_dev, dtype=jnp.int32)
    ) // GROUP_W
    doc_mask = (group_id % 2 == 1)[:, None]
    window = jnp.left_shift(2, group_id // 2 % 4)[:, None]
    lagged = jnp.zeros((channels_dev, positions), jnp.float32)
    for octave in range(4):
        window_len = 2 << octave
        begin = halo_len + 1 - window_len
        lagged = lagged + jnp.where(window == window_len, prefix[:, begin : begin + positions], 0.0)
    lower_at = jnp.maximum(upper_at[None, :] - window, start_here[None, :])
    win_sum = current - jnp.where(
        start_here[None, :] > upper_at[None, :] - window, at_start, lagged
    )
    win_count = (upper_at[None, :] - lower_at).astype(jnp.float32)
    opened = start_here >= halo_len
    local_sum = current - jnp.where(opened[None, :], at_start, prefix[:, halo_len : halo_len + 1])
    local_count = (upper_at - jnp.maximum(start_here, halo_len)).astype(jnp.float32)
    last_start = doc_start[length - 1]
    last_base = jnp.where(
        last_start >= halo_len,
        lax.dynamic_slice_in_dim(prefix, last_start, 1, 1)[:, 0],
        prefix[:, halo_len],
    )
    summary = (
        prefix[:, length] - last_base,
        (length - jnp.maximum(last_start, halo_len)).astype(jnp.float32),
        (last_start >= halo_len).astype(jnp.float32),
    )
    nothing = (jnp.zeros((channels_dev,), jnp.float32), jnp.float32(0.0), jnp.float32(0.0))
    carried = entering(summary, "sp", carry_join, nothing)
    doc_sum = local_sum + jnp.where(opened[None, :], 0.0, carried[0][:, None])
    doc_count = local_count + jnp.where(opened, 0.0, carried[1])
    pooled = (
        jnp.where(doc_mask, doc_sum / doc_count[None, :], win_sum / win_count)
        - inputs_ext[:, halo_len:]
    )
    return pooled.astype(jnp.bfloat16)


def body(
    pool_in,
    doc_ids,
    pool_map,
    pool_scale,
    w_out,
    gate_logit,
    residual,
    first_gain,
    first_bias,
    routes,
    route_weight,
    w_gate,
    w_up,
    w_down,
    second_gain,
    second_bias,
):
    pooled = pool_scales(pool_in, doc_ids)
    positions = pool_in.shape[1]
    features = residual.shape[1] * lax.axis_size("tp")
    gathered = lax.all_gather(pooled, "tp", axis=0, tiled=True)
    group_count = gathered.shape[0] // GROUP_W
    grouped = jnp.einsum(
        "gct,gcd->tgd",
        gathered.reshape(group_count, GROUP_W, positions),
        pool_map,
        preferred_element_type=jnp.float32,
    )
    mapped = (grouped.reshape(positions, group_count * GROUP_W) * pool_scale).astype(jnp.bfloat16)
    mixer_out = jnp.dot(mapped, w_out, preferred_element_type=jnp.float32) * jax.nn.sigmoid(
        gate_logit.astype(jnp.float32)
    )
    mixed_rows = ALPHA * residual.astype(jnp.float32) + mixer_out
    first_totals = lax.psum(
        (jnp.sum(mixed_rows, axis=1), jnp.sum(mixed_rows * mixed_rows, axis=1)), "tp"
    )
    normed = apply_norm(mixed_rows, first_totals, first_gain, first_bias, features).astype(
        jnp.bfloat16
    )
    experts = lax.axis_size("sp")
    pairs = routes.shape[1]
    slots_per = 2 * positions * pairs // experts
    flat_routes = routes.reshape(-1)
    one_hot = (flat_routes[:, None] == jnp.arange(experts, dtype=jnp.int32)[None, :]).astype(
        jnp.int32
    )
    slot_rank = jnp.sum((jnp.cumsum(one_hot, axis=0, dtype=jnp.int32) - 1) * one_hot, axis=1)
    slot_ids = flat_routes * slots_per + slot_rank
    token_of = jnp.arange(flat_routes.shape[0], dtype=jnp.int32) // pairs
    outgoing = (
        jnp.zeros((experts * slots_per, normed.shape[1]), jnp.bfloat16)
        .at[slot_ids]
        .set(normed[token_of])
    )
    arrived = lax.all_to_all(outgoing, "sp", split_axis=0, concat_axis=0, tiled=True)
    inputs = lax.all_gather(arrived, "tp", axis=1, tiled=True)
    gate_part = jnp.dot(inputs, w_gate[0], preferred_element_type=jnp.float32)
    up_part = jnp.dot(inputs, w_up[0], preferred_element_type=jnp.float32)
    hidden = (jax.nn.silu(gate_part) * up_part).astype(jnp.bfloat16)
    down_part = w_down[0]
    result = jnp.dot(
        lax.all_gather(hidden, "tp", axis=1, tiled=True),
        down_part,
        preferred_element_type=jnp.float32,
    )
    returned = lax.all_to_all(
        result.astype(jnp.bfloat16), "sp", split_axis=0, concat_axis=0, tiled=True
    )
    picked = returned[slot_ids].astype(jnp.float32).reshape(positions, pairs, returned.shape[1])
    moe_sum = jnp.sum(picked * route_weight[:, :, None], axis=1)
    final_rows = ALPHA * normed.astype(jnp.float32) + moe_sum
    second_totals = lax.psum(
        (jnp.sum(final_rows, axis=1), jnp.sum(final_rows * final_rows, axis=1)), "tp"
    )
    return apply_norm(final_rows, second_totals, second_gain, second_bias, features).astype(
        jnp.bfloat16
    )


def solution(mesh):
    return jax.shard_map(
        body,
        mesh=mesh,
        in_specs=(
            P("tp", "sp"),
            P("sp"),
            P(),
            P(),
            P(None, "tp"),
            P("sp", "tp"),
            P("sp", "tp"),
            P("tp"),
            P("tp"),
            P("sp", None),
            P("sp", None),
            P("sp", None, "tp"),
            P("sp", None, "tp"),
            P("sp", None, "tp"),
            P("tp"),
            P("tp"),
        ),
        out_specs=P("sp", "tp"),
        check_vma=False,
    )
```

profile of v0, /device:TPU:0, one launch (start us, length us, event | category | flops | bytes accessed | tf_op | source)
XLA Modules:
  0.0 351.1 jit_solution(9610846345740772719)
XLA Ops:
  6.5 1.1 copy.26
  8.6 2.4 collective-permute-start
  13.0 1.7 reduce-window.29
  15.6 1.3 dynamic-slice
  23.6 13.0 %all-gather = f32[1024,1]{0,1:T(1,128)S(1)} all-gather(f32[128,1]{0,1:T(1,128)S(1)} %get-tuple-element.181), channel_id=2, replica_groups=mesh['sp'=8,'tp'=4] {'sp'}, dimensions={0}, use_global_device_ids=true | all-gather | bytes 4608 | tf_op jit(solution)/shard_map/all_gather | solution.py:22
  36.6 13.9 %all-reduce.5 = (f32[8]{0:T(128)S(1)}, f32[8]{0:T(128)S(1)}) all-reduce(f32[8]{0:T(128)S(1)} %dynamic-update-slice, f32[8]{0:T(128)S(1)} %dynamic-update-slice.1), channel_id=1, replica_groups=mesh['sp'=8,'tp'=4] {'sp'}, use_global_device_ids=true, to_apply=%add.3 | all-reduce | flops 16 | bytes 128
  50.5 20.5 %while.16 = (s32[]{:T(128)}, f32[128]{0:T(128)S(1)}, f32[]{:T(128)}, s32[]{:T(128)}, f32[8,128]{1,0:T(8,128)S(1)}, /*index=5*/f32[8]{0:T(128)S(1)}, f32[8]{0:T(128)S(1)}, s32[]{:T(128)}, s32[]{:T(128)}, f32[1]{0:T(128)}) while((s32[]{:T(128)}, f32[128]{0:T(128)S(1)}, f32[]{:T(128)}, s32[]{:T(128)}, f32[8,128]{1,0:T(8,128)S(1)}, ...), condition=%wide.region_5.6_spmd.clone, body=%wide.region_4.5_spmd.clone.sunk | while | flops 520 | bytes 1738 | solution.py:34
  71.1 1.1 gather_fusion
  72.6 9.5 %all_gather.34 = bf16[512,384]{0,1:T(8,128)(2,1)S(1)} all-gather(bf16[128,384]{0,1:T(8,128)(2,1)S(1)} %fusion.26), channel_id=1, replica_groups=mesh['sp'=8,'tp'=4] {'tp'}, dimensions={0}, use_global_device_ids=true | all-gather | bytes 491520 | tf_op jit(solution)/shard_map/all_gather | solution.py:139
  84.0 9.2 %all-reduce.7 = (f32[384]{0:T(512)S(1)}, f32[384]{0:T(512)S(1)}) all-reduce(f32[384]{0:T(512)S(1)} %get-tuple-element.159, f32[384]{0:T(512)S(1)} %get-tuple-element.158), channel_id=1, replica_groups=mesh['sp'=8,'tp'=4] {'tp'}, use_global_device_ids=true, to_apply=%region_9.10 | all-reduce | flops 768 | bytes 6144 | tf_op jit(solution)/shard_map/psum | solution.py:152
  94.2 21.4 %scatter_custom_fusion = bf16[1536,512]{1,0:T(8,128)(2,1)S(1)} fusion(s32[768]{0:T(1024)S(1)} %fusion.29, bf16[384,512]{1,0:T(8,128)(2,1)} %add_convert_fusion.1, s32[1024]{0:T(1024)S(1)} %pad_clamp_fusion.1, bf16[]{:T(256)} %constant.167.clone.1), kind=kCustom, calls=%fused_computation.19 | custom fusion | bytes 1573376 | tf_op jit(solution)/shard_map/scatter | solution.py:171
  115.6 40.9 %all_to_all.24 = bf16[8,192,512]{2,1,0:T(8,128)(2,1)} all-to-all(bf16[8,192,512]{2,1,0:T(8,128)(2,1)S(1)} %bitcast.85), channel_id=1, replica_groups=mesh['sp'=8,'tp'=4] {'sp'}, dimensions={0} | all-to-all | bytes 3145728 | tf_op jit(solution)/shard_map/all_to_all | solution.py:173
  156.8 67.8 %all-gather.4.cloned.1.call-done = bf16[1536,2048]{1,0:T(8,128)(2,1)} async-done(((bf16[1536,512]{1,0:T(8,128)(2,1)}), bf16[1536,2048]{1,0:T(8,128)(2,1)}) %all-gather.4.cloned.1.call-update) | async-done | bytes 6291472 | tf_op jit(solution)/shard_map/all_gather | solution.py:174
  224.6 4.8 %fusion.4 = f32[1536,256]{1,0:T(8,128)S(1)} fusion(bf16[1536,2048]{1,0:T(8,128)(2,1)} %all-gather.4.cloned.1.call-done, bf16[1,2048,256]{2,1,0:T(8,128)(2,1)S(1)} %copy-done.10), kind=kOutput, calls=%fused_computation.15 | convolution fusion | flops 1610612736 | bytes 8912896 | tf_op jit(solution)/shard_map/dot_general | solution.py:175
  229.4 3.0 fusion
  232.4 43.9 %all-gather.6.cloned.1.call-done = bf16[1536,1024]{1,0:T(8,128)(2,1)} async-done(((bf16[1536,256]{1,0:T(8,128)(2,1)}), bf16[1536,1024]{1,0:T(8,128)(2,1)}) %all-gather.6.cloned.1.call-update) | async-done | bytes 3145744 | tf_op jit(solution)/shard_map/all_gather | solution.py:180
  276.3 4.8 %convolution_convert_fusion = bf16[1536,512]{1,0:T(8,128)(2,1)} fusion(bf16[1536,1024]{1,0:T(8,128)(2,1)} %all-gather.6.cloned.1.call-done, bf16[1,1024,512]{2,1,0:T(8,128)(2,1)S(1)} %copy-done), kind=kOutput, calls=%fused_computation.7 | convolution fusion | flops 1611399168 | bytes 5767168 | tf_op jit(solution)/shard_map/dot_general | solution.py:179
  281.1 4.7 %all-to-all-start.1 = ((bf16[8,192,512]{2,1,0:T(8,128)(2,1)}), bf16[8,192,512]{2,1,0:T(8,128)(2,1)S(1)}, u32[]{:S(2)}, u32[]{:S(2)}) async-start(bf16[8,192,512]{2,1,0:T(8,128)(2,1)} %bitcast.86), calls=%async_computation.1 | async-start | bytes 3145728 | tf_op jit(solution)/shard_map/all_to_all | solution.py:184
  286.7 37.0 %all-to-all-done.1 = bf16[8,192,512]{2,1,0:T(8,128)(2,1)S(1)} async-done(((bf16[8,192,512]{2,1,0:T(8,128)(2,1)}), bf16[8,192,512]{2,1,0:T(8,128)(2,1)S(1)}, u32[]{:S(2)}, u32[]{:S(2)}) %all-to-all-start.1) | async-done | bytes 1572896 | tf_op jit(solution)/shard_map/all_to_all | solution.py:184
  323.7 3.3 gather_fusion.1
  327.0 3.0 reshape.282
  330.0 3.6 %multiply_reduce_fusion = f32[384,512]{1,0:T(8,128)S(1)} fusion(f32[384,2,512]{2,1,0:T(2,128)} %reshape.282, f32[384,2]{1,0:T(8,128)S(1)} %copy-done.1), kind=kLoop, calls=%fused_computation.10 | loop fusion | flops 589824 | bytes 2362368 | tf_op jit(solution)/shard_map/reduce_sum | solution.py:188
  334.0 8.9 %all-reduce.6 = (f32[384]{0:T(512)S(1)}, f32[384]{0:T(512)S(1)}) all-reduce(f32[384]{0:T(512)S(1)} %get-tuple-element.157, f32[384]{0:T(512)S(1)} %get-tuple-element.156), channel_id=1, replica_groups=mesh['sp'=8,'tp'=4] {'tp'}, use_global_device_ids=true, to_apply=%region_18.19 | all-reduce | flops 768 | bytes 6144 | tf_op jit(solution)/shard_map/psum | solution.py:190
  342.9 1.3 add_convert_fusion
  (129 shorter events, 22.2 us)
Async XLA Ops:
  6.5 269.8 %copy-start = (bf16[1,1024,512]{2,1,0:T(8,128)(2,1)S(1)}, bf16[1,1024,512]{2,1,0:T(8,128)(2,1)}, u32[]{:S(2)}) copy-start(bf16[1,1024,512]{2,1,0:T(8,128)(2,1)} %param.31) | copy-start | bytes 3145732
  6.5 218.0 %all-gather.4.cloned.1.call-start = ((), (), s32[]{:S(2)}) async-start(), calls=%async_computation.2 | async-start | bytes 7864320 | tf_op jit(solution)/shard_map/all_gather | solution.py:174
  8.6 8.3 %collective-permute-start = (bf16[129,16]{0,1:T(8,128)(2,1)S(1)}, bf16[129,16]{0,1:T(8,128)(2,1)S(1)}, u32[]{:S(2)}, u32[]{:S(2)}) collective-permute-start(bf16[129,16]{0,1:T(8,128)(2,1)S(1)} %pad_maximum_fusion), channel_id=1, source_target_pairs={{0,4},{4,8},{8,12},{12,16},{16,20},{20,24},{24,28},{1,5},{5,9},{9,... | collective-permute-start | bytes 12392 | tf_op jit(solution)/shard_map/ppermute | solution.py:17
  72.2 10.1 %copy-start.2 = (bf16[8,64,64]{2,1,0:T(8,128)(2,1)S(1)}, bf16[8,64,64]{2,1,0:T(8,128)(2,1)}, u32[]{:S(2)}) copy-start(bf16[8,64,64]{2,1,0:T(8,128)(2,1)} %param.20) | copy-start | bytes 196612
  72.6 10.1 %copy-start.6 = (f32[512]{0:T(512)S(1)}, f32[512]{0:T(512)}, u32[]{:S(2)}) copy-start(f32[512]{0:T(512)} %param.21) | copy-start | bytes 6148
  82.1 1.0 copy-start.12
  82.1 1.2 copy-start.13
  82.1 1.3 copy-start.14
  83.4 9.9 %copy-start.3 = (f32[512]{0:T(512)S(1)}, f32[512]{0:T(512)}, u32[]{:S(2)}) copy-start(f32[512]{0:T(512)} %param.26) | copy-start | bytes 6148
  83.4 9.9 %copy-start.4 = (f32[512]{0:T(512)S(1)}, f32[512]{0:T(512)}, u32[]{:S(2)}) copy-start(f32[512]{0:T(512)} %param.25) | copy-start | bytes 6148
  156.6 68.0 %copy-start.10 = (bf16[1,2048,256]{2,1,0:T(8,128)(2,1)S(1)}, bf16[1,2048,256]{2,1,0:T(8,128)(2,1)}, u32[]{:S(2)}) copy-start(bf16[1,2048,256]{2,1,0:T(8,128)(2,1)} %param.29) | copy-start | bytes 3145732
  156.6 119.7 %all-gather.6.cloned.1.call-start = ((), (), s32[]{:S(2)}) async-start(), calls=%async_computation.3 | async-start | bytes 3932160 | tf_op jit(solution)/shard_map/all_gather | solution.py:180
  224.6 4.8 %copy-start.9 = (bf16[1536,2048]{1,0:T(8,128)(2,1)S(1)}, bf16[1536,2048]{1,0:T(8,128)(2,1)}, u32[]{:S(2)}) copy-start(bf16[1536,2048]{1,0:T(8,128)(2,1)} %all-gather.4.cloned.1.call-done) | copy-start | bytes 18874372
  224.6 4.9 %copy-start.11 = (bf16[1,2048,256]{2,1,0:T(8,128)(2,1)S(1)}, bf16[1,2048,256]{2,1,0:T(8,128)(2,1)}, u32[]{:S(2)}) copy-start(bf16[1,2048,256]{2,1,0:T(8,128)(2,1)} %param.30) | copy-start | bytes 3145732
  281.1 4.7 %copy-start.5 = (f32[384,2]{0,1:T(2,128)S(1)}, f32[384,2]{0,1:T(2,128)}, u32[]{:S(2)}) copy-start(f32[384,2]{0,1:T(2,128)} %param.28) | copy-start | bytes 9220
  281.1 42.5 %all-to-all-start.1 = ((bf16[8,192,512]{2,1,0:T(8,128)(2,1)}), bf16[8,192,512]{2,1,0:T(8,128)(2,1)S(1)}, u32[]{:S(2)}, u32[]{:S(2)}) async-start(bf16[8,192,512]{2,1,0:T(8,128)(2,1)} %bitcast.86), calls=%async_computation.1 | async-start | bytes 3145728 | tf_op jit(solution)/shard_map/all_to_all | solution.py:184
  327.0 3.0 copy-start.1
  330.0 12.9 %copy-start.7 = (f32[512]{0:T(512)S(1)}, f32[512]{0:T(512)}, u32[]{:S(2)}) copy-start(f32[512]{0:T(512)} %param.33) | copy-start | bytes 6148
  330.0 12.9 %copy-start.8 = (f32[512]{0:T(512)S(1)}, f32[512]{0:T(512)}, u32[]{:S(2)}) copy-start(f32[512]{0:T(512)} %param.32) | copy-start | bytes 6148
Sparse Core Ops, SparseCore 0:
  156.7 67.8 all-gather.3
  232.5 43.6 all-gather.5
where the time goes:
time: 352 us; the launch traced here: 351 us
  waiting for transfers between devices  149 us (42%)
  blocking collectives  95.5 us (27%)
  local copies, waits for them, and re-layouts  47 us (13%)
  between operations  16.8 us (5%)
  matrix products  13.6 us (4%)
  other arithmetic  11.7 us (3%)
  loops' own time  10.5 us (3%)
  starting transfers between devices  7.35 us (2%)
    all_gather x1, waiting for transfers between devices, body(): inputs = lax.all_gather(arrived, 'tp', axis=1, tiled=True)  67.8 us
    all_gather x1, waiting for transfers between devices, body(): lax.all_gather(hidden, 'tp', axis=1, tiled=True)  43.9 us
    all_to_all x1, blocking collectives, body(): lax.all_to_all(outgoing, 'sp', split_axis=0, concat_axis=0, tiled=True)  40.9 us
    all_to_all x1, waiting for transfers between devices, body(): lax.all_to_all(result.astype(jnp.bfloat16), 'sp', split_axis=0, concat_ax...  37 us
    scatter x1, local copies, waits for them, and re-layouts, body(): outgoing = jnp.zeros((experts * slots_per, normed.shape[1]), jnp.bfloat16...  21.4 us
    unnamed x1, blocking collectives  13.9 us
    all_gather x1, blocking collectives, entering(): everything = jax.tree.map(lambda part: lax.all_gather(part, axis), shard)  13 us
    another operation x1, loops' own time, entering(): return lax.fori_loop(0, size, turn, start)  10.5 us
  transfers between devices with their start and end apart: 4, of which 3 were waited for; matrix products, arithmetic and copies ran while one was open for 2% of the time, Pallas kernels for 0%

commit v1 on v0

v1 whole, which is shorter than its diff:
```python
import jax
import jax.numpy as jnp
from jax import lax
from jax.sharding import PartitionSpec as P


GROUP_W = 64
EPS = 1e-05
ALPHA = 8.0**0.25
HALO = 16
F32 = jnp.float32
BF16 = jnp.bfloat16


def swap_with(part, axis, bits):
    size = lax.axis_size(axis)
    return lax.ppermute(part, axis, [(i, i ^ bits) for i in range(size)])


def in_order(relative, index):
    stacked = jnp.stack(relative)
    return [
        lax.dynamic_index_in_dim(stacked, index ^ p, 0, keepdims=False)
        for p in range(len(relative))
    ]


def exchange_all(part, axis):
    return [part] + [swap_with(part, axis, k) for k in range(1, lax.axis_size(axis))]


def line_gather(part, axis):
    size = lax.axis_size(axis)
    mine = [part] + [swap_with(part, axis, 2 * k) for k in range(1, size // 2)]
    return mine + [swap_with(m, axis, 1) for m in mine]


def norm_rows(rows, features):
    mean = sum(jnp.sum(r, axis=1, keepdims=True) for r in rows) / features
    square = sum(jnp.sum(r * r, axis=1, keepdims=True) for r in rows) / features
    scale = lax.rsqrt(square - mean * mean + EPS)
    return [(r - mean) * scale for r in rows]


def weight_parts(w_gate, w_up, w_down, tp):
    if tp != 4:
        return tuple(exchange_all(w, "tp") for w in (w_gate, w_up, w_down))
    half = w_gate.shape[0] // 2
    gate1_top = swap_with(w_gate[:half], "tp", 1)
    up2_top = swap_with(w_up[:half], "tp", 2)
    gate1_low = swap_with(w_gate[half:], "tp", 1)
    up2_low = swap_with(w_up[half:], "tp", 2)
    up1 = swap_with(w_up, "tp", 1)
    gate2 = swap_with(w_gate, "tp", 2)
    up3_top = swap_with(up2_top, "tp", 1)
    up3_low = swap_with(up2_low, "tp", 1)
    gate3_top = swap_with(gate1_top, "tp", 2)
    gate3_low = swap_with(gate1_low, "tp", 2)
    down1 = swap_with(w_down, "tp", 1)
    down2 = swap_with(w_down, "tp", 2)
    dhalf = w_down.shape[0] // 2
    down3_low = swap_with(down2[dhalf:], "tp", 1)
    down3_top = swap_with(down1[:dhalf], "tp", 2)
    gate = [
        w_gate,
        jnp.concatenate([gate1_top, gate1_low]),
        gate2,
        jnp.concatenate([gate3_top, gate3_low]),
    ]
    up = [
        w_up,
        up1,
        jnp.concatenate([up2_top, up2_low]),
        jnp.concatenate([up3_top, up3_low]),
    ]
    down = [w_down, down1, down2, jnp.concatenate([down3_top, down3_low])]
    return gate, up, down


def body(
    pool_in,
    doc_ids,
    pool_map,
    pool_scale,
    w_out,
    gate_logit,
    residual,
    first_gain,
    first_bias,
    routes,
    route_weight,
    w_gate,
    w_up,
    w_down,
    second_gain,
    second_bias,
):
    sp, tp = lax.axis_size("sp"), lax.axis_size("tp")
    i, j = lax.axis_index("sp"), lax.axis_index("tp")
    channels, positions = pool_in.shape
    width = residual.shape[1]
    features = width * tp
    quarter = positions // tp
    pairs = routes.shape[1]

    docs = doc_ids.astype(F32)
    values = pool_in.astype(F32)
    ending = docs == docs[positions - 1]
    tail_sum = jnp.sum(jnp.where(ending[None, :], values, 0.0), axis=1)
    tail_count = jnp.sum(ending.astype(F32))
    halo = values[:, positions - HALO :]
    my_routes = lax.dynamic_slice_in_dim(routes, j * quarter, quarter, 0)
    my_weights = lax.dynamic_slice_in_dim(route_weight, j * quarter, quarter, 0)
    lead = jnp.concatenate([docs[positions - HALO :], tail_count[None]])
    flat = jnp.concatenate(
        [
            tail_sum,
            halo.reshape(-1),
            lead,
            my_routes.astype(F32).T.reshape(-1),
            my_weights.T.reshape(-1),
        ]
    )
    used = flat.shape[0]
    rows = -(-used // 128)
    flat = jnp.pad(flat, (0, rows * 128 - used)).reshape(rows, 128)
    pair = jnp.stack([flat, swap_with(flat, "sp", 1)])
    by_z = [pair] + [swap_with(pair, "sp", 2 * k) for k in range(1, sp // 2)]
    rel = [by_z[k // 2][k % 2].reshape(-1)[:used] for k in range(sp)]

    c1 = channels
    c2 = c1 + channels * HALO
    c3 = c2 + HALO + 1
    c4 = c3 + pairs * quarter
    carried_sum = jnp.zeros((channels,), F32)
    carried_count = jnp.zeros((), F32)
    prev = jnp.zeros((c3,), F32)
    for k in range(1, sp):
        source = i ^ k
        same = (source < i) & (rel[k][c2 + HALO - 1] == docs[0])
        carried_sum = carried_sum + jnp.where(same, rel[k][:c1], 0.0)
        carried_count = carried_count + jnp.where(same, rel[k][c2 + HALO], 0.0)
        prev = prev + jnp.where(source == i - 1, rel[k][:c3], 0.0)
    halo_in = prev[c1:c2].reshape(channels, HALO).astype(BF16)
    halo_docs = jnp.where(i == 0, -1.0, prev[c2 : c2 + HALO])

    t_at = jnp.arange(positions, dtype=jnp.int32)
    s_at = t_at[:, None]
    same_doc = (docs[:, None] == docs[None, :]) & (s_at <= t_at[None, :])
    local_count = jnp.sum(same_doc.astype(F32), axis=0)
    in_first = docs == docs[0]
    doc_count = local_count + jnp.where(in_first, carried_count, 0.0)
    unit = min(GROUP_W, channels)
    halo_at = jnp.arange(HALO, dtype=jnp.int32) - HALO
    halo_same = halo_docs[:, None] == docs[None, :]
    pooled_units = []
    for u in range(channels // unit):
        group = (j * channels + u * unit) // GROUP_W
        whole_doc = group % 2 == 1
        window = jnp.left_shift(2, group // 2 % 4)
        mask = same_doc & (whole_doc | (s_at > t_at[None, :] - window))
        here = pool_in[u * unit : (u + 1) * unit]
        total = jnp.dot(here, mask.astype(BF16), preferred_element_type=F32)
        halo_mask = halo_same & (halo_at[:, None] > t_at[None, :] - window) & ~whole_doc
        total = total + jnp.dot(
            halo_in[u * unit : (u + 1) * unit],
            halo_mask.astype(BF16),
            preferred_element_type=F32,
        )
        carry_here = carried_sum[u * unit : (u + 1) * unit]
        total = total + jnp.where(
            whole_doc & in_first[None, :], carry_here[:, None], 0.0
        )
        count = jnp.where(
            whole_doc, doc_count, jnp.minimum(doc_count, window.astype(F32))
        )
        pooled_units.append(total / count[None, :] - here.astype(F32))
    pooled = jnp.concatenate(pooled_units).astype(BF16)

    pooled_rel = exchange_all(pooled, "tp")
    gathered = jnp.concatenate(in_order(pooled_rel, j))
    group_count = gathered.shape[0] // GROUP_W
    grouped = jnp.einsum(
        "gct,gcd->tgd",
        gathered.reshape(group_count, GROUP_W, positions),
        pool_map,
        preferred_element_type=F32,
    )
    mapped = (grouped.reshape(positions, group_count * GROUP_W) * pool_scale).astype(BF16)
    mixer_out = jnp.dot(mapped, w_out, preferred_element_type=F32) * jax.nn.sigmoid(
        gate_logit.astype(F32)
    )
    mixed = ALPHA * residual.astype(F32) + mixer_out

    quarters = [
        lax.dynamic_slice_in_dim(mixed, (j ^ k) * quarter, quarter, 0) for k in range(tp)
    ]
    mixed_rel = [quarters[0]] + [swap_with(quarters[k], "tp", k) for k in range(1, tp)]
    gains = exchange_all(
        jnp.stack([first_gain, first_bias, second_gain, second_bias]), "tp"
    )
    normed_rel = [
        (r * gains[k][0] + gains[k][1]).astype(BF16)
        for k, r in enumerate(norm_rows(mixed_rel, features))
    ]
    tokens = jnp.concatenate(in_order(normed_rel, j), axis=1)

    gate_w, up_w, down_w = weight_parts(w_gate[0], w_up[0], w_down[0], tp)

    everyone = line_gather(tokens, "sp")
    inputs = jnp.concatenate(everyone)
    order = [2 * k for k in range(sp // 2)] + [2 * k + 1 for k in range(sp // 2)]
    mine = i.astype(F32)
    gate_cols = []
    for k in order:
        chosen = rel[k][c3:c4].reshape(pairs, quarter) == mine
        gate_cols.append(
            jnp.sum(jnp.where(chosen, rel[k][c4:].reshape(pairs, quarter), 0.0), axis=0)
        )
    share = jnp.concatenate(gate_cols)[:, None]

    hidden_rel = []
    for k in range(tp):
        gate_part = jnp.dot(inputs, gate_w[k], preferred_element_type=F32)
        up_part = jnp.dot(inputs, up_w[k], preferred_element_type=F32)
        hidden_rel.append((jax.nn.silu(gate_part) * up_part).astype(BF16))
    hidden = jnp.concatenate(in_order(hidden_rel, j), axis=1)

    final_rel = []
    half_rows = (sp // 2) * quarter
    for k in range(tp):
        result = jnp.dot(hidden, down_w[k], preferred_element_type=F32)
        partial = (result * share).astype(BF16)
        other = swap_with(partial[half_rows:], "sp", 1)
        joined = partial[:half_rows].astype(F32) + other.astype(F32)
        moe = joined[:quarter]
        sent = joined.astype(BF16)
        for d in range(1, sp // 2):
            got = swap_with(sent[d * quarter : (d + 1) * quarter], "sp", 2 * d)
            moe = moe + got.astype(F32)
        final_rel.append(ALPHA * normed_rel[k].astype(F32) + moe)
    out_rel = [
        (r * gains[k][2] + gains[k][3]).astype(BF16)
        for k, r in enumerate(norm_rows(final_rel, features))
    ]
    home_rel = [out_rel[0]] + [swap_with(out_rel[k], "tp", k) for k in range(1, tp)]
    return jnp.concatenate(in_order(home_rel, j))


def solution(mesh):
    return jax.shard_map(
        body,
        mesh=mesh,
        in_specs=(
            P("tp", "sp"),
            P("sp"),
            P(),
            P(),
            P(None, "tp"),
            P("sp", "tp"),
            P("sp", "tp"),
            P("tp"),
            P("tp"),
            P("sp", None),
            P("sp", None),
            P("sp", None, "tp"),
            P("sp", None, "tp"),
            P("sp", None, "tp"),
            P("tp"),
            P("tp"),
        ),
        out_specs=P("sp", "tp"),
        check_vma=False,
    )
```

time: 352 us -> 240 us (0.68)
  blocking collectives: 95.5 us -> 0 us
  starting transfers between devices: 7.35 us -> 70.3 us
  waiting for transfers between devices: 149 us -> 102 us
  local copies, waits for them, and re-layouts: 47 us -> 19.2 us
  loops' own time: 10.5 us -> 0 us
  matrix products: 13.6 us -> 22 us
    all_gather x2 -> x0, waiting for transfers between devices: 112 us -> none  [the longest x1 67.8 us: body(): inputs = lax.all_gather(arrived, 'tp', axis=1, tiled=True)]
    ppermute x1 -> x53, waiting for transfers between devices: 0.01 us -> 102 us  [swap_with(): return lax.ppermute(part, axis, [(i, i ^ bits) for i in range(size)])]
    ppermute x1 -> x53, starting transfers between devices: 2.39 us -> 70.3 us  [swap_with(): return lax.ppermute(part, axis, [(i, i ^ bits) for i in range(size)])]
    all_to_all x1 -> x0, blocking collectives: 40.9 us -> none  [body(): lax.all_to_all(outgoing, 'sp', split_axis=0, concat_axis=0, tiled=True)]
    all_to_all x1 -> x0, waiting for transfers between devices: 37 us -> none  [body(): lax.all_to_all(result.astype(jnp.bfloat16), 'sp', split_axis=0, concat_ax...]
    all_gather x2 -> x0, blocking collectives: 22.5 us -> none  [the longest x1 13 us: entering(): everything = jax.tree.map(lambda part: lax.all_gather(part, axis), shard)]
    scatter x1 -> x0, local copies, waits for them, and re-layouts: 21.4 us -> none  [body(): outgoing = jnp.zeros((experts * slots_per, normed.shape[1]), jnp.bfloat16...]
    psum x2 -> x0, blocking collectives: 18.1 us -> none  [the longest x1 9.2 us: body(): lax.psum((jnp.sum(mixed_rows, axis=1), jnp.sum(mixed_rows * mixed_rows, a...]
  transfers between devices with their start and end apart: 4 -> 53, of which waited for: 3 -> 21; matrix products, arithmetic and copies ran while one was open for 2% -> 21% of each run, Pallas kernels for 0% -> 0%
where the time goes in v1:
time: 240 us; the launch traced here: 239 us
  waiting for transfers between devices  102 us (42%)
  starting transfers between devices  70.3 us (29%)
  matrix products  22 us (9%)
  local copies, waits for them, and re-layouts  19.2 us (8%)
  between operations  14 us (6%)
  other arithmetic  11.7 us (5%)
    ppermute x53, waiting for transfers between devices, swap_with(): return lax.ppermute(part, axis, [(i, i ^ bits) for i in range(size)])  102 us
    ppermute x53, starting transfers between devices, swap_with(): return lax.ppermute(part, axis, [(i, i ^ bits) for i in range(size)])  70.3 us
    unnamed x40, local copies, waits for them, and re-layouts  7.68 us
    dot_general x4, matrix products, body(): gate_part = jnp.dot(inputs, gate_w[k], preferred_element_type=F32)  7.53 us
    dot_general x4, matrix products, body(): result = jnp.dot(hidden, down_w[k], preferred_element_type=F32)  6.47 us
  transfers between devices with their start and end apart: 53, of which 21 were waited for; matrix products, arithmetic and copies ran while one was open for 21% of the time, Pallas kernels for 0%

profile of v1, /device:TPU:0, one launch (start us, length us, event | category | flops | bytes accessed | tf_op | source)
XLA Modules:
  0.0 239.0 jit_solution(13385377653593498613)
XLA Ops:
  0.9 3.0 %collective-permute-start.10 = (f32[4,512]{1,0:T(4,128)S(1)}, f32[4,512]{1,0:T(4,128)S(1)}, u32[]{:S(2)}, u32[]{:S(2)}) collective-permute-start(f32[4,512]{1,0:T(4,128)S(1)} %pad_maximum_fusion.10), channel_id=1, source_target_pairs={{0,1},{1,0},{2,3},{3,2},{4,5},{5,4},{6,7},{7,6},{8,9},{9,8},{10,11... | collective-permute-start | bytes 24584 | tf_op jit(solution)/shard_map/ppermute | solution.py:17
  23.1 2.6 %collective-permute-start.2 = (f32[2,21,128]{2,1,0:T(8,128)S(1)}, f32[2,21,128]{2,1,0:T(8,128)S(1)}, u32[]{:S(2)}, u32[]{:S(2)}) collective-permute-start(f32[2,21,128]{2,1,0:T(8,128)S(1)} %pad_maximum_fusion.9), channel_id=1, source_target_pairs={{0,16},{4,20},{8,24},{12,28},{16,0},{20,4},{24,8},{28,12},{1,17},{... | collective-permute-start | bytes 64520 | tf_op jit(solution)/shard_map/ppermute | solution.py:17
  57.7 10.0 %collective-permute-done.9 = f32[96,512]{1,0:T(8,128)S(1)} collective-permute-done((f32[96,512]{1,0:T(8,128)S(1)}, f32[96,512]{1,0:T(8,128)S(1)}, u32[]{:S(2)}, u32[]{:S(2)}) %collective-permute-start.9) | collective-permute-done | bytes 196640 | tf_op jit(solution)/shard_map/ppermute | solution.py:17
  68.5 4.9 %collective-permute-done.7 = f32[96,512]{1,0:T(8,128)S(1)} collective-permute-done((f32[96,512]{1,0:T(8,128)S(1)}, f32[96,512]{1,0:T(8,128)S(1)}, u32[]{:S(2)}, u32[]{:S(2)}) %collective-permute-start.7) | collective-permute-done | bytes 196640 | tf_op jit(solution)/shard_map/ppermute | solution.py:17
  74.9 3.2 %collective-permute-start.14 = (bf16[96,2048]{1,0:T(8,128)(2,1)}, bf16[96,2048]{1,0:T(8,128)(2,1)}, u32[]{:S(2)}, u32[]{:S(2)}) collective-permute-start(bf16[96,2048]{1,0:T(8,128)(2,1)} %get-tuple-element.73), channel_id=1, source_target_pairs={{0,16},{4,20},{8,24},{12,28},{16,0},{20,4},{24,8},{28,12},{1,17},{... | collective-permute-start | bytes 1179656 | tf_op jit(solution)/shard_map/ppermute | solution.py:17
  78.9 11.4 %collective-permute-done.13 = bf16[96,2048]{1,0:T(8,128)(2,1)} collective-permute-done((bf16[96,2048]{1,0:T(8,128)(2,1)}, bf16[96,2048]{1,0:T(8,128)(2,1)}, u32[]{:S(2)}, u32[]{:S(2)}) %collective-permute-start.13) | collective-permute-done | bytes 393248 | tf_op jit(solution)/shard_map/ppermute | solution.py:17
  95.5 6.9 %collective-permute-done.15 = bf16[96,2048]{1,0:T(8,128)(2,1)S(1)} collective-permute-done((bf16[96,2048]{1,0:T(8,128)(2,1)}, bf16[96,2048]{1,0:T(8,128)(2,1)S(1)}, u32[]{:S(2)}, u32[]{:S(2)}) %collective-permute-start.15) | collective-permute-done | bytes 393248 | tf_op jit(solution)/shard_map/ppermute | solution.py:17
  112.9 3.1 %fusion.116 = f32[768,256]{0,1:T(8,128)S(1)} fusion(bf16[768,2048]{1,0:T(8,128)(2,1)} %constant_dynamic-update-slice_fusion, bf16[1,2048,256]{2,1,0:T(8,128)(2,1)S(1)} %copy-done.1), kind=kOutput, calls=%fused_computation.242 | convolution fusion | flops 805306368 | bytes 4980736 | tf_op jit(solution)/shard_map/dot_general | solution.py:224
  118.7 24.4 %collective-permute-done.25 = bf16[1024,256]{1,0:T(8,128)(2,1)S(1)} collective-permute-done((bf16[1024,256]{1,0:T(8,128)(2,1)S(1)}, bf16[1024,256]{1,0:T(8,128)(2,1)S(1)}, u32[]{:S(2)}, u32[]{:S(2)}) %collective-permute-start.25) | collective-permute-done | bytes 524320 | tf_op jit(solution)/shard_map/ppermute | solution.py:17
  144.6 9.8 %collective-permute-done.24 = bf16[1024,256]{1,0:T(8,128)(2,1)S(1)} collective-permute-done((bf16[1024,256]{1,0:T(8,128)(2,1)S(1)}, bf16[1024,256]{1,0:T(8,128)(2,1)S(1)}, u32[]{:S(2)}, u32[]{:S(2)}) %collective-permute-start.24) | collective-permute-done | bytes 524320 | tf_op jit(solution)/shard_map/ppermute | solution.py:17
  158.6 2.1 fusion.11
  161.9 3.6 %collective-permute-done.27 = bf16[1024,256]{1,0:T(8,128)(2,1)S(1)} collective-permute-done((bf16[1024,256]{1,0:T(8,128)(2,1)}, bf16[1024,256]{1,0:T(8,128)(2,1)S(1)}, u32[]{:S(2)}, u32[]{:S(2)}) %collective-permute-start.27) | collective-permute-done | bytes 524320 | tf_op jit(solution)/shard_map/ppermute | solution.py:17
  167.4 8.2 %collective-permute-done.26 = bf16[1024,256]{1,0:T(8,128)(2,1)S(1)} collective-permute-done((bf16[1024,256]{1,0:T(8,128)(2,1)S(1)}, bf16[1024,256]{1,0:T(8,128)(2,1)S(1)}, u32[]{:S(2)}, u32[]{:S(2)}) %collective-permute-start.26) | collective-permute-done | bytes 524320 | tf_op jit(solution)/shard_map/ppermute | solution.py:17
  183.9 2.2 multiply_convert_fusion.2
  186.7 2.2 multiply_convert_fusion.1
  189.2 5.2 %collective-permute-start.33 = (bf16[96,512]{1,0:T(8,128)(2,1)S(1)}, bf16[96,512]{1,0:T(8,128)(2,1)S(1)}, u32[]{:S(2)}, u32[]{:S(2)}) collective-permute-start(bf16[96,512]{1,0:T(8,128)(2,1)S(1)} %get-tuple-element.65), channel_id=1, source_target_pairs={{0,24},{4,28},{8,16},{12,20},{16,8},{20,12},{24,0},{28,4},{1,25},{... | collective-permute-start | bytes 294920 | tf_op jit(solution)/shard_map/ppermute | solution.py:17
  196.1 4.2 %collective-permute-start.42 = (bf16[96,512]{1,0:T(8,128)(2,1)S(1)}, bf16[96,512]{1,0:T(8,128)(2,1)S(1)}, u32[]{:S(2)}, u32[]{:S(2)}) collective-permute-start(bf16[96,512]{1,0:T(8,128)(2,1)S(1)} %get-tuple-element.69), channel_id=1, source_target_pairs={{0,16},{4,20},{8,24},{12,28},{16,0},{20,4},{24,8},{28,12},{1,17},{... | collective-permute-start | bytes 294920 | tf_op jit(solution)/shard_map/ppermute | solution.py:17
  201.8 7.2 %collective-permute-start.32 = (bf16[96,512]{1,0:T(8,128)(2,1)S(1)}, bf16[96,512]{1,0:T(8,128)(2,1)S(1)}, u32[]{:S(2)}, u32[]{:S(2)}) collective-permute-start(bf16[96,512]{1,0:T(8,128)(2,1)S(1)} %get-tuple-element.66), channel_id=1, source_target_pairs={{0,16},{4,20},{8,24},{12,28},{16,0},{20,4},{24,8},{28,12},{1,17},{... | collective-permute-start | bytes 294920 | tf_op jit(solution)/shard_map/ppermute | solution.py:17
  209.8 2.2 collective-permute-start.38
  214.7 2.2 collective-permute-start.49
  218.2 3.5 %collective-permute-start.47 = (bf16[96,512]{1,0:T(8,128)(2,1)S(1)}, bf16[96,512]{1,0:T(8,128)(2,1)S(1)}, u32[]{:S(2)}, u32[]{:S(2)}) collective-permute-start(bf16[96,512]{1,0:T(8,128)(2,1)S(1)} %get-tuple-element.70), channel_id=1, source_target_pairs={{0,8},{4,12},{8,0},{12,4},{16,24},{20,28},{24,16},{28,20},{1,9},{5... | collective-permute-start | bytes 294920 | tf_op jit(solution)/shard_map/ppermute | solution.py:17
  221.9 5.6 %collective-permute-done.37 = bf16[96,512]{1,0:T(8,128)(2,1)S(1)} collective-permute-done((bf16[96,512]{1,0:T(8,128)(2,1)S(1)}, bf16[96,512]{1,0:T(8,128)(2,1)S(1)}, u32[]{:S(2)}, u32[]{:S(2)}) %collective-permute-start.37) | collective-permute-done | bytes 98336 | tf_op jit(solution)/shard_map/ppermute | solution.py:17
  227.5 3.5 %collective-permute-done.48 = bf16[96,512]{1,0:T(8,128)(2,1)S(1)} collective-permute-done((bf16[96,512]{1,0:T(8,128)(2,1)S(1)}, bf16[96,512]{1,0:T(8,128)(2,1)S(1)}, u32[]{:S(2)}, u32[]{:S(2)}) %collective-permute-start.48) | collective-permute-done | bytes 98336 | tf_op jit(solution)/shard_map/ppermute | solution.py:17
  235.1 2.7 %collective-permute-done.52 = bf16[96,512]{1,0:T(8,128)(2,1)S(1)} collective-permute-done((bf16[96,512]{1,0:T(8,128)(2,1)S(1)}, bf16[96,512]{1,0:T(8,128)(2,1)S(1)}, u32[]{:S(2)}, u32[]{:S(2)}) %collective-permute-start.52) | collective-permute-done | bytes 98336 | tf_op jit(solution)/shard_map/ppermute | solution.py:17
  (238 shorter events, 90.9 us)
Async XLA Ops:
  0.9 20.9 %collective-permute-start.10 = (f32[4,512]{1,0:T(4,128)S(1)}, f32[4,512]{1,0:T(4,128)S(1)}, u32[]{:S(2)}, u32[]{:S(2)}) collective-permute-start(f32[4,512]{1,0:T(4,128)S(1)} %pad_maximum_fusion.10), channel_id=1, source_target_pairs={{0,1},{1,0},{2,3},{3,2},{4,5},{5,4},{6,7},{7,6},{8,9},{9,8},{10,11... | collective-permute-start | bytes 24584 | tf_op jit(solution)/shard_map/ppermute | solution.py:17
  3.9 18.0 %collective-permute-start.11 = (f32[4,512]{1,0:T(4,128)S(1)}, f32[4,512]{1,0:T(4,128)S(1)}, u32[]{:S(2)}, u32[]{:S(2)}) collective-permute-start(f32[4,512]{1,0:T(4,128)S(1)} %pad_maximum_fusion.10), channel_id=1, source_target_pairs={{0,2},{1,3},{2,0},{3,1},{4,6},{5,7},{6,4},{7,5},{8,10},{9,11},{10,... | collective-permute-start | bytes 24584 | tf_op jit(solution)/shard_map/ppermute | solution.py:17
  5.5 16.5 %collective-permute-start.12 = (f32[4,512]{1,0:T(4,128)S(1)}, f32[4,512]{1,0:T(4,128)S(1)}, u32[]{:S(2)}, u32[]{:S(2)}) collective-permute-start(f32[4,512]{1,0:T(4,128)S(1)} %pad_maximum_fusion.10), channel_id=1, source_target_pairs={{0,3},{1,2},{2,1},{3,0},{4,7},{5,6},{6,5},{7,4},{8,11},{9,10},{10,... | collective-permute-start | bytes 24584 | tf_op jit(solution)/shard_map/ppermute | solution.py:17
  5.5 100.3 %collective-permute-start.34 = (bf16[1024,512]{1,0:T(8,128)(2,1)}, bf16[1024,512]{1,0:T(8,128)(2,1)}, u32[]{:S(2)}, u32[]{:S(2)}) collective-permute-start(bf16[1024,512]{1,0:T(8,128)(2,1)} %bitcast.244), channel_id=1, source_target_pairs={{0,1},{1,0},{2,3},{3,2},{4,5},{5,4},{6,7},{7,6},{8,9},{9,8},{10,11... | collective-permute-start | bytes 3145736 | tf_op jit(solution)/shard_map/ppermute | solution.py:17
  7.4 97.1 %collective-permute-start.39 = (bf16[1024,512]{1,0:T(8,128)(2,1)}, bf16[1024,512]{1,0:T(8,128)(2,1)}, u32[]{:S(2)}, u32[]{:S(2)}) collective-permute-start(bf16[1024,512]{1,0:T(8,128)(2,1)} %bitcast.245), channel_id=1, source_target_pairs={{0,2},{1,3},{2,0},{3,1},{4,6},{5,7},{6,4},{7,5},{8,10},{9,11},{10,... | collective-permute-start | bytes 3145736 | tf_op jit(solution)/shard_map/ppermute | solution.py:17
  51.3 64.7 %collective-permute-start.21 = (bf16[1024,256]{1,0:T(8,128)(2,1)}, bf16[1024,256]{1,0:T(8,128)(2,1)}, u32[]{:S(2)}, u32[]{:S(2)}) collective-permute-start(bf16[1024,256]{1,0:T(8,128)(2,1)} %get-tuple-element.53), channel_id=1, source_target_pairs={{0,1},{1,0},{2,3},{3,2},{4,5},{5,4},{6,7},{7,6},{8,9},{9,8},{10,11... | collective-permute-start | bytes 1572872 | tf_op jit(solution)/shard_map/ppermute | solution.py:17
  74.8 15.5 %collective-permute-start.13 = (bf16[96,2048]{1,0:T(8,128)(2,1)}, bf16[96,2048]{1,0:T(8,128)(2,1)}, u32[]{:S(2)}, u32[]{:S(2)}) collective-permute-start(bf16[96,2048]{1,0:T(8,128)(2,1)} %get-tuple-element.73), channel_id=1, source_target_pairs={{0,8},{4,12},{8,0},{12,4},{16,24},{20,28},{24,16},{28,20},{1,9},{5... | collective-permute-start | bytes 1179656 | tf_op jit(solution)/shard_map/ppermute | solution.py:17
  74.9 18.8 %collective-permute-start.14 = (bf16[96,2048]{1,0:T(8,128)(2,1)}, bf16[96,2048]{1,0:T(8,128)(2,1)}, u32[]{:S(2)}, u32[]{:S(2)}) collective-permute-start(bf16[96,2048]{1,0:T(8,128)(2,1)} %get-tuple-element.73), channel_id=1, source_target_pairs={{0,16},{4,20},{8,24},{12,28},{16,0},{20,4},{24,8},{28,12},{1,17},{... | collective-permute-start | bytes 1179656 | tf_op jit(solution)/shard_map/ppermute | solution.py:17
  104.5 13.8 %collective-permute-start.20 = (bf16[1024,256]{1,0:T(8,128)(2,1)S(1)}, bf16[1024,256]{1,0:T(8,128)(2,1)S(1)}, u32[]{:S(2)}, u32[]{:S(2)}) collective-permute-start(bf16[1024,256]{1,0:T(8,128)(2,1)S(1)} %copy-done.5), channel_id=1, source_target_pairs={{0,1},{1,0},{2,3},{3,2},{4,5},{5,4},{6,7},{7,6},{8,9},{9,8},{10,11... | collective-permute-start | bytes 1572872 | tf_op jit(solution)/shard_map/ppermute | solution.py:17
  105.8 50.4 %collective-permute-start.23 = (bf16[2048,256]{1,0:T(8,128)(2,1)S(1)}, bf16[2048,256]{1,0:T(8,128)(2,1)S(1)}, u32[]{:S(2)}, u32[]{:S(2)}) collective-permute-start(bf16[2048,256]{1,0:T(8,128)(2,1)S(1)} %bitcast.207), channel_id=1, source_target_pairs={{0,2},{1,3},{2,0},{3,1},{4,6},{5,7},{6,4},{7,5},{8,10},{9,11},{10,... | collective-permute-start | bytes 3145736 | tf_op jit(solution)/shard_map/ppermute | solution.py:17
  109.3 33.9 %collective-permute-start.25 = (bf16[1024,256]{1,0:T(8,128)(2,1)S(1)}, bf16[1024,256]{1,0:T(8,128)(2,1)S(1)}, u32[]{:S(2)}, u32[]{:S(2)}) collective-permute-start(bf16[1024,256]{1,0:T(8,128)(2,1)S(1)} %copy-done.4), channel_id=1, source_target_pairs={{0,2},{1,3},{2,0},{3,1},{4,6},{5,7},{6,4},{7,5},{8,10},{9,11},{10,... | collective-permute-start | bytes 1572872 | tf_op jit(solution)/shard_map/ppermute | solution.py:17
  110.6 43.7 %collective-permute-start.24 = (bf16[1024,256]{1,0:T(8,128)(2,1)S(1)}, bf16[1024,256]{1,0:T(8,128)(2,1)S(1)}, u32[]{:S(2)}, u32[]{:S(2)}) collective-permute-start(bf16[1024,256]{1,0:T(8,128)(2,1)S(1)} %copy-done.3), channel_id=1, source_target_pairs={{0,2},{1,3},{2,0},{3,1},{4,6},{5,7},{6,4},{7,5},{8,10},{9,11},{10,... | collective-permute-start | bytes 1572872 | tf_op jit(solution)/shard_map/ppermute | solution.py:17
  115.9 62.4 %collective-permute-start.22 = (bf16[2048,256]{1,0:T(8,128)(2,1)S(1)}, bf16[2048,256]{1,0:T(8,128)(2,1)S(1)}, u32[]{:S(2)}, u32[]{:S(2)}) collective-permute-start(bf16[2048,256]{1,0:T(8,128)(2,1)S(1)} %bitcast.208), channel_id=1, source_target_pairs={{0,1},{1,0},{2,3},{3,2},{4,5},{5,4},{6,7},{7,6},{8,9},{9,8},{10,11... | collective-permute-start | bytes 3145736 | tf_op jit(solution)/shard_map/ppermute | solution.py:17
  118.3 47.2 %collective-permute-start.27 = (bf16[1024,256]{1,0:T(8,128)(2,1)}, bf16[1024,256]{1,0:T(8,128)(2,1)S(1)}, u32[]{:S(2)}, u32[]{:S(2)}) collective-permute-start(bf16[1024,256]{1,0:T(8,128)(2,1)} %collective-permute-done.21), channel_id=1, source_target_pairs={{0,2},{1,3},{2,0},{3,1},{4,6},{5,7},{6,4},{7,5},{8,10},{9,11},{10,... | collective-permute-start | bytes 1572872 | tf_op jit(solution)/shard_map/ppermute | solution.py:17
  143.1 32.6 %collective-permute-start.26 = (bf16[1024,256]{1,0:T(8,128)(2,1)S(1)}, bf16[1024,256]{1,0:T(8,128)(2,1)S(1)}, u32[]{:S(2)}, u32[]{:S(2)}) collective-permute-start(bf16[1024,256]{1,0:T(8,128)(2,1)S(1)} %collective-permute-done.20), channel_id=1, source_target_pairs={{0,2},{1,3},{2,0},{3,1},{4,6},{5,7},{6,4},{7,5},{8,10},{9,11},{10,... | collective-permute-start | bytes 1572872 | tf_op jit(solution)/shard_map/ppermute | solution.py:17
  154.3 25.1 %collective-permute-start.29 = (bf16[1024,256]{1,0:T(8,128)(2,1)S(1)}, bf16[1024,256]{1,0:T(8,128)(2,1)S(1)}, u32[]{:S(2)}, u32[]{:S(2)}) collective-permute-start(bf16[1024,256]{1,0:T(8,128)(2,1)S(1)} %collective-permute-done.25), channel_id=1, source_target_pairs={{0,1},{1,0},{2,3},{3,2},{4,5},{5,4},{6,7},{7,6},{8,9},{9,8},{10,11... | collective-permute-start | bytes 1572872 | tf_op jit(solution)/shard_map/ppermute | solution.py:17
  156.2 24.2 %collective-permute-start.28 = (bf16[1024,256]{1,0:T(8,128)(2,1)S(1)}, bf16[1024,256]{1,0:T(8,128)(2,1)S(1)}, u32[]{:S(2)}, u32[]{:S(2)}) collective-permute-start(bf16[1024,256]{1,0:T(8,128)(2,1)S(1)} %collective-permute-done.24), channel_id=1, source_target_pairs={{0,1},{1,0},{2,3},{3,2},{4,5},{5,4},{6,7},{7,6},{8,9},{9,8},{10,11... | collective-permute-start | bytes 1572872 | tf_op jit(solution)/shard_map/ppermute | solution.py:17
  165.6 34.9 %collective-permute-start.45 = (bf16[512,512]{1,0:T(8,128)(2,1)S(1)}, bf16[512,512]{1,0:T(8,128)(2,1)S(1)}, u32[]{:S(2)}, u32[]{:S(2)}) collective-permute-start(bf16[512,512]{1,0:T(8,128)(2,1)S(1)} %slice.581), channel_id=1, source_target_pairs={{0,1},{1,0},{2,3},{3,2},{4,5},{5,4},{6,7},{7,6},{8,9},{9,8},{10,11... | collective-permute-start | bytes 1572872 | tf_op jit(solution)/shard_map/ppermute | solution.py:17
  175.7 24.9 %collective-permute-start.44 = (bf16[512,512]{1,0:T(8,128)(2,1)S(1)}, bf16[512,512]{1,0:T(8,128)(2,1)S(1)}, u32[]{:S(2)}, u32[]{:S(2)}) collective-permute-start(bf16[512,512]{1,0:T(8,128)(2,1)S(1)} %slice.580), channel_id=1, source_target_pairs={{0,2},{1,3},{2,0},{3,1},{4,6},{5,7},{6,4},{7,5},{8,10},{9,11},{10,... | collective-permute-start | bytes 1572872 | tf_op jit(solution)/shard_map/ppermute | solution.py:17
  189.2 24.5 %collective-permute-start.33 = (bf16[96,512]{1,0:T(8,128)(2,1)S(1)}, bf16[96,512]{1,0:T(8,128)(2,1)S(1)}, u32[]{:S(2)}, u32[]{:S(2)}) collective-permute-start(bf16[96,512]{1,0:T(8,128)(2,1)S(1)} %get-tuple-element.65), channel_id=1, source_target_pairs={{0,24},{4,28},{8,16},{12,20},{16,8},{20,12},{24,0},{28,4},{1,25},{... | collective-permute-start | bytes 294920 | tf_op jit(solution)/shard_map/ppermute | solution.py:17
  196.1 13.7 %collective-permute-start.42 = (bf16[96,512]{1,0:T(8,128)(2,1)S(1)}, bf16[96,512]{1,0:T(8,128)(2,1)S(1)}, u32[]{:S(2)}, u32[]{:S(2)}) collective-permute-start(bf16[96,512]{1,0:T(8,128)(2,1)S(1)} %get-tuple-element.69), channel_id=1, source_target_pairs={{0,16},{4,20},{8,24},{12,28},{16,0},{20,4},{24,8},{28,12},{1,17},{... | collective-permute-start | bytes 294920 | tf_op jit(solution)/shard_map/ppermute | solution.py:17
  212.2 15.3 %collective-permute-start.37 = (bf16[96,512]{1,0:T(8,128)(2,1)S(1)}, bf16[96,512]{1,0:T(8,128)(2,1)S(1)}, u32[]{:S(2)}, u32[]{:S(2)}) collective-permute-start(bf16[96,512]{1,0:T(8,128)(2,1)S(1)} %get-tuple-element.63), channel_id=1, source_target_pairs={{0,16},{4,20},{8,24},{12,28},{16,0},{20,4},{24,8},{28,12},{1,17},{... | collective-permute-start | bytes 294920 | tf_op jit(solution)/shard_map/ppermute | solution.py:17
  213.7 13.8 %collective-permute-start.36 = (bf16[96,512]{1,0:T(8,128)(2,1)S(1)}, bf16[96,512]{1,0:T(8,128)(2,1)S(1)}, u32[]{:S(2)}, u32[]{:S(2)}) collective-permute-start(bf16[96,512]{1,0:T(8,128)(2,1)S(1)} %get-tuple-element.61), channel_id=1, source_target_pairs={{0,8},{4,12},{8,0},{12,4},{16,24},{20,28},{24,16},{28,20},{1,9},{5... | collective-permute-start | bytes 294920 | tf_op jit(solution)/shard_map/ppermute | solution.py:17
  216.9 14.1 %collective-permute-start.48 = (bf16[96,512]{1,0:T(8,128)(2,1)S(1)}, bf16[96,512]{1,0:T(8,128)(2,1)S(1)}, u32[]{:S(2)}, u32[]{:S(2)}) collective-permute-start(bf16[96,512]{1,0:T(8,128)(2,1)S(1)} %get-tuple-element.72), channel_id=1, source_target_pairs={{0,16},{4,20},{8,24},{12,28},{16,0},{20,4},{24,8},{28,12},{1,17},{... | collective-permute-start | bytes 294920 | tf_op jit(solution)/shard_map/ppermute | solution.py:17
  (46 other events, 633.4 us)

commit v2 on v1

--- a/solution.py
+++ b/solution.py
@@ -1,6 +1,8 @@
 import jax
 import jax.numpy as jnp
 from jax import lax
+from jax.experimental import pallas as pl
+from jax.experimental.pallas import tpu as pltpu
 from jax.sharding import PartitionSpec as P
 
 
@@ -33,6 +35,141 @@
     size = lax.axis_size(axis)
     mine = [part] + [swap_with(part, axis, 2 * k) for k in range(1, size // 2)]
     return mine + [swap_with(m, axis, 1) for m in mine]
+
+
+TABLE = HALO + 8
+
+
+def table_kernel(x_ref, docs_ref, table_ref, start_ref):
+    channels, positions = x_ref.shape
+    docs = jnp.broadcast_to(docs_ref[...], (8, positions))
+    lane = lax.broadcasted_iota(jnp.int32, (8, positions), 1)
+    opens = (docs != pltpu.roll(docs, 1, 1)) & (lane > 0)
+    start = jnp.where(opens, lane, 0)
+    step = 1
+    while step < positions:
+        moved = pltpu.roll(start, step, 1)
+        start = jnp.maximum(start, jnp.where(lane >= step, moved, 0))
+        step *= 2
+    start_ref[...] = start
+    last_start = start[:1, positions - 1 :]
+    last_doc = docs[:1, positions - 1 :]
+    row = lax.broadcasted_iota(jnp.int32, (TABLE, positions), 0)
+    col = lax.broadcasted_iota(jnp.int32, (TABLE, positions), 1)
+    pick = ((row < HALO) & (col == positions - HALO + row)) | (
+        (row == HALO) & (col >= last_start)
+    )
+    got = lax.dot_general(
+        pick.astype(BF16), x_ref[...], (((1,), (1,)), ((), ())), preferred_element_type=F32
+    )
+    row = lax.broadcasted_iota(jnp.int32, (TABLE, channels), 0)
+    got = jnp.where(row == HALO + 1, last_doc.astype(F32), got)
+    table_ref[...] = jnp.where(row == HALO + 2, (positions - last_start).astype(F32), got)
+
+
+def units_of(channels, j):
+    unit = min(GROUP_W, channels)
+    for u in range(channels // unit):
+        group = (j * channels + u * unit) // GROUP_W
+        yield slice(u * unit, (u + 1) * unit), group % 2 == 1, lax.shift_left(2, group // 2 % 4)
+
+
+def local_kernel(place_ref, x_ref, start_ref, sum_ref):
+    channels, positions = x_ref.shape
+    s_at = lax.broadcasted_iota(jnp.int32, (positions, positions), 0)
+    t_at = lax.broadcasted_iota(jnp.int32, (positions, positions), 1)
+    for rows, whole_doc, window in units_of(channels, place_ref[1]):
+        reach = jnp.where(whole_doc, positions, window)
+        lower = jnp.maximum(start_ref[:1, :], t_at[:1, :] + 1 - reach)
+        mask = (s_at >= lower) & (s_at <= t_at)
+        sum_ref[rows, :] = jnp.dot(
+            x_ref[rows, :], mask.astype(BF16), preferred_element_type=F32
+        )
+
+
+def pooled_kernel(place_ref, x_ref, docs_ref, start_ref, sum_ref, *rest):
+    *table_refs, out_ref = rest
+    channels, positions = x_ref.shape
+    i, j = place_ref[0], place_ref[1]
+    first_doc = docs_ref[:1, :1].astype(F32)
+    before = jnp.zeros((TABLE, channels), F32)
+    carried = jnp.zeros((TABLE, channels), F32)
+    for k in range(1, 2 * len(table_refs)):
+        table = table_refs[k // 2][k % 2]
+        earlier = jnp.where((i ^ k) < i, 1.0, 0.0)
+        previous = jnp.where((i ^ k) == i - 1, 1.0, 0.0)
+        same = jnp.where(table[HALO + 1 : HALO + 2, :1] == first_doc, earlier, 0.0)
+        carried = carried + same * table
+        before = before + previous * table
+    count = carried[HALO + 2 : HALO + 3, :1]
+    t_at = lax.broadcasted_iota(jnp.int32, (1, positions), 1)
+    start = start_ref[:1, :]
+    in_first = jnp.where(start == 0, 1.0, 0.0)
+    doc_count = (t_at + 1 - start).astype(F32) + in_first * count
+    row = lax.broadcasted_iota(jnp.int32, (TABLE, channels), 0)
+    carry_row = jnp.where(row == HALO, carried, 0.0)
+    over_first = jnp.broadcast_to(in_first, (TABLE, positions))
+    carry = lax.dot_general(
+        carry_row,
+        over_first,
+        (((0,), (0,)), ((), ())),
+        precision=lax.Precision.HIGHEST,
+        preferred_element_type=F32,
+    )
+    h_at = lax.broadcasted_iota(jnp.int32, (TABLE, positions), 0) - HALO
+    reached = jnp.where(h_at.astype(F32) >= -count, over_first, 0.0)
+    reached = jnp.where(h_at < 0, reached, 0.0)
+    for rows, whole_doc, window in units_of(channels, j):
+        halo_mask = jnp.where(h_at >= t_at + 1 - window, reached, 0.0)
+        halo = lax.dot_general(
+            before.astype(BF16),
+            halo_mask.astype(BF16),
+            (((0,), (0,)), ((), ())),
+            preferred_element_type=F32,
+        )
+        whole = jnp.where(whole_doc, 1.0, 0.0)
+        total = sum_ref[rows, :] + whole * carry[rows] + (1.0 - whole) * halo[rows]
+        most = jnp.where(whole_doc, float(1 << 30), window.astype(F32))
+        total = total / jnp.minimum(doc_count, most)
+        out_ref[rows, :] = (total - x_ref[rows, :].astype(F32)).astype(BF16)
+
+
+def in_vmem(count):
+    return [pl.BlockSpec(memory_space=pltpu.VMEM)] * count
+
+
+def pooled_channels(pool_in, doc_ids, place):
+    channels, positions = pool_in.shape
+    docs = doc_ids.reshape(1, positions)
+    scalars = pl.BlockSpec(memory_space=pltpu.SMEM)
+    table, start = pl.pallas_call(
+        table_kernel,
+        out_shape=(
+            jax.ShapeDtypeStruct((TABLE, channels), F32),
+            jax.ShapeDtypeStruct((8, positions), jnp.int32),
+        ),
+        in_specs=in_vmem(2),
+        out_specs=tuple(in_vmem(2)),
+        name="table",
+    )(pool_in, docs)
+    pair = jnp.stack([table, swap_with(table, "sp", 1)])
+    sums = pl.pallas_call(
+        local_kernel,
+        out_shape=jax.ShapeDtypeStruct((channels, positions), F32),
+        in_specs=[scalars] + in_vmem(2),
+        out_specs=in_vmem(1)[0],
+        name="local",
+    )(place, pool_in, start)
+    tables = [pair] + [
+        swap_with(pair, "sp", 2 * k) for k in range(1, lax.axis_size("sp") // 2)
+    ]
+    return pl.pallas_call(
+        pooled_kernel,
+        out_shape=jax.ShapeDtypeStruct((channels, positions), BF16),
+        in_specs=[scalars] + in_vmem(4 + len(tables)),
+        out_specs=in_vmem(1)[0],
+        name="pooled",
+    )(place, pool_in, docs, start, sums, *tables)
 
 
 def norm_rows(rows, features):
@@ -97,86 +234,12 @@
 ):
     sp, tp = lax.axis_size("sp"), lax.axis_size("tp")
     i, j = lax.axis_index("sp"), lax.axis_index("tp")
-    channels, positions = pool_in.shape
+    _, positions = pool_in.shape
     width = residual.shape[1]
     features = width * tp
     quarter = positions // tp
-    pairs = routes.shape[1]
-
-    docs = doc_ids.astype(F32)
-    values = pool_in.astype(F32)
-    ending = docs == docs[positions - 1]
-    tail_sum = jnp.sum(jnp.where(ending[None, :], values, 0.0), axis=1)
-    tail_count = jnp.sum(ending.astype(F32))
-    halo = values[:, positions - HALO :]
-    my_routes = lax.dynamic_slice_in_dim(routes, j * quarter, quarter, 0)
-    my_weights = lax.dynamic_slice_in_dim(route_weight, j * quarter, quarter, 0)
-    lead = jnp.concatenate([docs[positions - HALO :], tail_count[None]])
-    flat = jnp.concatenate(
-        [
-            tail_sum,
-            halo.reshape(-1),
-            lead,
-            my_routes.astype(F32).T.reshape(-1),
-            my_weights.T.reshape(-1),
-        ]
-    )
-    used = flat.shape[0]
-    rows = -(-used // 128)
-    flat = jnp.pad(flat, (0, rows * 128 - used)).reshape(rows, 128)
-    pair = jnp.stack([flat, swap_with(flat, "sp", 1)])
-    by_z = [pair] + [swap_with(pair, "sp", 2 * k) for k in range(1, sp // 2)]
-    rel = [by_z[k // 2][k % 2].reshape(-1)[:used] for k in range(sp)]
-
-    c1 = channels
-    c2 = c1 + channels * HALO
-    c3 = c2 + HALO + 1
-    c4 = c3 + pairs * quarter
-    carried_sum = jnp.zeros((channels,), F32)
-    carried_count = jnp.zeros((), F32)
-    prev = jnp.zeros((c3,), F32)
-    for k in range(1, sp):
-        source = i ^ k
-        same = (source < i) & (rel[k][c2 + HALO - 1] == docs[0])
-        carried_sum = carried_sum + jnp.where(same, rel[k][:c1], 0.0)
-        carried_count = carried_count + jnp.where(same, rel[k][c2 + HALO], 0.0)
-        prev = prev + jnp.where(source == i - 1, rel[k][:c3], 0.0)
-    halo_in = prev[c1:c2].reshape(channels, HALO).astype(BF16)
-    halo_docs = jnp.where(i == 0, -1.0, prev[c2 : c2 + HALO])
-
-    t_at = jnp.arange(positions, dtype=jnp.int32)
-    s_at = t_at[:, None]
-    same_doc = (docs[:, None] == docs[None, :]) & (s_at <= t_at[None, :])
-    local_count = jnp.sum(same_doc.astype(F32), axis=0)
-    in_first = docs == docs[0]
-    doc_count = local_count + jnp.where(in_first, carried_count, 0.0)
-    unit = min(GROUP_W, channels)
-    halo_at = jnp.arange(HALO, dtype=jnp.int32) - HALO
-    halo_same = halo_docs[:, None] == docs[None, :]
-    pooled_units = []
-    for u in range(channels // unit):
-        group = (j * channels + u * unit) // GROUP_W
-        whole_doc = group % 2 == 1
-        window = jnp.left_shift(2, group // 2 % 4)
-        mask = same_doc & (whole_doc | (s_at > t_at[None, :] - window))
-        here = pool_in[u * unit : (u + 1) * unit]
-        total = jnp.dot(here, mask.astype(BF16), preferred_element_type=F32)
-        halo_mask = halo_same & (halo_at[:, None] > t_at[None, :] - window) & ~whole_doc
-        total = total + jnp.dot(
-            halo_in[u * unit : (u + 1) * unit],
-            halo_mask.astype(BF16),
-            preferred_element_type=F32,
-        )
-        carry_here = carried_sum[u * unit : (u + 1) * unit]
-        total = total + jnp.where(
-            whole_doc & in_first[None, :], carry_here[:, None], 0.0
-        )
-        count = jnp.where(
-            whole_doc, doc_count, jnp.minimum(doc_count, window.astype(F32))
-        )
-        pooled_units.append(total / count[None, :] - here.astype(F32))
-    pooled = jnp.concatenate(pooled_units).astype(BF16)
-
+
+    pooled = pooled_channels(pool_in, doc_ids, jnp.stack([i, j]))
     pooled_rel = exchange_all(pooled, "tp")
     gathered = jnp.concatenate(in_order(pooled_rel, j))
     group_count = gathered.shape[0] // GROUP_W
@@ -195,10 +258,13 @@
     quarters = [
         lax.dynamic_slice_in_dim(mixed, (j ^ k) * quarter, quarter, 0) for k in range(tp)
     ]
-    mixed_rel = [quarters[0]] + [swap_with(quarters[k], "tp", k) for k in range(1, tp)]
-    gains = exchange_all(
-        jnp.stack([first_gain, first_bias, second_gain, second_bias]), "tp"
-    )
+    scales = jnp.pad(
+        jnp.stack([first_gain, first_bias, second_gain, second_bias]), ((0, 4), (0, 0))
+    )
+    both = [jnp.concatenate([q, scales]) for q in quarters]
+    both = [both[0]] + [swap_with(both[k], "tp", k) for k in range(1, tp)]
+    mixed_rel = [b[:quarter] for b in both]
+    gains = [b[quarter:] for b in both]
     normed_rel = [
         (r * gains[k][0] + gains[k][1]).astype(BF16)
         for k, r in enumerate(norm_rows(mixed_rel, features))
@@ -209,15 +275,12 @@
 
     everyone = line_gather(tokens, "sp")
     inputs = jnp.concatenate(everyone)
-    order = [2 * k for k in range(sp // 2)] + [2 * k + 1 for k in range(sp // 2)]
-    mine = i.astype(F32)
-    gate_cols = []
-    for k in order:
-        chosen = rel[k][c3:c4].reshape(pairs, quarter) == mine
-        gate_cols.append(
-            jnp.sum(jnp.where(chosen, rel[k][c4:].reshape(pairs, quarter), 0.0), axis=0)
-        )
-    share = jnp.concatenate(gate_cols)[:, None]
+    my_routes = lax.dynamic_slice_in_dim(routes, j * quarter, quarter, 0)
+    my_weights = lax.dynamic_slice_in_dim(route_weight, j * quarter, quarter, 0)
+    chosen = jnp.stack([my_routes.astype(F32).T, my_weights.T])
+    chosen = jnp.concatenate([c[None] for c in line_gather(chosen, "sp")])
+    chosen = jnp.where(chosen[:, 0] == i.astype(F32), chosen[:, 1], 0.0)
+    share = jnp.sum(chosen, axis=1).reshape(-1, 1)
 
     hidden_rel = []
     for k in range(tp):

time: 240 us -> 247 us (1.029)
  waiting for transfers between devices: 102 us -> 116 us
  between operations: 14 us -> 0.78 us
  Pallas kernels: 0 us -> 6.23 us
  starting transfers between devices: 70.3 us -> 75.7 us
  other arithmetic: 11.7 us -> 7.45 us
  matrix products: 22 us -> 19.4 us
    ppermute x53 -> x57, waiting for transfers between devices: 102 us -> 116 us  [swap_with(): return lax.ppermute(part, axis, [(i, i ^ bits) for i in range(size)])]
    pallas_call x0 -> x3, Pallas kernels: none -> 6.23 us  [the longest x1 2.28 us: pooled_channels(): pl.pallas_call(table_kernel, out_shape=(jax.ShapeDtypeStruct((TABLE, chan...]
    ppermute x53 -> x57, starting transfers between devices: 70.3 us -> 75.7 us  [swap_with(): return lax.ppermute(part, axis, [(i, i ^ bits) for i in range(size)])]
    slice x11 -> x0, local copies, waits for them, and re-layouts: 4.41 us -> none  [the longest x4 2.61 us: body(): carried_count = carried_count + jnp.where(same, rel[k][c2 + HALO], 0.0)]
    reduce_sum x11 -> x1, other arithmetic: 4.05 us -> 0.61 us  [body(): share = jnp.sum(chosen, axis=1).reshape(-1, 1)]
    dot_general x4 -> x0, matrix products: 2.63 us -> none  [the longest x2 2.2 us: body(): total = jnp.dot(here, mask.astype(BF16), preferred_element_type=F32)]
    unnamed x40 -> x64, local copies, waits for them, and re-layouts: 7.68 us -> 8.82 us
  transfers between devices with their start and end apart: 53 -> 57, of which waited for: 21 -> 20; matrix products, arithmetic and copies ran while one was open for 21% -> 18% of each run, Pallas kernels for 0% -> 3%
where the time goes in v2:
time: 247 us; the launch traced here: 246 us
  waiting for transfers between devices  116 us (47%)
  starting transfers between devices  75.7 us (31%)
  local copies, waits for them, and re-layouts  20.1 us (8%)
  matrix products  19.4 us (8%)
  other arithmetic  7.45 us (3%)
  Pallas kernels  6.23 us (3%)
    ppermute x57, waiting for transfers between devices, swap_with(): return lax.ppermute(part, axis, [(i, i ^ bits) for i in range(size)])  116 us
    ppermute x57, starting transfers between devices, swap_with(): return lax.ppermute(part, axis, [(i, i ^ bits) for i in range(size)])  75.7 us
    unnamed x64, local copies, waits for them, and re-layouts  8.82 us
    dot_general x4, matrix products, body(): gate_part = jnp.dot(inputs, gate_w[k], preferred_element_type=F32)  7.55 us
    dot_general x4, matrix products, body(): result = jnp.dot(hidden, down_w[k], preferred_element_type=F32)  6.54 us
  transfers between devices with their start and end apart: 57, of which 20 were waited for; matrix products, arithmetic and copies ran while one was open for 18% of the time, Pallas kernels for 3%

profile of v2, /device:TPU:0, one launch (start us, length us, event | category | flops | bytes accessed | tf_op | source)
XLA Modules:
  0.0 246.1 jit_solution(16998205294362076606)
XLA Ops:
  1.6 3.1 %collective-permute-start.27 = (f32[2,2,96]{2,1,0:T(2,128)S(1)}, f32[2,2,96]{2,1,0:T(2,128)S(1)}, u32[]{:S(2)}, u32[]{:S(2)}) collective-permute-start(f32[2,2,96]{2,1,0:T(2,128)S(1)} %pad_maximum_fusion.12), channel_id=1, source_target_pairs={{0,8},{4,12},{8,0},{12,4},{16,24},{20,28},{24,16},{28,20},{1,9},{5... | collective-permute-start | bytes 4616 | tf_op jit(solution)/shard_map/ppermute | solution.py:19
  4.7 2.6 %collective-permute-start.28 = (f32[2,2,96]{2,1,0:T(2,128)S(1)}, f32[2,2,96]{2,1,0:T(2,128)}, u32[]{:S(2)}, u32[]{:S(2)}) collective-permute-start(f32[2,2,96]{2,1,0:T(2,128)S(1)} %pad_maximum_fusion.12), channel_id=1, source_target_pairs={{0,16},{4,20},{8,24},{12,28},{16,0},{20,4},{24,8},{28,12},{1,17},{... | collective-permute-start | bytes 4616 | tf_op jit(solution)/shard_map/ppermute | solution.py:19
  8.5 2.3 table.1
  20.4 3.5 %collective-permute-start.2 = (f32[2,24,128]{2,1,0:T(8,128)S(1)}, f32[2,24,128]{2,1,0:T(8,128)S(1)}, u32[]{:S(2)}, u32[]{:S(2)}) collective-permute-start(f32[2,24,128]{2,1,0:T(8,128)S(1)} %pad_maximum_fusion.11.rest_0_), channel_id=1, source_target_pairs={{0,16},{4,20},{8,24},{12,28},{16,0},{20,4},{24,8},{28,12},{1,17},{... | collective-permute-start | bytes 73736 | tf_op jit(solution)/shard_map/ppermute | solution.py:19
  26.4 3.2 %collective-permute-done.3.rest_3_ = f32[2,24,128]{2,1,0:T(8,128)S(1)} collective-permute-done((f32[2,24,128]{2,1,0:T(8,128)S(1)}, f32[2,24,128]{2,1,0:T(8,128)S(1)}, u32[]{:S(2)}, u32[]{:S(2)}) %collective-permute-start.3) | collective-permute-done | bytes 24608 | tf_op jit(solution)/shard_map/ppermute | solution.py:19
  35.8 9.8 %collective-permute-done.4 = bf16[128,384]{1,0:T(8,128)(2,1)S(1)} collective-permute-done((bf16[128,384]{1,0:T(8,128)(2,1)}, bf16[128,384]{1,0:T(8,128)(2,1)S(1)}, u32[]{:S(2)}, u32[]{:S(2)}) %collective-permute-start.4) | collective-permute-done | bytes 98336 | tf_op jit(solution)/shard_map/ppermute | solution.py:19
  47.3 6.0 %collective-permute-done.5 = bf16[128,384]{1,0:T(8,128)(2,1)S(1)} collective-permute-done((bf16[128,384]{1,0:T(8,128)(2,1)}, bf16[128,384]{1,0:T(8,128)(2,1)S(1)}, u32[]{:S(2)}, u32[]{:S(2)}) %collective-permute-start.5) | collective-permute-done | bytes 98336 | tf_op jit(solution)/shard_map/ppermute | solution.py:19
  57.7 5.6 %collective-permute-done.7 = f32[104,512]{1,0:T(8,128)S(1)} collective-permute-done((f32[104,512]{1,0:T(8,128)S(1)}, f32[104,512]{1,0:T(8,128)S(1)}, u32[]{:S(2)}, u32[]{:S(2)}) %collective-permute-start.7) | collective-permute-done | bytes 213024 | tf_op jit(solution)/shard_map/ppermute | solution.py:19
  65.6 5.4 %collective-permute-done.9 = f32[104,512]{1,0:T(8,128)S(1)} collective-permute-done((f32[104,512]{1,0:T(8,128)S(1)}, f32[104,512]{1,0:T(8,128)S(1)}, u32[]{:S(2)}, u32[]{:S(2)}) %collective-permute-start.9) | collective-permute-done | bytes 213024 | tf_op jit(solution)/shard_map/ppermute | solution.py:19
  74.8 3.5 %collective-permute-start.11 = (bf16[96,2048]{1,0:T(8,128)(2,1)}, bf16[96,2048]{1,0:T(8,128)(2,1)}, u32[]{:S(2)}, u32[]{:S(2)}) collective-permute-start(bf16[96,2048]{1,0:T(8,128)(2,1)} %get-tuple-element.68), channel_id=1, source_target_pairs={{0,16},{4,20},{8,24},{12,28},{16,0},{20,4},{24,8},{28,12},{1,17},{... | collective-permute-start | bytes 1179656 | tf_op jit(solution)/shard_map/ppermute | solution.py:19
  79.7 14.5 %collective-permute-done.10 = bf16[96,2048]{1,0:T(8,128)(2,1)} collective-permute-done((bf16[96,2048]{1,0:T(8,128)(2,1)}, bf16[96,2048]{1,0:T(8,128)(2,1)}, u32[]{:S(2)}, u32[]{:S(2)}) %collective-permute-start.10) | collective-permute-done | bytes 393248 | tf_op jit(solution)/shard_map/ppermute | solution.py:19
  99.5 7.5 %collective-permute-done.12 = bf16[96,2048]{1,0:T(8,128)(2,1)S(1)} collective-permute-done((bf16[96,2048]{1,0:T(8,128)(2,1)}, bf16[96,2048]{1,0:T(8,128)(2,1)S(1)}, u32[]{:S(2)}, u32[]{:S(2)}) %collective-permute-start.12) | collective-permute-done | bytes 393248 | tf_op jit(solution)/shard_map/ppermute | solution.py:19
  118.3 3.1 %fusion.54 = f32[768,256]{0,1:T(8,128)S(1)} fusion(bf16[768,2048]{1,0:T(8,128)(2,1)} %constant_dynamic-update-slice_fusion, bf16[1,2048,256]{2,1,0:T(8,128)(2,1)S(1)} %copy-done.1), kind=kOutput, calls=%fused_computation.152 | convolution fusion | flops 805306368 | bytes 4980736 | tf_op jit(solution)/shard_map/dot_general | solution.py:287
  124.4 24.1 %collective-permute-done.21 = bf16[1024,256]{1,0:T(8,128)(2,1)S(1)} collective-permute-done((bf16[1024,256]{1,0:T(8,128)(2,1)S(1)}, bf16[1024,256]{1,0:T(8,128)(2,1)S(1)}, u32[]{:S(2)}, u32[]{:S(2)}) %collective-permute-start.21) | collective-permute-done | bytes 524320 | tf_op jit(solution)/shard_map/ppermute | solution.py:19
  150.0 9.7 %collective-permute-done.22 = bf16[1024,256]{1,0:T(8,128)(2,1)S(1)} collective-permute-done((bf16[1024,256]{1,0:T(8,128)(2,1)S(1)}, bf16[1024,256]{1,0:T(8,128)(2,1)S(1)}, u32[]{:S(2)}, u32[]{:S(2)}) %collective-permute-start.22) | collective-permute-done | bytes 524320 | tf_op jit(solution)/shard_map/ppermute | solution.py:19
  167.3 3.7 %collective-permute-done.23 = bf16[1024,256]{1,0:T(8,128)(2,1)S(1)} collective-permute-done((bf16[1024,256]{1,0:T(8,128)(2,1)}, bf16[1024,256]{1,0:T(8,128)(2,1)S(1)}, u32[]{:S(2)}, u32[]{:S(2)}) %collective-permute-start.23) | collective-permute-done | bytes 524320 | tf_op jit(solution)/shard_map/ppermute | solution.py:19
  172.5 9.7 %collective-permute-done.24 = bf16[1024,256]{1,0:T(8,128)(2,1)S(1)} collective-permute-done((bf16[1024,256]{1,0:T(8,128)(2,1)S(1)}, bf16[1024,256]{1,0:T(8,128)(2,1)S(1)}, u32[]{:S(2)}, u32[]{:S(2)}) %collective-permute-start.24) | collective-permute-done | bytes 524320 | tf_op jit(solution)/shard_map/ppermute | solution.py:19
  187.2 2.2 multiply_convert_fusion.2
  189.6 2.3 multiply_convert_fusion.1
  193.8 7.0 %collective-permute-start.40 = (bf16[96,512]{1,0:T(8,128)(2,1)S(1)}, bf16[96,512]{1,0:T(8,128)(2,1)S(1)}, u32[]{:S(2)}, u32[]{:S(2)}) collective-permute-start(bf16[96,512]{1,0:T(8,128)(2,1)S(1)} %get-tuple-element.56), channel_id=1, source_target_pairs={{0,8},{4,12},{8,0},{12,4},{16,24},{20,28},{24,16},{28,20},{1,9},{5... | collective-permute-start | bytes 294920 | tf_op jit(solution)/shard_map/ppermute | solution.py:19
  211.7 7.8 %collective-permute-start.36 = (bf16[96,512]{1,0:T(8,128)(2,1)S(1)}, bf16[96,512]{1,0:T(8,128)(2,1)S(1)}, u32[]{:S(2)}, u32[]{:S(2)}) collective-permute-start(bf16[96,512]{1,0:T(8,128)(2,1)S(1)} %get-tuple-element.61), channel_id=1, source_target_pairs={{0,16},{4,20},{8,24},{12,28},{16,0},{20,4},{24,8},{28,12},{1,17},{... | collective-permute-start | bytes 294920 | tf_op jit(solution)/shard_map/ppermute | solution.py:19
  219.9 2.3 collective-permute-start.37
  224.7 2.3 collective-permute-start.53
  229.4 7.2 %collective-permute-done.52 = bf16[96,512]{1,0:T(8,128)(2,1)S(1)} collective-permute-done((bf16[96,512]{1,0:T(8,128)(2,1)S(1)}, bf16[96,512]{1,0:T(8,128)(2,1)S(1)}, u32[]{:S(2)}, u32[]{:S(2)}) %collective-permute-start.52) | collective-permute-done | bytes 98336 | tf_op jit(solution)/shard_map/ppermute | solution.py:19
  (227 shorter events, 97.0 us)
Async XLA Ops:
  1.6 15.7 %collective-permute-start.27 = (f32[2,2,96]{2,1,0:T(2,128)S(1)}, f32[2,2,96]{2,1,0:T(2,128)S(1)}, u32[]{:S(2)}, u32[]{:S(2)}) collective-permute-start(f32[2,2,96]{2,1,0:T(2,128)S(1)} %pad_maximum_fusion.12), channel_id=1, source_target_pairs={{0,8},{4,12},{8,0},{12,4},{16,24},{20,28},{24,16},{28,20},{1,9},{5... | collective-permute-start | bytes 4616 | tf_op jit(solution)/shard_map/ppermute | solution.py:19
  4.7 14.3 %collective-permute-start.28 = (f32[2,2,96]{2,1,0:T(2,128)S(1)}, f32[2,2,96]{2,1,0:T(2,128)}, u32[]{:S(2)}, u32[]{:S(2)}) collective-permute-start(f32[2,2,96]{2,1,0:T(2,128)S(1)} %pad_maximum_fusion.12), channel_id=1, source_target_pairs={{0,16},{4,20},{8,24},{12,28},{16,0},{20,4},{24,8},{28,12},{1,17},{... | collective-permute-start | bytes 4616 | tf_op jit(solution)/shard_map/ppermute | solution.py:19
  7.3 16.7 %collective-permute-start.29 = (f32[2,2,96]{2,1,0:T(2,128)S(1)}, f32[2,2,96]{2,1,0:T(2,128)}, u32[]{:S(2)}, u32[]{:S(2)}) collective-permute-start(f32[2,2,96]{2,1,0:T(2,128)S(1)} %pad_maximum_fusion.12), channel_id=1, source_target_pairs={{0,24},{4,28},{8,16},{12,20},{16,8},{20,12},{24,0},{28,4},{1,25},{... | collective-permute-start | bytes 4616 | tf_op jit(solution)/shard_map/ppermute | solution.py:19
  7.3 27.1 %collective-permute-start.30 = (f32[2,2,96]{2,1,0:T(2,128)S(1)}, f32[2,2,96]{2,1,0:T(2,128)S(1)}, u32[]{:S(2)}, u32[]{:S(2)}) collective-permute-start(f32[2,2,96]{2,1,0:T(2,128)S(1)} %pad_maximum_fusion.12), channel_id=1, source_target_pairs={{0,4},{4,0},{8,12},{12,8},{16,20},{20,16},{24,28},{28,24},{1,5},{5... | collective-permute-start | bytes 4616 | tf_op jit(solution)/shard_map/ppermute | solution.py:19
  17.3 91.8 %collective-permute-start.38 = (bf16[1024,512]{1,0:T(8,128)(2,1)}, bf16[1024,512]{1,0:T(8,128)(2,1)}, u32[]{:S(2)}, u32[]{:S(2)}) collective-permute-start(bf16[1024,512]{1,0:T(8,128)(2,1)} %bitcast.171), channel_id=1, source_target_pairs={{0,1},{1,0},{2,3},{3,2},{4,5},{5,4},{6,7},{7,6},{8,9},{9,8},{10,11... | collective-permute-start | bytes 3145736 | tf_op jit(solution)/shard_map/ppermute | solution.py:19
  24.8 86.3 %collective-permute-start.43 = (bf16[1024,512]{1,0:T(8,128)(2,1)}, bf16[1024,512]{1,0:T(8,128)(2,1)}, u32[]{:S(2)}, u32[]{:S(2)}) collective-permute-start(bf16[1024,512]{1,0:T(8,128)(2,1)} %bitcast.172), channel_id=1, source_target_pairs={{0,2},{1,3},{2,0},{3,1},{4,6},{5,7},{6,4},{7,5},{8,10},{9,11},{10,... | collective-permute-start | bytes 3145736 | tf_op jit(solution)/shard_map/ppermute | solution.py:19
  32.8 20.4 %collective-permute-start.5 = (bf16[128,384]{1,0:T(8,128)(2,1)}, bf16[128,384]{1,0:T(8,128)(2,1)S(1)}, u32[]{:S(2)}, u32[]{:S(2)}) collective-permute-start(bf16[128,384]{1,0:T(8,128)(2,1)} %pooled.1), channel_id=1, source_target_pairs={{0,2},{1,3},{2,0},{3,1},{4,6},{5,7},{6,4},{7,5},{8,10},{9,11},{10,... | collective-permute-start | bytes 294920 | tf_op jit(solution)/shard_map/ppermute | solution.py:19
  34.4 18.9 %collective-permute-start.6 = (bf16[128,384]{1,0:T(8,128)(2,1)}, bf16[128,384]{1,0:T(8,128)(2,1)S(1)}, u32[]{:S(2)}, u32[]{:S(2)}) collective-permute-start(bf16[128,384]{1,0:T(8,128)(2,1)} %pooled.1), channel_id=1, source_target_pairs={{0,3},{1,2},{2,1},{3,0},{4,7},{5,6},{6,5},{7,4},{8,11},{9,10},{10,... | collective-permute-start | bytes 294920 | tf_op jit(solution)/shard_map/ppermute | solution.py:19
  45.6 75.8 %collective-permute-start.17 = (bf16[1024,256]{1,0:T(8,128)(2,1)}, bf16[1024,256]{1,0:T(8,128)(2,1)}, u32[]{:S(2)}, u32[]{:S(2)}) collective-permute-start(bf16[1024,256]{1,0:T(8,128)(2,1)} %get-tuple-element.47), channel_id=1, source_target_pairs={{0,1},{1,0},{2,3},{3,2},{4,5},{5,4},{6,7},{7,6},{8,9},{9,8},{10,11... | collective-permute-start | bytes 1572872 | tf_op jit(solution)/shard_map/ppermute | solution.py:19
  74.2 20.0 %collective-permute-start.10 = (bf16[96,2048]{1,0:T(8,128)(2,1)}, bf16[96,2048]{1,0:T(8,128)(2,1)}, u32[]{:S(2)}, u32[]{:S(2)}) collective-permute-start(bf16[96,2048]{1,0:T(8,128)(2,1)} %get-tuple-element.68), channel_id=1, source_target_pairs={{0,8},{4,12},{8,0},{12,4},{16,24},{20,28},{24,16},{28,20},{1,9},{5... | collective-permute-start | bytes 1179656 | tf_op jit(solution)/shard_map/ppermute | solution.py:19
  74.8 22.9 %collective-permute-start.11 = (bf16[96,2048]{1,0:T(8,128)(2,1)}, bf16[96,2048]{1,0:T(8,128)(2,1)}, u32[]{:S(2)}, u32[]{:S(2)}) collective-permute-start(bf16[96,2048]{1,0:T(8,128)(2,1)} %get-tuple-element.68), channel_id=1, source_target_pairs={{0,16},{4,20},{8,24},{12,28},{16,0},{20,4},{24,8},{28,12},{1,17},{... | collective-permute-start | bytes 1179656 | tf_op jit(solution)/shard_map/ppermute | solution.py:19
  111.2 49.6 %collective-permute-start.20 = (bf16[2048,256]{1,0:T(8,128)(2,1)S(1)}, bf16[2048,256]{1,0:T(8,128)(2,1)S(1)}, u32[]{:S(2)}, u32[]{:S(2)}) collective-permute-start(bf16[2048,256]{1,0:T(8,128)(2,1)S(1)} %bitcast.140), channel_id=1, source_target_pairs={{0,2},{1,3},{2,0},{3,1},{4,6},{5,7},{6,4},{7,5},{8,10},{9,11},{10,... | collective-permute-start | bytes 3145736 | tf_op jit(solution)/shard_map/ppermute | solution.py:19
  114.7 33.8 %collective-permute-start.21 = (bf16[1024,256]{1,0:T(8,128)(2,1)S(1)}, bf16[1024,256]{1,0:T(8,128)(2,1)S(1)}, u32[]{:S(2)}, u32[]{:S(2)}) collective-permute-start(bf16[1024,256]{1,0:T(8,128)(2,1)S(1)} %get-tuple-element.45), channel_id=1, source_target_pairs={{0,2},{1,3},{2,0},{3,1},{4,6},{5,7},{6,4},{7,5},{8,10},{9,11},{10,... | collective-permute-start | bytes 1572872 | tf_op jit(solution)/shard_map/ppermute | solution.py:19
  116.0 43.7 %collective-permute-start.22 = (bf16[1024,256]{1,0:T(8,128)(2,1)S(1)}, bf16[1024,256]{1,0:T(8,128)(2,1)S(1)}, u32[]{:S(2)}, u32[]{:S(2)}) collective-permute-start(bf16[1024,256]{1,0:T(8,128)(2,1)S(1)} %get-tuple-element.46), channel_id=1, source_target_pairs={{0,2},{1,3},{2,0},{3,1},{4,6},{5,7},{6,4},{7,5},{8,10},{9,11},{10,... | collective-permute-start | bytes 1572872 | tf_op jit(solution)/shard_map/ppermute | solution.py:19
  121.4 63.1 %collective-permute-start.19 = (bf16[2048,256]{1,0:T(8,128)(2,1)S(1)}, bf16[2048,256]{1,0:T(8,128)(2,1)S(1)}, u32[]{:S(2)}, u32[]{:S(2)}) collective-permute-start(bf16[2048,256]{1,0:T(8,128)(2,1)S(1)} %bitcast.141), channel_id=1, source_target_pairs={{0,1},{1,0},{2,3},{3,2},{4,5},{5,4},{6,7},{7,6},{8,9},{9,8},{10,11... | collective-permute-start | bytes 3145736 | tf_op jit(solution)/shard_map/ppermute | solution.py:19
  122.9 48.1 %collective-permute-start.23 = (bf16[1024,256]{1,0:T(8,128)(2,1)}, bf16[1024,256]{1,0:T(8,128)(2,1)S(1)}, u32[]{:S(2)}, u32[]{:S(2)}) collective-permute-start(bf16[1024,256]{1,0:T(8,128)(2,1)} %collective-permute-done.17), channel_id=1, source_target_pairs={{0,2},{1,3},{2,0},{3,1},{4,6},{5,7},{6,4},{7,5},{8,10},{9,11},{10,... | collective-permute-start | bytes 1572872 | tf_op jit(solution)/shard_map/ppermute | solution.py:19
  148.5 33.7 %collective-permute-start.24 = (bf16[1024,256]{1,0:T(8,128)(2,1)S(1)}, bf16[1024,256]{1,0:T(8,128)(2,1)S(1)}, u32[]{:S(2)}, u32[]{:S(2)}) collective-permute-start(bf16[1024,256]{1,0:T(8,128)(2,1)S(1)} %collective-permute-done.18), channel_id=1, source_target_pairs={{0,2},{1,3},{2,0},{3,1},{4,6},{5,7},{6,4},{7,5},{8,10},{9,11},{10,... | collective-permute-start | bytes 1572872 | tf_op jit(solution)/shard_map/ppermute | solution.py:19
  159.7 26.0 %collective-permute-start.25 = (bf16[1024,256]{1,0:T(8,128)(2,1)S(1)}, bf16[1024,256]{1,0:T(8,128)(2,1)S(1)}, u32[]{:S(2)}, u32[]{:S(2)}) collective-permute-start(bf16[1024,256]{1,0:T(8,128)(2,1)S(1)} %collective-permute-done.21), channel_id=1, source_target_pairs={{0,1},{1,0},{2,3},{3,2},{4,5},{5,4},{6,7},{7,6},{8,9},{9,8},{10,11... | collective-permute-start | bytes 1572872 | tf_op jit(solution)/shard_map/ppermute | solution.py:19
  160.8 24.9 %collective-permute-start.26 = (bf16[1024,256]{1,0:T(8,128)(2,1)S(1)}, bf16[1024,256]{1,0:T(8,128)(2,1)S(1)}, u32[]{:S(2)}, u32[]{:S(2)}) collective-permute-start(bf16[1024,256]{1,0:T(8,128)(2,1)S(1)} %collective-permute-done.22), channel_id=1, source_target_pairs={{0,1},{1,0},{2,3},{3,2},{4,5},{5,4},{6,7},{7,6},{8,9},{9,8},{10,11... | collective-permute-start | bytes 1572872 | tf_op jit(solution)/shard_map/ppermute | solution.py:19
  171.0 32.7 %collective-permute-start.48 = (bf16[512,512]{1,0:T(8,128)(2,1)S(1)}, bf16[512,512]{1,0:T(8,128)(2,1)S(1)}, u32[]{:S(2)}, u32[]{:S(2)}) collective-permute-start(bf16[512,512]{1,0:T(8,128)(2,1)S(1)} %slice.256), channel_id=1, source_target_pairs={{0,2},{1,3},{2,0},{3,1},{4,6},{5,7},{6,4},{7,5},{8,10},{9,11},{10,... | collective-permute-start | bytes 1572872 | tf_op jit(solution)/shard_map/ppermute | solution.py:19
  182.2 22.5 %collective-permute-start.49 = (bf16[512,512]{1,0:T(8,128)(2,1)S(1)}, bf16[512,512]{1,0:T(8,128)(2,1)S(1)}, u32[]{:S(2)}, u32[]{:S(2)}) collective-permute-start(bf16[512,512]{1,0:T(8,128)(2,1)S(1)} %slice.257), channel_id=1, source_target_pairs={{0,1},{1,0},{2,3},{3,2},{4,5},{5,4},{6,7},{7,6},{8,9},{9,8},{10,11... | collective-permute-start | bytes 1572872 | tf_op jit(solution)/shard_map/ppermute | solution.py:19
  204.8 15.2 %collective-permute-start.46 = (bf16[96,512]{1,0:T(8,128)(2,1)S(1)}, bf16[96,512]{1,0:T(8,128)(2,1)S(1)}, u32[]{:S(2)}, u32[]{:S(2)}) collective-permute-start(bf16[96,512]{1,0:T(8,128)(2,1)S(1)} %get-tuple-element.64), channel_id=1, source_target_pairs={{0,16},{4,20},{8,24},{12,28},{16,0},{20,4},{24,8},{28,12},{1,17},{... | collective-permute-start | bytes 294920 | tf_op jit(solution)/shard_map/ppermute | solution.py:19
  207.8 14.4 %collective-permute-start.47 = (bf16[96,512]{1,0:T(8,128)(2,1)S(1)}, bf16[96,512]{1,0:T(8,128)(2,1)S(1)}, u32[]{:S(2)}, u32[]{:S(2)}) collective-permute-start(bf16[96,512]{1,0:T(8,128)(2,1)S(1)} %get-tuple-element.63), channel_id=1, source_target_pairs={{0,24},{4,28},{8,16},{12,20},{16,8},{20,12},{24,0},{28,4},{1,25},{... | collective-permute-start | bytes 294920 | tf_op jit(solution)/shard_map/ppermute | solution.py:19
  211.7 17.3 %collective-permute-start.36 = (bf16[96,512]{1,0:T(8,128)(2,1)S(1)}, bf16[96,512]{1,0:T(8,128)(2,1)S(1)}, u32[]{:S(2)}, u32[]{:S(2)}) collective-permute-start(bf16[96,512]{1,0:T(8,128)(2,1)S(1)} %get-tuple-element.61), channel_id=1, source_target_pairs={{0,16},{4,20},{8,24},{12,28},{16,0},{20,4},{24,8},{28,12},{1,17},{... | collective-permute-start | bytes 294920 | tf_op jit(solution)/shard_map/ppermute | solution.py:19
  (59 other events, 906.9 us)

commit v3 on v2

--- a/solution.py
+++ b/solution.py
@@ -1,3 +1,5 @@
+import functools
+
 import jax
 import jax.numpy as jnp
 from jax import lax
@@ -179,9 +181,58 @@
     return [(r - mean) * scale for r in rows]
 
 
+def gather_rows_kernel(*refs):
+    *parts, out_ref = refs
+    rows = parts[0].shape[0]
+    for p, part in enumerate(parts):
+        out_ref[p * rows : (p + 1) * rows, :] = part[...]
+
+
+def hidden_kernel(count, *refs):
+    row_refs, rest = refs[: count[0]], refs[count[0] :]
+    gates, ups = rest[: count[1]], rest[count[1] : count[1] + count[2]]
+    outs = rest[count[1] + count[2] :]
+    if len(outs) == 2:
+        gather_rows_kernel(*row_refs, outs[0])
+        rows = outs[0]
+    else:
+        rows = row_refs[0]
+
+    def product(parts):
+        total, at = None, 0
+        for part in parts:
+            depth = part.shape[0]
+            piece = jnp.dot(
+                rows[:, at : at + depth], part[...], preferred_element_type=F32
+            )
+            total = piece if total is None else total + piece
+            at += depth
+        return total
+
+    gated = product(gates)
+    outs[-1][...] = (gated * jax.nn.sigmoid(gated) * product(ups)).astype(BF16)
+
+
+def hidden_units(row_parts, gates, ups):
+    count = (len(row_parts), len(gates), len(ups))
+    rows = sum(r.shape[0] for r in row_parts)
+    shape = jax.ShapeDtypeStruct((rows, gates[0].shape[1]), BF16)
+    joined = jax.ShapeDtypeStruct((rows, row_parts[0].shape[1]), BF16)
+    outs = (joined, shape) if len(row_parts) > 1 else (shape,)
+    got = pl.pallas_call(
+        functools.partial(hidden_kernel, count),
+        out_shape=outs,
+        in_specs=in_vmem(sum(count)),
+        out_specs=tuple(in_vmem(len(outs))),
+        name="hidden",
+    )(*row_parts, *gates, *ups)
+    return (got[0], got[-1])
+
+
 def weight_parts(w_gate, w_up, w_down, tp):
     if tp != 4:
-        return tuple(exchange_all(w, "tp") for w in (w_gate, w_up, w_down))
+        gate, up, down = (exchange_all(w, "tp") for w in (w_gate, w_up, w_down))
+        return [[w] for w in gate], [[w] for w in up], down
     half = w_gate.shape[0] // 2
     gate1_top = swap_with(w_gate[:half], "tp", 1)
     up2_top = swap_with(w_up[:half], "tp", 2)
@@ -198,18 +249,8 @@
     dhalf = w_down.shape[0] // 2
     down3_low = swap_with(down2[dhalf:], "tp", 1)
     down3_top = swap_with(down1[:dhalf], "tp", 2)
-    gate = [
-        w_gate,
-        jnp.concatenate([gate1_top, gate1_low]),
-        gate2,
-        jnp.concatenate([gate3_top, gate3_low]),
-    ]
-    up = [
-        w_up,
-        up1,
-        jnp.concatenate([up2_top, up2_low]),
-        jnp.concatenate([up3_top, up3_low]),
-    ]
+    gate = [[w_gate], [gate1_top, gate1_low], [gate2], [gate3_top, gate3_low]]
+    up = [[w_up], [up1], [up2_top, up2_low], [up3_top, up3_low]]
     down = [w_down, down1, down2, jnp.concatenate([down3_top, down3_low])]
     return gate, up, down
 
@@ -274,7 +315,6 @@
     gate_w, up_w, down_w = weight_parts(w_gate[0], w_up[0], w_down[0], tp)
 
     everyone = line_gather(tokens, "sp")
-    inputs = jnp.concatenate(everyone)
     my_routes = lax.dynamic_slice_in_dim(routes, j * quarter, quarter, 0)
     my_weights = lax.dynamic_slice_in_dim(route_weight, j * quarter, quarter, 0)
     chosen = jnp.stack([my_routes.astype(F32).T, my_weights.T])
@@ -282,11 +322,10 @@
     chosen = jnp.where(chosen[:, 0] == i.astype(F32), chosen[:, 1], 0.0)
     share = jnp.sum(chosen, axis=1).reshape(-1, 1)
 
-    hidden_rel = []
-    for k in range(tp):
-        gate_part = jnp.dot(inputs, gate_w[k], preferred_element_type=F32)
-        up_part = jnp.dot(inputs, up_w[k], preferred_element_type=F32)
-        hidden_rel.append((jax.nn.silu(gate_part) * up_part).astype(BF16))
+    inputs, first_hidden = hidden_units(everyone, gate_w[0], up_w[0])
+    hidden_rel = [first_hidden] + [
+        hidden_units([inputs], gate_w[k], up_w[k])[1] for k in range(1, tp)
+    ]
     hidden = jnp.concatenate(in_order(hidden_rel, j), axis=1)
 
     final_rel = []

time: 247 us -> 211 us (0.85)
  waiting for transfers between devices: 116 us -> 88.5 us
  Pallas kernels: 6.23 us -> 27.2 us
  matrix products: 19.4 us -> 8.4 us
  starting transfers between devices: 75.7 us -> 67 us
  local copies, waits for them, and re-layouts: 20.1 us -> 12.2 us
    ppermute x57, waiting for transfers between devices: 116 us -> 88.5 us  [swap_with(): return lax.ppermute(part, axis, [(i, i ^ bits) for i in range(size)])]
    pallas_call x0 -> x4, Pallas kernels: none -> 20.9 us  [hidden_units(): pl.pallas_call(functools.partial(hidden_kernel, count), out_shape=outs, i...]
    dot_general x8 -> x0, matrix products: 12.1 us -> none  [the longest x4 7.55 us: body(): gate_part = jnp.dot(inputs, gate_w[k], preferred_element_type=F32)]
    ppermute x57, starting transfers between devices: 75.7 us -> 67 us  [swap_with(): return lax.ppermute(part, axis, [(i, i ^ bits) for i in range(size)])]
    unnamed x64 -> x68, local copies, waits for them, and re-layouts: 8.82 us -> 2.69 us
  transfers between devices with their start and end apart: 57 -> 57, of which waited for: 20 -> 19; matrix products, arithmetic and copies ran while one was open for 18% -> 10% of each run, Pallas kernels for 3% -> 13%
where the time goes in v3:
time: 211 us
  waiting for transfers between devices  88.5 us (42%)
  starting transfers between devices  67 us (32%)
  Pallas kernels  27.2 us (13%)
  local copies, waits for them, and re-layouts  12.2 us (6%)
  matrix products  8.4 us (4%)
  other arithmetic  6.89 us (3%)
    ppermute x57, waiting for transfers between devices, swap_with(): return lax.ppermute(part, axis, [(i, i ^ bits) for i in range(size)])  88.5 us
    ppermute x57, starting transfers between devices, swap_with(): return lax.ppermute(part, axis, [(i, i ^ bits) for i in range(size)])  67 us
    pallas_call x4, Pallas kernels, hidden_units(): pl.pallas_call(functools.partial(hidden_kernel, count), out_shape=outs, i...  20.9 us
    dot_general x4, matrix products, body(): result = jnp.dot(hidden, down_w[k], preferred_element_type=F32)  7.64 us
  transfers between devices with their start and end apart: 57, of which 19 were waited for; matrix products, arithmetic and copies ran while one was open for 10% of the time, Pallas kernels for 13%

profile of v3, /device:TPU:0, one launch (start us, length us, event | category | flops | bytes accessed | tf_op | source)
XLA Modules:
  0.0 210.8 jit_solution(16333338214316525670)
XLA Ops:
  1.6 3.1 %collective-permute-start.27 = (f32[2,2,96]{2,1,0:T(2,128)S(1)}, f32[2,2,96]{2,1,0:T(2,128)S(1)}, u32[]{:S(2)}, u32[]{:S(2)}) collective-permute-start(f32[2,2,96]{2,1,0:T(2,128)S(1)} %pad_maximum_fusion.12), channel_id=1, source_target_pairs={{0,8},{4,12},{8,0},{12,4},{16,24},{20,28},{24,16},{28,20},{1,9},{5... | collective-permute-start | bytes 4616 | tf_op jit(solution)/shard_map/ppermute | solution.py:21
  4.7 2.6 %collective-permute-start.28 = (f32[2,2,96]{2,1,0:T(2,128)S(1)}, f32[2,2,96]{2,1,0:T(2,128)S(1)}, u32[]{:S(2)}, u32[]{:S(2)}) collective-permute-start(f32[2,2,96]{2,1,0:T(2,128)S(1)} %pad_maximum_fusion.12), channel_id=1, source_target_pairs={{0,16},{4,20},{8,24},{12,28},{16,0},{20,4},{24,8},{28,12},{1,17},{... | collective-permute-start | bytes 4616 | tf_op jit(solution)/shard_map/ppermute | solution.py:21
  10.8 2.3 %slice_bitcast_fusion.2 = (bf16[1024,256]{1,0:T(8,128)(2,1)}, bf16[1024,256]{1,0:T(8,128)(2,1)}) fusion(bf16[1,2048,256]{2,1,0:T(8,128)(2,1)} %param.27), kind=kLoop, calls=%fused_computation.19 | loop fusion | bytes 2097152 | tf_op jit(solution)/shard_map/slice | solution.py:239
  13.7 3.9 %collective-permute-start.3 = (f32[2,24,128]{2,1,0:T(8,128)S(1)}, f32[2,24,128]{2,1,0:T(8,128)S(1)}, u32[]{:S(2)}, u32[]{:S(2)}) collective-permute-start(f32[2,24,128]{2,1,0:T(8,128)S(1)} %pad_maximum_fusion.11.rest_0_), channel_id=1, source_target_pairs={{0,24},{4,28},{8,16},{12,20},{16,8},{20,12},{24,0},{28,4},{1,25},{... | collective-permute-start | bytes 73736 | tf_op jit(solution)/shard_map/ppermute | solution.py:21
  28.3 3.3 %collective-permute-start.29 = (f32[2,2,96]{2,1,0:T(2,128)S(1)}, f32[2,2,96]{2,1,0:T(2,128)S(1)}, u32[]{:S(2)}, u32[]{:S(2)}) collective-permute-start(f32[2,2,96]{2,1,0:T(2,128)S(1)} %pad_maximum_fusion.12), channel_id=1, source_target_pairs={{0,24},{4,28},{8,16},{12,20},{16,8},{20,12},{24,0},{28,4},{1,25},{... | collective-permute-start | bytes 4616 | tf_op jit(solution)/shard_map/ppermute | solution.py:21
  37.9 3.0 %collective-permute-done.7 = f32[104,512]{1,0:T(8,128)S(1)} collective-permute-done((f32[104,512]{1,0:T(8,128)S(1)}, f32[104,512]{1,0:T(8,128)S(1)}, u32[]{:S(2)}, u32[]{:S(2)}) %collective-permute-start.7) | collective-permute-done | bytes 213024 | tf_op jit(solution)/shard_map/ppermute | solution.py:21
  44.2 5.8 %collective-permute-done.9 = f32[104,512]{1,0:T(8,128)S(1)} collective-permute-done((f32[104,512]{1,0:T(8,128)S(1)}, f32[104,512]{1,0:T(8,128)S(1)}, u32[]{:S(2)}, u32[]{:S(2)}) %collective-permute-start.9) | collective-permute-done | bytes 213024 | tf_op jit(solution)/shard_map/ppermute | solution.py:21
  56.1 4.6 %collective-permute-done.17.refs_1_ = bf16[1024,256]{1,0:T(8,128)(2,1)S(1)} collective-permute-done((bf16[1024,256]{1,0:T(8,128)(2,1)}, bf16[1024,256]{1,0:T(8,128)(2,1)S(1)}, u32[]{:S(2)}, u32[]{:S(2)}) %collective-permute-start.17) | collective-permute-done | bytes 524320 | tf_op jit(solution)/shard_map/ppermute | solution.py:21
  61.7 10.3 %collective-permute-done.18.refs_2_ = bf16[1024,256]{1,0:T(8,128)(2,1)S(1)} collective-permute-done((bf16[1024,256]{1,0:T(8,128)(2,1)}, bf16[1024,256]{1,0:T(8,128)(2,1)S(1)}, u32[]{:S(2)}, u32[]{:S(2)}) %collective-permute-start.18) | collective-permute-done | bytes 524320 | tf_op jit(solution)/shard_map/ppermute | solution.py:21
  73.7 3.7 %collective-permute-done.22.refs_3_ = bf16[1024,256]{1,0:T(8,128)(2,1)} collective-permute-done((bf16[1024,256]{1,0:T(8,128)(2,1)}, bf16[1024,256]{1,0:T(8,128)(2,1)}, u32[]{:S(2)}, u32[]{:S(2)}) %collective-permute-start.22) | collective-permute-done | bytes 524320 | tf_op jit(solution)/shard_map/ppermute | solution.py:21
  80.4 18.2 %collective-permute-done.11.refs_2_ = bf16[96,2048]{1,0:T(8,128)(2,1)} collective-permute-done((bf16[96,2048]{1,0:T(8,128)(2,1)S(1)}, bf16[96,2048]{1,0:T(8,128)(2,1)}, u32[]{:S(2)}, u32[]{:S(2)}) %collective-permute-start.11) | collective-permute-done | bytes 393248 | tf_op jit(solution)/shard_map/ppermute | solution.py:21
  101.0 12.4 %collective-permute-done.38 = bf16[1024,512]{1,0:T(8,128)(2,1)} collective-permute-done((bf16[1024,512]{1,0:T(8,128)(2,1)}, bf16[1024,512]{1,0:T(8,128)(2,1)}, u32[]{:S(2)}, u32[]{:S(2)}) %collective-permute-start.38) | collective-permute-done | bytes 1048608 | tf_op jit(solution)/shard_map/ppermute | solution.py:21
  121.5 5.9 %hidden.4 = (bf16[768,2048]{1,0:T(8,128)(2,1)}, bf16[768,256]{1,0:T(8,128)(2,1)}) custom-call(bf16[96,2048]{1,0:T(8,128)(2,1)} %copy-done.3, bf16[96,2048]{1,0:T(8,128)(2,1)} %collective-permute-done.10.refs_1_, bf16[96,2048]{1,0:T(8,128)(2,1)} %collective-permute-done.11.refs_2_, bf16[96,2048]{1,0:T(8,128)(2,1)} %copy-done.10, bf16[96,2048]{1,0:T(8,128)(2,1)} %copy-done.11, ...), custom_call_target="tpu_custom_call" | custom-call | tf_op jit(solution)/shard_map/hidden/pallas_call | solution.py:222
  127.4 5.0 %hidden.5 = bf16[768,256]{1,0:T(8,128)(2,1)} custom-call(bf16[768,2048]{1,0:T(8,128)(2,1)} %get-tuple-element.12.refs_0_, bf16[1024,256]{1,0:T(8,128)(2,1)} %copy-done.7, bf16[1024,256]{1,0:T(8,128)(2,1)} %copy-done.8, bf16[2048,256]{1,0:T(8,128)(2,1)} %collective-permute-done.19.refs_3_), custom_call_target="tpu_custom_call" | custom-call | tf_op jit(solution)/shard_map/hidden/pallas_call | solution.py:222
  133.6 5.0 %hidden.6 = bf16[768,256]{1,0:T(8,128)(2,1)} custom-call(bf16[768,2048]{1,0:T(8,128)(2,1)} %get-tuple-element.12.refs_0_, bf16[2048,256]{1,0:T(8,128)(2,1)} %collective-permute-done.20.refs_1_, bf16[1024,256]{1,0:T(8,128)(2,1)} %copy-done.9, bf16[1024,256]{1,0:T(8,128)(2,1)} %collective-permute-done.22.refs_3_), custom_call_target="tpu_custom_call" | custom-call | tf_op jit(solution)/shard_map/hidden/pallas_call | solution.py:222
  140.6 7.2 %collective-permute-done.24.refs_2_ = bf16[1024,256]{1,0:T(8,128)(2,1)} collective-permute-done((bf16[1024,256]{1,0:T(8,128)(2,1)}, bf16[1024,256]{1,0:T(8,128)(2,1)}, u32[]{:S(2)}, u32[]{:S(2)}) %collective-permute-start.24) | collective-permute-done | bytes 524320 | tf_op jit(solution)/shard_map/ppermute | solution.py:21
  147.9 5.0 %hidden.7 = bf16[768,256]{1,0:T(8,128)(2,1)} custom-call(bf16[768,2048]{1,0:T(8,128)(2,1)} %get-tuple-element.12.refs_0_, bf16[1024,256]{1,0:T(8,128)(2,1)} %collective-permute-done.23.refs_1_, bf16[1024,256]{1,0:T(8,128)(2,1)} %collective-permute-done.24.refs_2_, bf16[1024,256]{1,0:T(8,128)(2,1)} %collective-permute-done.25.refs_3_, ...), custom_call_target="tpu_custom_call" | custom-call | tf_op jit(solution)/shard_map/hidden/pallas_call | solution.py:222
  154.2 2.3 %multiply_convert_fusion.2 = bf16[768,512]{1,0:T(8,128)(2,1)S(1)} fusion(bf16[1024,512]{1,0:T(8,128)(2,1)} %collective-permute-done.38, f32[768]{0:T(1024)S(1)} %mul.270, bf16[768,256]{1,0:T(8,128)(2,1)S(1)} %get-tuple-element.38, bf16[768,256]{1,0:T(8,128)(2,1)S(1)} %get-tuple-element.39, bf16[768,256]{1,0:T(8,128)(2,1)S(1)} %get-tuple-element.40, ...), kind=kOutput, calls=%fused_computation.4 | convolution fusion | flops 812384256 | bytes 3410944 | tf_op jit(solution)/shard_map/dot_general | solution.py:334
  160.9 5.1 %collective-permute-start.40 = (bf16[96,512]{1,0:T(8,128)(2,1)S(1)}, bf16[96,512]{1,0:T(8,128)(2,1)S(1)}, u32[]{:S(2)}, u32[]{:S(2)}) collective-permute-start(bf16[96,512]{1,0:T(8,128)(2,1)S(1)} %get-tuple-element.60), channel_id=1, source_target_pairs={{0,8},{4,12},{8,0},{12,4},{16,24},{20,28},{24,16},{28,20},{1,9},{5... | collective-permute-start | bytes 294920 | tf_op jit(solution)/shard_map/ppermute | solution.py:21
  166.2 2.5 %collective-permute-start.42 = (bf16[96,512]{1,0:T(8,128)(2,1)S(1)}, bf16[96,512]{1,0:T(8,128)(2,1)S(1)}, u32[]{:S(2)}, u32[]{:S(2)}) collective-permute-start(bf16[96,512]{1,0:T(8,128)(2,1)S(1)} %get-tuple-element.61), channel_id=1, source_target_pairs={{0,24},{4,28},{8,16},{12,20},{16,8},{20,12},{24,0},{28,4},{1,25},{... | collective-permute-start | bytes 294920 | tf_op jit(solution)/shard_map/ppermute | solution.py:21
  172.9 2.5 %collective-permute-start.47 = (bf16[96,512]{1,0:T(8,128)(2,1)S(1)}, bf16[96,512]{1,0:T(8,128)(2,1)S(1)}, u32[]{:S(2)}, u32[]{:S(2)}) collective-permute-start(bf16[96,512]{1,0:T(8,128)(2,1)S(1)} %get-tuple-element.67), channel_id=1, source_target_pairs={{0,24},{4,28},{8,16},{12,20},{16,8},{20,12},{24,0},{28,4},{1,25},{... | collective-permute-start | bytes 294920 | tf_op jit(solution)/shard_map/ppermute | solution.py:21
  177.0 6.2 %collective-permute-start.36 = (bf16[96,512]{1,0:T(8,128)(2,1)S(1)}, bf16[96,512]{1,0:T(8,128)(2,1)S(1)}, u32[]{:S(2)}, u32[]{:S(2)}) collective-permute-start(bf16[96,512]{1,0:T(8,128)(2,1)S(1)} %get-tuple-element.65), channel_id=1, source_target_pairs={{0,16},{4,20},{8,24},{12,28},{16,0},{20,4},{24,8},{28,12},{1,17},{... | collective-permute-start | bytes 294920 | tf_op jit(solution)/shard_map/ppermute | solution.py:21
  190.9 6.8 %collective-permute-done.36 = bf16[96,512]{1,0:T(8,128)(2,1)S(1)} collective-permute-done((bf16[96,512]{1,0:T(8,128)(2,1)S(1)}, bf16[96,512]{1,0:T(8,128)(2,1)S(1)}, u32[]{:S(2)}, u32[]{:S(2)}) %collective-permute-start.36) | collective-permute-done | bytes 98336 | tf_op jit(solution)/shard_map/ppermute | solution.py:21
  197.8 4.0 %collective-permute-done.52 = bf16[96,512]{1,0:T(8,128)(2,1)S(1)} collective-permute-done((bf16[96,512]{1,0:T(8,128)(2,1)S(1)}, bf16[96,512]{1,0:T(8,128)(2,1)S(1)}, u32[]{:S(2)}, u32[]{:S(2)}) %collective-permute-start.52) | collective-permute-done | bytes 98336 | tf_op jit(solution)/shard_map/ppermute | solution.py:21
  (226 shorter events, 79.4 us)
Async XLA Ops:
  1.6 49.9 %collective-permute-start.27 = (f32[2,2,96]{2,1,0:T(2,128)S(1)}, f32[2,2,96]{2,1,0:T(2,128)S(1)}, u32[]{:S(2)}, u32[]{:S(2)}) collective-permute-start(f32[2,2,96]{2,1,0:T(2,128)S(1)} %pad_maximum_fusion.12), channel_id=1, source_target_pairs={{0,8},{4,12},{8,0},{12,4},{16,24},{20,28},{24,16},{28,20},{1,9},{5... | collective-permute-start | bytes 4616 | tf_op jit(solution)/shard_map/ppermute | solution.py:21
  4.7 46.9 %collective-permute-start.28 = (f32[2,2,96]{2,1,0:T(2,128)S(1)}, f32[2,2,96]{2,1,0:T(2,128)S(1)}, u32[]{:S(2)}, u32[]{:S(2)}) collective-permute-start(f32[2,2,96]{2,1,0:T(2,128)S(1)} %pad_maximum_fusion.12), channel_id=1, source_target_pairs={{0,16},{4,20},{8,24},{12,28},{16,0},{20,4},{24,8},{28,12},{1,17},{... | collective-permute-start | bytes 4616 | tf_op jit(solution)/shard_map/ppermute | solution.py:21
  28.3 24.2 %collective-permute-start.29 = (f32[2,2,96]{2,1,0:T(2,128)S(1)}, f32[2,2,96]{2,1,0:T(2,128)S(1)}, u32[]{:S(2)}, u32[]{:S(2)}) collective-permute-start(f32[2,2,96]{2,1,0:T(2,128)S(1)} %pad_maximum_fusion.12), channel_id=1, source_target_pairs={{0,24},{4,28},{8,16},{12,20},{16,8},{20,12},{24,0},{28,4},{1,25},{... | collective-permute-start | bytes 4616 | tf_op jit(solution)/shard_map/ppermute | solution.py:21
  44.1 16.7 %collective-permute-start.17 = (bf16[1024,256]{1,0:T(8,128)(2,1)}, bf16[1024,256]{1,0:T(8,128)(2,1)S(1)}, u32[]{:S(2)}, u32[]{:S(2)}) collective-permute-start(bf16[1024,256]{1,0:T(8,128)(2,1)} %get-tuple-element.52), channel_id=1, source_target_pairs={{0,1},{1,0},{2,3},{3,2},{4,5},{5,4},{6,7},{7,6},{8,9},{9,8},{10,11... | collective-permute-start | bytes 1572872 | tf_op jit(solution)/shard_map/ppermute | solution.py:21
  50.0 22.0 %collective-permute-start.18 = (bf16[1024,256]{1,0:T(8,128)(2,1)}, bf16[1024,256]{1,0:T(8,128)(2,1)S(1)}, u32[]{:S(2)}, u32[]{:S(2)}) collective-permute-start(bf16[1024,256]{1,0:T(8,128)(2,1)} %get-tuple-element.51), channel_id=1, source_target_pairs={{0,1},{1,0},{2,3},{3,2},{4,5},{5,4},{6,7},{7,6},{8,9},{9,8},{10,11... | collective-permute-start | bytes 1572872 | tf_op jit(solution)/shard_map/ppermute | solution.py:21
  51.6 21.3 %collective-permute-start.21 = (bf16[1024,256]{1,0:T(8,128)(2,1)S(1)}, bf16[1024,256]{1,0:T(8,128)(2,1)S(1)}, u32[]{:S(2)}, u32[]{:S(2)}) collective-permute-start(bf16[1024,256]{1,0:T(8,128)(2,1)S(1)} %get-tuple-element.50), channel_id=1, source_target_pairs={{0,2},{1,3},{2,0},{3,1},{4,6},{5,7},{6,4},{7,5},{8,10},{9,11},{10,... | collective-permute-start | bytes 1572872 | tf_op jit(solution)/shard_map/ppermute | solution.py:21
  53.7 23.7 %collective-permute-start.22 = (bf16[1024,256]{1,0:T(8,128)(2,1)}, bf16[1024,256]{1,0:T(8,128)(2,1)}, u32[]{:S(2)}, u32[]{:S(2)}) collective-permute-start(bf16[1024,256]{1,0:T(8,128)(2,1)} %get-tuple-element.49), channel_id=1, source_target_pairs={{0,2},{1,3},{2,0},{3,1},{4,6},{5,7},{6,4},{7,5},{8,10},{9,11},{10,... | collective-permute-start | bytes 1572872 | tf_op jit(solution)/shard_map/ppermute | solution.py:21
  56.1 22.1 %collective-permute-start.10 = (bf16[96,2048]{1,0:T(8,128)(2,1)S(1)}, bf16[96,2048]{1,0:T(8,128)(2,1)}, u32[]{:S(2)}, u32[]{:S(2)}) collective-permute-start(bf16[96,2048]{1,0:T(8,128)(2,1)S(1)} %pad_maximum_fusion.5.refs_0_), channel_id=1, source_target_pairs={{0,8},{4,12},{8,0},{12,4},{16,24},{20,28},{24,16},{28,20},{1,9},{5... | collective-permute-start | bytes 1179656 | tf_op jit(solution)/shard_map/ppermute | solution.py:21
  60.7 40.0 %collective-permute-start.19 = (bf16[2048,256]{1,0:T(8,128)(2,1)S(1)}, bf16[2048,256]{1,0:T(8,128)(2,1)}, u32[]{:S(2)}, u32[]{:S(2)}) collective-permute-start(bf16[2048,256]{1,0:T(8,128)(2,1)S(1)} %bitcast.120), channel_id=1, source_target_pairs={{0,1},{1,0},{2,3},{3,2},{4,5},{5,4},{6,7},{7,6},{8,9},{9,8},{10,11... | collective-permute-start | bytes 3145736 | tf_op jit(solution)/shard_map/ppermute | solution.py:21
  71.9 41.4 %collective-permute-start.38 = (bf16[1024,512]{1,0:T(8,128)(2,1)}, bf16[1024,512]{1,0:T(8,128)(2,1)}, u32[]{:S(2)}, u32[]{:S(2)}) collective-permute-start(bf16[1024,512]{1,0:T(8,128)(2,1)} %bitcast.47), channel_id=1, source_target_pairs={{0,1},{1,0},{2,3},{3,2},{4,5},{5,4},{6,7},{7,6},{8,9},{9,8},{10,11... | collective-permute-start | bytes 3145736 | tf_op jit(solution)/shard_map/ppermute | solution.py:21
  73.7 24.9 %collective-permute-start.11 = (bf16[96,2048]{1,0:T(8,128)(2,1)S(1)}, bf16[96,2048]{1,0:T(8,128)(2,1)}, u32[]{:S(2)}, u32[]{:S(2)}) collective-permute-start(bf16[96,2048]{1,0:T(8,128)(2,1)S(1)} %pad_maximum_fusion.5.refs_0_), channel_id=1, source_target_pairs={{0,16},{4,20},{8,24},{12,28},{16,0},{20,4},{24,8},{28,12},{1,17},{... | collective-permute-start | bytes 1179656 | tf_op jit(solution)/shard_map/ppermute | solution.py:21
  77.4 36.0 %collective-permute-start.43 = (bf16[1024,512]{1,0:T(8,128)(2,1)}, bf16[1024,512]{1,0:T(8,128)(2,1)S(1)}, u32[]{:S(2)}, u32[]{:S(2)}) collective-permute-start(bf16[1024,512]{1,0:T(8,128)(2,1)} %bitcast.47), channel_id=1, source_target_pairs={{0,2},{1,3},{2,0},{3,1},{4,6},{5,7},{6,4},{7,5},{8,10},{9,11},{10,... | collective-permute-start | bytes 3145736 | tf_op jit(solution)/shard_map/ppermute | solution.py:21
  78.2 20.4 %collective-permute-start.12 = (bf16[96,2048]{1,0:T(8,128)(2,1)S(1)}, bf16[96,2048]{1,0:T(8,128)(2,1)S(1)}, u32[]{:S(2)}, u32[]{:S(2)}) collective-permute-start(bf16[96,2048]{1,0:T(8,128)(2,1)S(1)} %pad_maximum_fusion.5.refs_0_), channel_id=1, source_target_pairs={{0,24},{4,28},{8,16},{12,20},{16,8},{20,12},{24,0},{28,4},{1,25},{... | collective-permute-start | bytes 1179656 | tf_op jit(solution)/shard_map/ppermute | solution.py:21
  98.6 33.8 %collective-permute-start.20 = (bf16[2048,256]{1,0:T(8,128)(2,1)S(1)}, bf16[2048,256]{1,0:T(8,128)(2,1)}, u32[]{:S(2)}, u32[]{:S(2)}) collective-permute-start(bf16[2048,256]{1,0:T(8,128)(2,1)S(1)} %bitcast.122), channel_id=1, source_target_pairs={{0,2},{1,3},{2,0},{3,1},{4,6},{5,7},{6,4},{7,5},{8,10},{9,11},{10,... | collective-permute-start | bytes 3145736 | tf_op jit(solution)/shard_map/ppermute | solution.py:21
  100.4 14.1 %collective-permute-start.14 = (bf16[96,2048]{1,0:T(8,128)(2,1)}, bf16[96,2048]{1,0:T(8,128)(2,1)S(1)}, u32[]{:S(2)}, u32[]{:S(2)}) collective-permute-start(bf16[96,2048]{1,0:T(8,128)(2,1)} %collective-permute-done.10.refs_1_), channel_id=1, source_target_pairs={{0,4},{4,0},{8,12},{12,8},{16,20},{20,16},{24,28},{28,24},{1,5},{5... | collective-permute-start | bytes 1179656 | tf_op jit(solution)/shard_map/ppermute | solution.py:21
  100.7 14.8 %collective-permute-start.15 = (bf16[96,2048]{1,0:T(8,128)(2,1)}, bf16[96,2048]{1,0:T(8,128)(2,1)S(1)}, u32[]{:S(2)}, u32[]{:S(2)}) collective-permute-start(bf16[96,2048]{1,0:T(8,128)(2,1)} %collective-permute-done.11.refs_2_), channel_id=1, source_target_pairs={{0,4},{4,0},{8,12},{12,8},{16,20},{20,16},{24,28},{28,24},{1,5},{5... | collective-permute-start | bytes 1179656 | tf_op jit(solution)/shard_map/ppermute | solution.py:21
  113.4 25.2 %collective-permute-start.23 = (bf16[1024,256]{1,0:T(8,128)(2,1)}, bf16[1024,256]{1,0:T(8,128)(2,1)}, u32[]{:S(2)}, u32[]{:S(2)}) collective-permute-start(bf16[1024,256]{1,0:T(8,128)(2,1)} %copy-done.7), channel_id=1, source_target_pairs={{0,2},{1,3},{2,0},{3,1},{4,6},{5,7},{6,4},{7,5},{8,10},{9,11},{10,... | collective-permute-start | bytes 1572872 | tf_op jit(solution)/shard_map/ppermute | solution.py:21
  114.5 33.4 %collective-permute-start.24 = (bf16[1024,256]{1,0:T(8,128)(2,1)}, bf16[1024,256]{1,0:T(8,128)(2,1)}, u32[]{:S(2)}, u32[]{:S(2)}) collective-permute-start(bf16[1024,256]{1,0:T(8,128)(2,1)} %copy-done.8), channel_id=1, source_target_pairs={{0,2},{1,3},{2,0},{3,1},{4,6},{5,7},{6,4},{7,5},{8,10},{9,11},{10,... | collective-permute-start | bytes 1572872 | tf_op jit(solution)/shard_map/ppermute | solution.py:21
  115.5 32.4 %collective-permute-start.25 = (bf16[1024,256]{1,0:T(8,128)(2,1)}, bf16[1024,256]{1,0:T(8,128)(2,1)}, u32[]{:S(2)}, u32[]{:S(2)}) collective-permute-start(bf16[1024,256]{1,0:T(8,128)(2,1)} %copy-done.9), channel_id=1, source_target_pairs={{0,1},{1,0},{2,3},{3,2},{4,5},{5,4},{6,7},{7,6},{8,9},{9,8},{10,11... | collective-permute-start | bytes 1572872 | tf_op jit(solution)/shard_map/ppermute | solution.py:21
  116.7 31.1 %collective-permute-start.26 = (bf16[1024,256]{1,0:T(8,128)(2,1)}, bf16[1024,256]{1,0:T(8,128)(2,1)}, u32[]{:S(2)}, u32[]{:S(2)}) collective-permute-start(bf16[1024,256]{1,0:T(8,128)(2,1)} %collective-permute-done.22.refs_3_), channel_id=1, source_target_pairs={{0,1},{1,0},{2,3},{3,2},{4,5},{5,4},{6,7},{7,6},{8,9},{9,8},{10,11... | collective-permute-start | bytes 1572872 | tf_op jit(solution)/shard_map/ppermute | solution.py:21
  132.4 36.4 %collective-permute-start.48 = (bf16[512,512]{1,0:T(8,128)(2,1)}, bf16[512,512]{1,0:T(8,128)(2,1)S(1)}, u32[]{:S(2)}, u32[]{:S(2)}) collective-permute-start(bf16[512,512]{1,0:T(8,128)(2,1)} %slice.256), channel_id=1, source_target_pairs={{0,2},{1,3},{2,0},{3,1},{4,6},{5,7},{6,4},{7,5},{8,10},{9,11},{10,... | collective-permute-start | bytes 1572872 | tf_op jit(solution)/shard_map/ppermute | solution.py:21
  138.6 31.4 %collective-permute-start.49 = (bf16[512,512]{1,0:T(8,128)(2,1)S(1)}, bf16[512,512]{1,0:T(8,128)(2,1)}, u32[]{:S(2)}, u32[]{:S(2)}) collective-permute-start(bf16[512,512]{1,0:T(8,128)(2,1)S(1)} %copy-done.6), channel_id=1, source_target_pairs={{0,1},{1,0},{2,3},{3,2},{4,5},{5,4},{6,7},{7,6},{8,9},{9,8},{10,11... | collective-permute-start | bytes 1572872 | tf_op jit(solution)/shard_map/ppermute | solution.py:21
  170.0 15.0 %collective-permute-start.46 = (bf16[96,512]{1,0:T(8,128)(2,1)S(1)}, bf16[96,512]{1,0:T(8,128)(2,1)S(1)}, u32[]{:S(2)}, u32[]{:S(2)}) collective-permute-start(bf16[96,512]{1,0:T(8,128)(2,1)S(1)} %get-tuple-element.68), channel_id=1, source_target_pairs={{0,16},{4,20},{8,24},{12,28},{16,0},{20,4},{24,8},{28,12},{1,17},{... | collective-permute-start | bytes 294920 | tf_op jit(solution)/shard_map/ppermute | solution.py:21
  177.0 20.7 %collective-permute-start.36 = (bf16[96,512]{1,0:T(8,128)(2,1)S(1)}, bf16[96,512]{1,0:T(8,128)(2,1)S(1)}, u32[]{:S(2)}, u32[]{:S(2)}) collective-permute-start(bf16[96,512]{1,0:T(8,128)(2,1)S(1)} %get-tuple-element.65), channel_id=1, source_target_pairs={{0,16},{4,20},{8,24},{12,28},{16,0},{20,4},{24,8},{28,12},{1,17},{... | collective-permute-start | bytes 294920 | tf_op jit(solution)/shard_map/ppermute | solution.py:21
  (64 other events, 631.8 us)

commit v4 on v3

v4 whole, which is shorter than its diff:
```python
import functools

import jax
import jax.numpy as jnp
from jax import lax
from jax.experimental import pallas as pl
from jax.experimental.pallas import tpu as pltpu
from jax.sharding import PartitionSpec as P


GROUP_W = 64
EPS = 1e-05
ALPHA = 8.0**0.25
HALO = 16
F32 = jnp.float32
BF16 = jnp.bfloat16


def swap_with(part, axis, bits):
    size = lax.axis_size(axis)
    return lax.ppermute(part, axis, [(i, i ^ bits) for i in range(size)])


def in_order(relative, index):
    stacked = jnp.stack(relative)
    return [
        lax.dynamic_index_in_dim(stacked, index ^ p, 0, keepdims=False)
        for p in range(len(relative))
    ]


def exchange_all(part, axis):
    return [part] + [swap_with(part, axis, k) for k in range(1, lax.axis_size(axis))]


def line_gather(part, axis):
    size = lax.axis_size(axis)
    mine = [part]
    for k in range(1, size // 2):
        mine.append(swap_with(part, axis, 2 * k))
    return mine + [swap_with(m, axis, 1) for m in mine]


TABLE = HALO + 8


def table_kernel(x_ref, docs_ref, table_ref):
    channels, positions = x_ref.shape
    docs = docs_ref[...].astype(F32).reshape(1, positions)
    last_doc = docs[:, positions - 1 :]
    ending = jnp.where(docs == last_doc, 1.0, 0.0)
    length = jnp.sum(ending, axis=1, keepdims=True)
    row = lax.broadcasted_iota(jnp.int32, (TABLE, positions), 0)
    col = lax.broadcasted_iota(jnp.int32, (TABLE, positions), 1)
    pick = jnp.where(col == positions - HALO + row, 1.0, 0.0)
    pick = jnp.where(row == HALO, jnp.broadcast_to(ending, pick.shape), pick)
    got = lax.dot_general(
        pick.astype(BF16), x_ref[...], (((1,), (1,)), ((), ())), preferred_element_type=F32
    )
    row = lax.broadcasted_iota(jnp.int32, (TABLE, channels), 0)
    got = jnp.where(row == HALO + 1, last_doc, got)
    table_ref[...] = jnp.where(row == HALO + 2, length, got)


def starts_of(docs_ref, positions):
    docs = jnp.broadcast_to(docs_ref[...].reshape(1, positions), (8, positions))
    lane = lax.broadcasted_iota(jnp.int32, (8, positions), 1)
    opens = (docs != pltpu.roll(docs, 1, 1)) & (lane > 0)
    start = jnp.where(opens, lane, 0)
    step = 1
    while step < positions:
        moved = pltpu.roll(start, step, 1)
        start = jnp.maximum(start, jnp.where(lane >= step, moved, 0))
        step *= 2
    return start


def units_of(channels, j):
    unit = min(GROUP_W, channels)
    for u in range(channels // unit):
        group = (j * channels + u * unit) // GROUP_W
        yield slice(u * unit, (u + 1) * unit), group % 2 == 1, lax.shift_left(2, group // 2 % 4)


def local_kernel(place_ref, x_ref, docs_ref, sum_ref, start_ref):
    channels, positions = x_ref.shape
    start_ref[...] = starts_of(docs_ref, positions)
    s_at = lax.broadcasted_iota(jnp.int32, (positions, positions), 0)
    t_at = lax.broadcasted_iota(jnp.int32, (positions, positions), 1)
    for rows, whole_doc, window in units_of(channels, place_ref[1]):
        reach = jnp.where(whole_doc, positions, window)
        lower = jnp.maximum(start_ref[:1, :], t_at[:1, :] + 1 - reach)
        mask = (s_at >= lower) & (s_at <= t_at)
        sum_ref[rows, :] = jnp.dot(
            x_ref[rows, :], mask.astype(BF16), preferred_element_type=F32
        )


def pooled_kernel(place_ref, x_ref, docs_ref, start_ref, sum_ref, *rest):
    *table_refs, out_ref = rest
    channels, positions = x_ref.shape
    i, j = place_ref[0], place_ref[1]
    first_doc = docs_ref[...].astype(F32).reshape(1, positions)[:, :1]
    before = jnp.zeros((TABLE, channels), F32)
    carried = jnp.zeros((TABLE, channels), F32)
    near_ref, *far_refs = table_refs
    for k in range(1, 2 * len(table_refs)):
        table = near_ref[...] if k == 1 else far_refs[k // 2 - 1][k % 2]
        earlier = jnp.where((i ^ k) < i, 1.0, 0.0)
        previous = jnp.where((i ^ k) == i - 1, 1.0, 0.0)
        same = jnp.where(table[HALO + 1 : HALO + 2, :1] == first_doc, earlier, 0.0)
        carried = carried + same * table
        before = before + previous * table
    count = carried[HALO + 2 : HALO + 3, :1]
    t_at = lax.broadcasted_iota(jnp.int32, (1, positions), 1)
    start = start_ref[:1, :]
    in_first = jnp.where(start == 0, 1.0, 0.0)
    doc_count = (t_at + 1 - start).astype(F32) + in_first * count
    row = lax.broadcasted_iota(jnp.int32, (TABLE, channels), 0)
    carry_row = jnp.where(row == HALO, carried, 0.0)
    over_first = jnp.broadcast_to(in_first, (TABLE, positions))
    carry = lax.dot_general(
        carry_row,
        over_first,
        (((0,), (0,)), ((), ())),
        precision=lax.Precision.HIGHEST,
        preferred_element_type=F32,
    )
    h_at = lax.broadcasted_iota(jnp.int32, (TABLE, positions), 0) - HALO
    reached = jnp.where(h_at.astype(F32) >= -count, over_first, 0.0)
    reached = jnp.where(h_at < 0, reached, 0.0)
    for rows, whole_doc, window in units_of(channels, j):
        halo_mask = jnp.where(h_at >= t_at + 1 - window, reached, 0.0)
        halo = lax.dot_general(
            before.astype(BF16),
            halo_mask.astype(BF16),
            (((0,), (0,)), ((), ())),
            preferred_element_type=F32,
        )
        whole = jnp.where(whole_doc, 1.0, 0.0)
        total = sum_ref[rows, :] + whole * carry[rows] + (1.0 - whole) * halo[rows]
        most = jnp.where(whole_doc, float(1 << 30), window.astype(F32))
        total = total / jnp.minimum(doc_count, most)
        out_ref[rows, :] = (total - x_ref[rows, :].astype(F32)).astype(BF16)


def in_vmem(count):
    return [pl.BlockSpec(memory_space=pltpu.VMEM)] * count


def room(mebibytes):
    return pltpu.CompilerParams(vmem_limit_bytes=mebibytes << 20)


def pooled_channels(pool_in, doc_ids, place):
    channels, positions = pool_in.shape
    scalars = pl.BlockSpec(memory_space=pltpu.SMEM)
    table = pl.pallas_call(
        table_kernel,
        out_shape=jax.ShapeDtypeStruct((TABLE, channels), F32),
        in_specs=in_vmem(2),
        out_specs=in_vmem(1)[0],
        compiler_params=room(4),
        name="table",
    )(pool_in, doc_ids)
    near = swap_with(table, "sp", 1)
    pair = jnp.stack([table, near])
    sums, start = pl.pallas_call(
        local_kernel,
        out_shape=(
            jax.ShapeDtypeStruct((channels, positions), F32),
            jax.ShapeDtypeStruct((8, positions), jnp.int32),
        ),
        in_specs=[scalars] + in_vmem(2),
        out_specs=tuple(in_vmem(2)),
        compiler_params=room(8),
        name="local",
    )(place, pool_in, doc_ids)
    far = [swap_with(pair, "sp", 2 * k) for k in range(1, lax.axis_size("sp") // 2)]
    return pl.pallas_call(
        pooled_kernel,
        out_shape=jax.ShapeDtypeStruct((channels, positions), BF16),
        in_specs=[scalars] + in_vmem(5 + len(far)),
        out_specs=in_vmem(1)[0],
        compiler_params=room(8),
        name="pooled",
    )(place, pool_in, doc_ids, start, sums, near, *far)


def norm_rows(rows, features):
    mean = sum(jnp.sum(r, axis=1, keepdims=True) for r in rows) / features
    square = sum(jnp.sum(r * r, axis=1, keepdims=True) for r in rows) / features
    scale = lax.rsqrt(square - mean * mean + EPS)
    return [(r - mean) * scale for r in rows]


def gather_rows_kernel(*refs):
    *parts, out_ref = refs
    rows = parts[0].shape[0]
    for p, part in enumerate(parts):
        out_ref[p * rows : (p + 1) * rows, :] = part[...]


def hidden_kernel(count, *refs):
    row_refs, weights, outs = refs[:count], refs[count:-1], refs[-1:]
    if count > 1:
        weights, outs = refs[count:-2], refs[-2:]
        gather_rows_kernel(*row_refs, outs[0])
    rows = outs[0] if count > 1 else row_refs[0]
    if len(weights) == 1:
        both = jnp.dot(rows[...], weights[0][...], preferred_element_type=F32)
        half = both.shape[1] // 2
        gated, up = both[:, :half], both[:, half:]
    else:
        gated, up = (
            jnp.dot(rows[...], w[...], preferred_element_type=F32) for w in weights
        )
    outs[-1][...] = (gated * jax.nn.sigmoid(gated) * up).astype(BF16)


def hidden_units(row_parts, weights):
    count = len(row_parts)
    rows = sum(r.shape[0] for r in row_parts)
    wide = sum(w.shape[1] for w in weights) // 2
    shape = jax.ShapeDtypeStruct((rows, wide), BF16)
    joined = jax.ShapeDtypeStruct((rows, row_parts[0].shape[1]), BF16)
    outs = (joined, shape) if count > 1 else (shape,)
    got = pl.pallas_call(
        functools.partial(hidden_kernel, count),
        out_shape=outs,
        in_specs=in_vmem(count + len(weights)),
        out_specs=tuple(in_vmem(len(outs))),
        compiler_params=room(20),
        name="hidden",
    )(*row_parts, *weights)
    return (got[0], got[-1])


def stage_kernel(*refs):
    parts = len(refs) // 3
    for k in range(parts):
        half = refs[2 * k].shape[1]
        refs[2 * parts + k][:, :half] = refs[2 * k][...]
        refs[2 * parts + k][:, half:] = refs[2 * k + 1][...]


def staged(pairs):
    flat = [w for pair in pairs for w in pair]
    return pl.pallas_call(
        stage_kernel,
        out_shape=tuple(
            jax.ShapeDtypeStruct((g.shape[0], 2 * g.shape[1]), BF16) for g, _ in pairs
        ),
        in_specs=in_vmem(len(flat)),
        out_specs=tuple(in_vmem(len(pairs))),
        compiler_params=room(16),
        name="stage",
    )(*flat)


def down_kernel(parts, place_ref, share_ref, *refs):
    hidden, weights, out_ref = refs[:parts], refs[parts:-1], refs[-1]
    depth, at = hidden[0].shape[1], 0
    for weight in weights:
        total = None
        for k in range(parts):
            rows = pl.ds(pl.multiple_of((place_ref[1] ^ k) * depth, depth), depth)
            piece = jnp.dot(hidden[k][...], weight[rows, :], preferred_element_type=F32)
            total = piece if total is None else total + piece
        wide = weight.shape[1]
        out_ref[:, at : at + wide] = (total * share_ref[...]).astype(BF16)
        at += wide


def weighted_outputs(place, share, hidden, weights):
    wide = sum(w.shape[1] for w in weights)
    return pl.pallas_call(
        functools.partial(down_kernel, len(hidden)),
        out_shape=jax.ShapeDtypeStruct((hidden[0].shape[0], wide), BF16),
        in_specs=[pl.BlockSpec(memory_space=pltpu.SMEM)]
        + in_vmem(1 + len(hidden) + len(weights)),
        out_specs=in_vmem(1)[0],
        compiler_params=room(14),
        name="down",
    )(place, share, *hidden, *weights)


def first_norm_kernel(parts, place_ref, *refs):
    rows, (tokens_ref, normed_ref, scale_ref) = refs[:parts], refs[parts:]
    count, wide = normed_ref.shape[1:]
    total = square = 0.0
    for ref in rows:
        part = ref[:count, :]
        total = total + jnp.sum(part, axis=1, keepdims=True)
        square = square + jnp.sum(part * part, axis=1, keepdims=True)
    mean = total / (parts * wide)
    scale = lax.rsqrt(square / (parts * wide) - mean * mean + EPS)
    for k, ref in enumerate(rows):
        gains = ref[count:, :]
        scale_ref[k] = gains
        part = (ref[:count, :] - mean) * scale * gains[:1] + gains[1:2]
        part = part.astype(BF16)
        normed_ref[k] = part
        at = pl.multiple_of((place_ref[1] ^ k) * wide, wide)
        tokens_ref[:, pl.ds(at, wide)] = part


def first_norm(place, rows, count):
    parts, wide = len(rows), rows[0].shape[1]
    tokens, normed, scales = pl.pallas_call(
        functools.partial(first_norm_kernel, parts),
        out_shape=(
            jax.ShapeDtypeStruct((count, parts * wide), BF16),
            jax.ShapeDtypeStruct((parts, count, wide), BF16),
            jax.ShapeDtypeStruct((parts, rows[0].shape[0] - count, wide), F32),
        ),
        in_specs=[pl.BlockSpec(memory_space=pltpu.SMEM)] + in_vmem(parts),
        out_specs=tuple(in_vmem(3)),
        compiler_params=room(8),
        name="norm",
    )(place, *rows)
    return tokens, [normed[k] for k in range(parts)], [scales[k] for k in range(parts)]


def weight_parts(w_gate, w_up, w_down, tp):
    if tp != 4:
        gate, up, down = (exchange_all(w, "tp") for w in (w_gate, w_up, w_down))
        return [list(pair) for pair in zip(gate, up)], [[w] for w in down]
    gate1 = swap_with(w_gate, "tp", 1)
    up2 = swap_with(w_up, "tp", 2)
    up1 = swap_with(w_up, "tp", 1)
    gate2 = swap_with(w_gate, "tp", 2)
    up3 = swap_with(up2, "tp", 1)
    gate3 = swap_with(gate1, "tp", 2)
    wide = w_down.shape[1] // 2
    left, right = w_down[:, :wide], w_down[:, wide:]
    down1_left = swap_with(left, "tp", 1)
    down2_right = swap_with(right, "tp", 2)
    down1_right = swap_with(right, "tp", 1)
    down2_left = swap_with(left, "tp", 2)
    down3_right = swap_with(down2_right, "tp", 1)
    down3_left = swap_with(down1_left, "tp", 2)
    near = staged([(w_gate, w_up), (gate1, up1), (gate2, up2)])
    first = [[w] for w in near] + [[gate3, up3]]
    down = [
        [w_down],
        [down1_left, down1_right],
        [down2_left, down2_right],
        [down3_left, down3_right],
    ]
    return first, down


def body(
    pool_in,
    doc_ids,
    pool_map,
    pool_scale,
    w_out,
    gate_logit,
    residual,
    first_gain,
    first_bias,
    routes,
    route_weight,
    w_gate,
    w_up,
    w_down,
    second_gain,
    second_bias,
):
    sp, tp = lax.axis_size("sp"), lax.axis_size("tp")
    i, j = lax.axis_index("sp"), lax.axis_index("tp")
    _, positions = pool_in.shape
    width = residual.shape[1]
    features = width * tp
    quarter = positions // tp

    place = jnp.stack([i, j])
    pooled = pooled_channels(pool_in, doc_ids, place)
    pooled_rel = exchange_all(pooled, "tp")
    my_routes = lax.dynamic_slice_in_dim(routes, j * quarter, quarter, 0)
    my_weights = lax.dynamic_slice_in_dim(route_weight, j * quarter, quarter, 0)
    chosen = jnp.stack([my_routes.astype(F32).T, my_weights.T])
    chosen = jnp.stack([chosen, swap_with(chosen, "sp", 1)])
    chosen = [chosen] + [swap_with(chosen, "sp", 2 * k) for k in range(1, sp // 2)]
    chosen = jnp.concatenate([c[core][None] for core in range(2) for c in chosen])
    chosen = jnp.where(chosen[:, 0] == i.astype(F32), chosen[:, 1], 0.0)
    share = jnp.sum(chosen, axis=1).reshape(-1, 1)

    gathered = jnp.concatenate(in_order(pooled_rel, j))
    group_count = gathered.shape[0] // GROUP_W
    grouped = jnp.einsum(
        "gct,gcd->tgd",
        gathered.reshape(group_count, GROUP_W, positions),
        pool_map,
        preferred_element_type=F32,
    )
    mapped = (grouped.reshape(positions, group_count * GROUP_W) * pool_scale).astype(BF16)
    mixer_out = jnp.dot(mapped, w_out, preferred_element_type=F32) * jax.nn.sigmoid(
        gate_logit.astype(F32)
    )
    mixed = ALPHA * residual.astype(F32) + mixer_out

    quarters = [
        lax.dynamic_slice_in_dim(mixed, (j ^ k) * quarter, quarter, 0) for k in range(tp)
    ]
    scales = jnp.pad(
        jnp.stack([first_gain, first_bias, second_gain, second_bias]), ((0, 4), (0, 0))
    )
    both = [jnp.concatenate([q, scales]) for q in quarters]
    both = [both[0]] + [swap_with(both[k], "tp", k) for k in range(1, tp)]
    tokens, normed_rel, gains = first_norm(place, both, quarter)

    down_own, tokens = lax.optimization_barrier((w_down[0], tokens))
    first_w, down_w = weight_parts(w_gate[0], w_up[0], down_own, tp)

    everyone = line_gather(tokens, "sp")
    inputs, first_hidden = hidden_units(everyone, first_w[0])
    hidden_rel = [first_hidden] + [
        hidden_units([inputs], first_w[k])[1] for k in range(1, tp)
    ]

    final_rel = []
    half_rows = (sp // 2) * quarter
    for k in range(tp):
        partial = weighted_outputs(place, share, hidden_rel, down_w[k])
        other = swap_with(partial[half_rows:], "sp", 1)
        joined = partial[:half_rows].astype(F32) + other.astype(F32)
        moe = joined[:quarter]
        sent = joined.astype(BF16)
        for d in range(1, sp // 2):
            got = swap_with(sent[d * quarter : (d + 1) * quarter], "sp", 2 * d)
            moe = moe + got.astype(F32)
        final_rel.append(ALPHA * normed_rel[k].astype(F32) + moe)
    out_rel = [
        (r * gains[k][2] + gains[k][3]).astype(BF16)
        for k, r in enumerate(norm_rows(final_rel, features))
    ]
    home_rel = [out_rel[0]] + [swap_with(out_rel[k], "tp", k) for k in range(1, tp)]
    return jnp.concatenate(in_order(home_rel, j))


def solution(mesh):
    return jax.shard_map(
        body,
        mesh=mesh,
        in_specs=(
            P("tp", "sp"),
            P("sp"),
            P(),
            P(),
            P(None, "tp"),
            P("sp", "tp"),
            P("sp", "tp"),
            P("tp"),
            P("tp"),
            P("sp", None),
            P("sp", None),
            P("sp", None, "tp"),
            P("sp", None, "tp"),
            P("sp", None, "tp"),
            P("tp"),
            P("tp"),
        ),
        out_specs=P("sp", "tp"),
        check_vma=False,
    )
```

time: 211 us -> 212 us (level)
  waiting for transfers between devices: 88.5 us -> 109 us
  starting transfers between devices: 67 us -> 55.2 us
  matrix products: 8.4 us -> 0.78 us
  local copies, waits for them, and re-layouts: 12.2 us -> 18.5 us
  Pallas kernels: 27.2 us -> 22.9 us
  other arithmetic: 6.89 us -> 3.99 us
    ppermute x57 -> x52, waiting for transfers between devices: 88.5 us -> 109 us  [swap_with(): return lax.ppermute(part, axis, [(i, i ^ bits) for i in range(size)])]
    pallas_call x4, Pallas kernels: 20.9 us -> 8.43 us  [hidden_units(): pl.pallas_call(functools.partial(hidden_kernel, count), out_shape=outs, i...]
    ppermute x57 -> x52, starting transfers between devices: 67 us -> 55.2 us  [swap_with(): return lax.ppermute(part, axis, [(i, i ^ bits) for i in range(size)])]
    unnamed x68 -> x78, local copies, waits for them, and re-layouts: 2.69 us -> 14.3 us
    pallas_call x2 -> x8, Pallas kernels: 4.13 us -> 13.4 us  [the longest x4 7.95 us: weighted_outputs(): pl.pallas_call(functools.partial(down_kernel, len(hidden)), out_shape=jax...]
    dot_general x4 -> x0, matrix products: 7.64 us -> none  [body(): result = jnp.dot(hidden, down_w[k], preferred_element_type=F32)]
    slice x4 -> x1, local copies, waits for them, and re-layouts: 6.94 us -> 1.15 us  [weight_parts(): left, right = (w_down[:, :wide], w_down[:, wide:])]
    another operation x5 -> x3, other arithmetic: 2.48 us -> 0.32 us  [in_order(): stacked = jnp.stack(relative)]
  transfers between devices with their start and end apart: 57 -> 52, of which waited for: 19 -> 21; matrix products, arithmetic and copies ran while one was open for 10% -> 5% of each run, Pallas kernels for 13% -> 10%
where the time goes in v4:
time: 212 us; the launch traced here: 211 us
  waiting for transfers between devices  109 us (51%)
  starting transfers between devices  55.2 us (26%)
  Pallas kernels  22.9 us (11%)
  local copies, waits for them, and re-layouts  18.5 us (9%)
  other arithmetic  3.99 us (2%)
    ppermute x52, waiting for transfers between devices, swap_with(): return lax.ppermute(part, axis, [(i, i ^ bits) for i in range(size)])  109 us
    ppermute x52, starting transfers between devices, swap_with(): return lax.ppermute(part, axis, [(i, i ^ bits) for i in range(size)])  55.2 us
    unnamed x78, local copies, waits for them, and re-layouts  14.3 us
    pallas_call x4, Pallas kernels, hidden_units(): pl.pallas_call(functools.partial(hidden_kernel, count), out_shape=outs, i...  8.43 us
    pallas_call x4, Pallas kernels, weighted_outputs(): pl.pallas_call(functools.partial(down_kernel, len(hidden)), out_shape=jax...  7.95 us
  transfers between devices with their start and end apart: 52, of which 21 were waited for; matrix products, arithmetic and copies ran while one was open for 5% of the time, Pallas kernels for 10%

profile of v4, /device:TPU:0, one launch (start us, length us, event | category | flops | bytes accessed | tf_op | source)
XLA Modules:
  0.0 211.4 jit_solution(1909698641336825181)
XLA Ops:
  3.2 2.9 %collective-permute-start.1 = (f32[2,24,128]{2,1,0:T(8,128)S(1)}, f32[2,24,128]{2,1,0:T(8,128)S(1)}, u32[]{:S(2)}, u32[]{:S(2)}) collective-permute-start(f32[2,24,128]{2,1,0:T(8,128)S(1)} %pad_maximum_fusion.8), channel_id=1, source_target_pairs={{0,8},{4,12},{8,0},{12,4},{16,24},{20,28},{24,16},{28,20},{1,9},{5... | collective-permute-start | bytes 73736 | tf_op jit(solution)/shard_map/ppermute | solution.py:21
  6.1 2.6 %collective-permute-start.2 = (f32[2,24,128]{2,1,0:T(8,128)S(1)}, f32[2,24,128]{2,1,0:T(8,128)S(1)}, u32[]{:S(2)}, u32[]{:S(2)}) collective-permute-start(f32[2,24,128]{2,1,0:T(8,128)S(1)} %pad_maximum_fusion.8), channel_id=1, source_target_pairs={{0,16},{4,20},{8,24},{12,28},{16,0},{20,4},{24,8},{28,12},{1,17},{... | collective-permute-start | bytes 73736 | tf_op jit(solution)/shard_map/ppermute | solution.py:21
  11.7 2.6 %collective-permute-done.3.rest_3_ = f32[2,24,128]{2,1,0:T(8,128)S(1)} collective-permute-done((f32[2,24,128]{2,1,0:T(8,128)S(1)}, f32[2,24,128]{2,1,0:T(8,128)S(1)}, u32[]{:S(2)}, u32[]{:S(2)}) %collective-permute-start.3) | collective-permute-done | bytes 24608 | tf_op jit(solution)/shard_map/ppermute | solution.py:21
  28.4 2.4 %collective-permute-start.9 = (f32[104,512]{1,0:T(8,128)S(1)}, f32[104,512]{1,0:T(8,128)S(1)}, u32[]{:S(2)}, u32[]{:S(2)}) collective-permute-start(f32[104,512]{1,0:T(8,128)S(1)} %get-tuple-element.91), channel_id=1, source_target_pairs={{0,3},{1,2},{2,1},{3,0},{4,7},{5,6},{6,5},{7,4},{8,11},{9,10},{10,... | collective-permute-start | bytes 638984 | tf_op jit(solution)/shard_map/ppermute | solution.py:21
  30.9 3.6 %collective-permute-done.7.refs_1_ = f32[104,512]{1,0:T(8,128)S(1)} collective-permute-done((f32[104,512]{1,0:T(8,128)S(1)}, f32[104,512]{1,0:T(8,128)S(1)}, u32[]{:S(2)}, u32[]{:S(2)}) %collective-permute-start.7) | collective-permute-done | bytes 213024 | tf_op jit(solution)/shard_map/ppermute | solution.py:21
  34.5 2.6 %collective-permute-done.8.refs_2_ = f32[104,512]{1,0:T(8,128)S(1)} collective-permute-done((f32[104,512]{1,0:T(8,128)S(1)}, f32[104,512]{1,0:T(8,128)S(1)}, u32[]{:S(2)}, u32[]{:S(2)}) %collective-permute-start.8) | collective-permute-done | bytes 213024 | tf_op jit(solution)/shard_map/ppermute | solution.py:21
  40.9 2.5 %collective-permute-start.15 = (bf16[96,2048]{1,0:T(8,128)(2,1)S(1)}, bf16[96,2048]{1,0:T(8,128)(2,1)S(1)}, u32[]{:S(2)}, u32[]{:S(2)}) collective-permute-start(bf16[96,2048]{1,0:T(8,128)(2,1)S(1)} %get-tuple-element.21.refs_0_), channel_id=1, source_target_pairs={{0,16},{4,20},{8,24},{12,28},{16,0},{20,4},{24,8},{28,12},{1,17},{... | collective-permute-start | bytes 1179656 | tf_op jit(solution)/shard_map/ppermute | solution.py:21
  44.6 2.8 %collective-permute-start.12 = (f32[2,2,2,96]{3,2,1,0:T(2,128)S(1)}, f32[2,2,2,96]{3,2,1,0:T(2,128)S(1)}, u32[]{:S(2)}, u32[]{:S(2)}) collective-permute-start(f32[2,2,2,96]{3,2,1,0:T(2,128)S(1)} %pad_maximum_fusion.9), channel_id=1, source_target_pairs={{0,16},{4,20},{8,24},{12,28},{16,0},{20,4},{24,8},{28,12},{1,17},{... | collective-permute-start | bytes 9224 | tf_op jit(solution)/shard_map/ppermute | solution.py:21
  47.4 5.6 %collective-permute-done.11 = f32[2,2,2,96]{3,2,1,0:T(2,128)} collective-permute-done((f32[2,2,2,96]{3,2,1,0:T(2,128)S(1)}, f32[2,2,2,96]{3,2,1,0:T(2,128)}, u32[]{:S(2)}, u32[]{:S(2)}) %collective-permute-start.11) | collective-permute-done | bytes 3104 | tf_op jit(solution)/shard_map/ppermute | solution.py:21
  54.9 2.9 %collective-permute-done.12 = f32[2,2,2,96]{3,2,1,0:T(2,128)S(1)} collective-permute-done((f32[2,2,2,96]{3,2,1,0:T(2,128)S(1)}, f32[2,2,2,96]{3,2,1,0:T(2,128)S(1)}, u32[]{:S(2)}, u32[]{:S(2)}) %collective-permute-start.12) | collective-permute-done | bytes 3104 | tf_op jit(solution)/shard_map/ppermute | solution.py:21
  63.2 5.7 %collective-permute-done.16.refs_3_ = bf16[96,2048]{1,0:T(8,128)(2,1)S(1)} collective-permute-done((bf16[96,2048]{1,0:T(8,128)(2,1)S(1)}, bf16[96,2048]{1,0:T(8,128)(2,1)S(1)}, u32[]{:S(2)}, u32[]{:S(2)}) %collective-permute-start.16) | collective-permute-done | bytes 393248 | tf_op jit(solution)/shard_map/ppermute | solution.py:21
  71.6 23.7 %collective-permute-done.38.refs_5_ = bf16[1024,256]{1,0:T(8,128)(2,1)S(1)} collective-permute-done((bf16[1024,256]{1,0:T(8,128)(2,1)}, bf16[1024,256]{1,0:T(8,128)(2,1)S(1)}, u32[]{:S(2)}, u32[]{:S(2)}) %collective-permute-start.38) | collective-permute-done | bytes 524320 | tf_op jit(solution)/shard_map/ppermute | solution.py:21
  100.8 9.6 %collective-permute-done.31.refs_4_ = bf16[1024,256]{1,0:T(8,128)(2,1)} collective-permute-done((bf16[1024,256]{1,0:T(8,128)(2,1)}, bf16[1024,256]{1,0:T(8,128)(2,1)}, u32[]{:S(2)}, u32[]{:S(2)}) %collective-permute-start.31) | collective-permute-done | bytes 524320 | tf_op jit(solution)/shard_map/ppermute | solution.py:21
  110.9 6.9 %collective-permute-done.23.refs_4_ = bf16[2048,256]{1,0:T(8,128)(2,1)} collective-permute-done((bf16[2048,256]{1,0:T(8,128)(2,1)S(1)}, bf16[2048,256]{1,0:T(8,128)(2,1)}, u32[]{:S(2)}, u32[]{:S(2)}) %collective-permute-start.23) | collective-permute-done | bytes 1048608 | tf_op jit(solution)/shard_map/ppermute | solution.py:21
  124.7 15.6 %collective-permute-done.25.refs_1_ = bf16[2048,256]{1,0:T(8,128)(2,1)S(1)} collective-permute-done((bf16[2048,256]{1,0:T(8,128)(2,1)}, bf16[2048,256]{1,0:T(8,128)(2,1)S(1)}, u32[]{:S(2)}, u32[]{:S(2)}) %collective-permute-start.25) | collective-permute-done | bytes 1048608 | tf_op jit(solution)/shard_map/ppermute | solution.py:21
  143.3 3.1 %stage.1 = (bf16[2048,512]{1,0:T(8,128)(2,1)S(1)}, bf16[2048,512]{1,0:T(8,128)(2,1)S(1)}, bf16[2048,512]{1,0:T(8,128)(2,1)S(1)}) custom-call(bf16[2048,256]{1,0:T(8,128)(2,1)S(1)} %bitcast.84, bf16[2048,256]{1,0:T(8,128)(2,1)} %bitcast.28.refs_1_, bf16[2048,256]{1,0:T(8,128)(2,1)} %collective-permute-done.21.refs_2_, ...), custom_call_target="tpu_custom_call" | custom-call | tf_op jit(solution)/shard_map/stage/pallas_call | solution.py:249
  152.1 3.0 %hidden.7.refs_3_ = bf16[768,256]{1,0:T(8,128)(2,1)S(1)} custom-call(bf16[768,2048]{1,0:T(8,128)(2,1)S(1)} %get-tuple-element.24.refs_0_, bf16[2048,256]{1,0:T(8,128)(2,1)S(1)} %copy-done.4, bf16[2048,256]{1,0:T(8,128)(2,1)} %collective-permute-done.26.refs_2_), custom_call_target="tpu_custom_call" | custom-call | tf_op jit(solution)/shard_map/hidden/pallas_call | solution.py:228
  159.7 2.2 %down.7 = bf16[768,512]{1,0:T(8,128)(2,1)S(1)} custom-call(s32[2]{0:T(128)S(1)} %pad_add_fusion.place_ref, f32[768,1]{1,0:T(8,128)S(1)} %reshape.93.share_ref, bf16[768,256]{1,0:T(8,128)(2,1)S(1)} %get-tuple-element.23.refs_0_, bf16[768,256]{1,0:T(8,128)(2,1)S(1)} %hidden.5.refs_1_, bf16[768,256]{1,0:T(8,128)(2,1)S(1)} %hidden.6.refs_2_, ...), custom_call_target="tpu_custom_call" | custom-call | tf_op jit(solution)/shard_map/down/pallas_call | solution.py:277
  162.7 2.2 %down.5 = bf16[768,512]{1,0:T(8,128)(2,1)S(1)} custom-call(s32[2]{0:T(128)S(1)} %pad_add_fusion.place_ref, f32[768,1]{1,0:T(8,128)S(1)} %reshape.93.share_ref, bf16[768,256]{1,0:T(8,128)(2,1)S(1)} %get-tuple-element.23.refs_0_, bf16[768,256]{1,0:T(8,128)(2,1)S(1)} %hidden.5.refs_1_, bf16[768,256]{1,0:T(8,128)(2,1)S(1)} %hidden.6.refs_2_, ...), custom_call_target="tpu_custom_call" | custom-call | tf_op jit(solution)/shard_map/down/pallas_call | solution.py:277
  165.8 2.5 %collective-permute-start.41 = (bf16[96,512]{1,0:T(8,128)(2,1)S(1)}, bf16[96,512]{1,0:T(8,128)(2,1)S(1)}, u32[]{:S(2)}, u32[]{:S(2)}) collective-permute-start(bf16[96,512]{1,0:T(8,128)(2,1)S(1)} %get-tuple-element.75), channel_id=1, source_target_pairs={{0,16},{4,20},{8,24},{12,28},{16,0},{20,4},{24,8},{28,12},{1,17},{... | collective-permute-start | bytes 294920 | tf_op jit(solution)/shard_map/ppermute | solution.py:21
  173.4 3.3 %collective-permute-done.41 = bf16[96,512]{1,0:T(8,128)(2,1)S(1)} collective-permute-done((bf16[96,512]{1,0:T(8,128)(2,1)S(1)}, bf16[96,512]{1,0:T(8,128)(2,1)S(1)}, u32[]{:S(2)}, u32[]{:S(2)}) %collective-permute-start.41) | collective-permute-done | bytes 98336 | tf_op jit(solution)/shard_map/ppermute | solution.py:21
  182.3 7.5 %collective-permute-done.29 = bf16[96,512]{1,0:T(8,128)(2,1)S(1)} collective-permute-done((bf16[96,512]{1,0:T(8,128)(2,1)S(1)}, bf16[96,512]{1,0:T(8,128)(2,1)S(1)}, u32[]{:S(2)}, u32[]{:S(2)}) %collective-permute-start.29) | collective-permute-done | bytes 98336 | tf_op jit(solution)/shard_map/ppermute | solution.py:21
  191.9 5.9 %collective-permute-done.47 = bf16[96,512]{1,0:T(8,128)(2,1)S(1)} collective-permute-done((bf16[96,512]{1,0:T(8,128)(2,1)S(1)}, bf16[96,512]{1,0:T(8,128)(2,1)S(1)}, u32[]{:S(2)}, u32[]{:S(2)}) %collective-permute-start.47) | collective-permute-done | bytes 98336 | tf_op jit(solution)/shard_map/ppermute | solution.py:21
  197.8 4.2 %collective-permute-done.35 = bf16[96,512]{1,0:T(8,128)(2,1)S(1)} collective-permute-done((bf16[96,512]{1,0:T(8,128)(2,1)S(1)}, bf16[96,512]{1,0:T(8,128)(2,1)S(1)}, u32[]{:S(2)}, u32[]{:S(2)}) %collective-permute-start.35) | collective-permute-done | bytes 98336 | tf_op jit(solution)/shard_map/ppermute | solution.py:21
  (211 shorter events, 84.6 us)
Async XLA Ops:
  39.3 21.8 %collective-permute-start.14 = (bf16[96,2048]{1,0:T(8,128)(2,1)S(1)}, bf16[96,2048]{1,0:T(8,128)(2,1)S(1)}, u32[]{:S(2)}, u32[]{:S(2)}) collective-permute-start(bf16[96,2048]{1,0:T(8,128)(2,1)S(1)} %get-tuple-element.21.refs_0_), channel_id=1, source_target_pairs={{0,8},{4,12},{8,0},{12,4},{16,24},{20,28},{24,16},{28,20},{1,9},{5... | collective-permute-start | bytes 1179656 | tf_op jit(solution)/shard_map/ppermute | solution.py:21
  40.9 21.5 %collective-permute-start.15 = (bf16[96,2048]{1,0:T(8,128)(2,1)S(1)}, bf16[96,2048]{1,0:T(8,128)(2,1)S(1)}, u32[]{:S(2)}, u32[]{:S(2)}) collective-permute-start(bf16[96,2048]{1,0:T(8,128)(2,1)S(1)} %get-tuple-element.21.refs_0_), channel_id=1, source_target_pairs={{0,16},{4,20},{8,24},{12,28},{16,0},{20,4},{24,8},{28,12},{1,17},{... | collective-permute-start | bytes 1179656 | tf_op jit(solution)/shard_map/ppermute | solution.py:21
  43.4 53.6 %collective-permute-start.21 = (bf16[2048,256]{1,0:T(8,128)(2,1)S(1)}, bf16[2048,256]{1,0:T(8,128)(2,1)}, u32[]{:S(2)}, u32[]{:S(2)}) collective-permute-start(bf16[2048,256]{1,0:T(8,128)(2,1)S(1)} %bitcast.82), channel_id=1, source_target_pairs={{0,1},{1,0},{2,3},{3,2},{4,5},{5,4},{6,7},{7,6},{8,9},{9,8},{10,11... | collective-permute-start | bytes 3145736 | tf_op jit(solution)/shard_map/ppermute | solution.py:21
  44.6 13.2 %collective-permute-start.12 = (f32[2,2,2,96]{3,2,1,0:T(2,128)S(1)}, f32[2,2,2,96]{3,2,1,0:T(2,128)S(1)}, u32[]{:S(2)}, u32[]{:S(2)}) collective-permute-start(f32[2,2,2,96]{3,2,1,0:T(2,128)S(1)} %pad_maximum_fusion.9), channel_id=1, source_target_pairs={{0,16},{4,20},{8,24},{12,28},{16,0},{20,4},{24,8},{28,12},{1,17},{... | collective-permute-start | bytes 9224 | tf_op jit(solution)/shard_map/ppermute | solution.py:21
  57.8 41.2 %collective-permute-start.24 = (bf16[2048,256]{1,0:T(8,128)(2,1)}, bf16[2048,256]{1,0:T(8,128)(2,1)}, u32[]{:S(2)}, u32[]{:S(2)}) collective-permute-start(bf16[2048,256]{1,0:T(8,128)(2,1)} %bitcast.28.refs_1_), channel_id=1, source_target_pairs={{0,2},{1,3},{2,0},{3,1},{4,6},{5,7},{6,4},{7,5},{8,10},{9,11},{10,... | collective-permute-start | bytes 3145736 | tf_op jit(solution)/shard_map/ppermute | solution.py:21
  62.4 32.9 %collective-permute-start.38 = (bf16[1024,256]{1,0:T(8,128)(2,1)}, bf16[1024,256]{1,0:T(8,128)(2,1)S(1)}, u32[]{:S(2)}, u32[]{:S(2)}) collective-permute-start(bf16[1024,256]{1,0:T(8,128)(2,1)} %get-tuple-element.51), channel_id=1, source_target_pairs={{0,2},{1,3},{2,0},{3,1},{4,6},{5,7},{6,4},{7,5},{8,10},{9,11},{10,... | collective-permute-start | bytes 1572872 | tf_op jit(solution)/shard_map/ppermute | solution.py:21
  68.9 41.5 %collective-permute-start.22 = (bf16[2048,256]{1,0:T(8,128)(2,1)}, bf16[2048,256]{1,0:T(8,128)(2,1)}, u32[]{:S(2)}, u32[]{:S(2)}) collective-permute-start(bf16[2048,256]{1,0:T(8,128)(2,1)} %bitcast.28.refs_1_), channel_id=1, source_target_pairs={{0,1},{1,0},{2,3},{3,2},{4,5},{5,4},{6,7},{7,6},{8,9},{9,8},{10,11... | collective-permute-start | bytes 3145736 | tf_op jit(solution)/shard_map/ppermute | solution.py:21
  70.7 47.2 %collective-permute-start.23 = (bf16[2048,256]{1,0:T(8,128)(2,1)S(1)}, bf16[2048,256]{1,0:T(8,128)(2,1)}, u32[]{:S(2)}, u32[]{:S(2)}) collective-permute-start(bf16[2048,256]{1,0:T(8,128)(2,1)S(1)} %bitcast.83), channel_id=1, source_target_pairs={{0,2},{1,3},{2,0},{3,1},{4,6},{5,7},{6,4},{7,5},{8,10},{9,11},{10,... | collective-permute-start | bytes 3145736 | tf_op jit(solution)/shard_map/ppermute | solution.py:21
  95.3 15.1 %collective-permute-start.31 = (bf16[1024,256]{1,0:T(8,128)(2,1)}, bf16[1024,256]{1,0:T(8,128)(2,1)}, u32[]{:S(2)}, u32[]{:S(2)}) collective-permute-start(bf16[1024,256]{1,0:T(8,128)(2,1)} %get-tuple-element.52), channel_id=1, source_target_pairs={{0,1},{1,0},{2,3},{3,2},{4,5},{5,4},{6,7},{7,6},{8,9},{9,8},{10,11... | collective-permute-start | bytes 1572872 | tf_op jit(solution)/shard_map/ppermute | solution.py:21
  97.1 43.1 %collective-permute-start.25 = (bf16[2048,256]{1,0:T(8,128)(2,1)}, bf16[2048,256]{1,0:T(8,128)(2,1)S(1)}, u32[]{:S(2)}, u32[]{:S(2)}) collective-permute-start(bf16[2048,256]{1,0:T(8,128)(2,1)} %collective-permute-done.21.refs_2_), channel_id=1, source_target_pairs={{0,2},{1,3},{2,0},{3,1},{4,6},{5,7},{6,4},{7,5},{8,10},{9,11},{10,... | collective-permute-start | bytes 3145736 | tf_op jit(solution)/shard_map/ppermute | solution.py:21
  99.0 53.0 %collective-permute-start.26 = (bf16[2048,256]{1,0:T(8,128)(2,1)}, bf16[2048,256]{1,0:T(8,128)(2,1)}, u32[]{:S(2)}, u32[]{:S(2)}) collective-permute-start(bf16[2048,256]{1,0:T(8,128)(2,1)} %collective-permute-done.24.refs_5_), channel_id=1, source_target_pairs={{0,1},{1,0},{2,3},{3,2},{4,5},{5,4},{6,7},{7,6},{8,9},{9,8},{10,11... | collective-permute-start | bytes 3145736 | tf_op jit(solution)/shard_map/ppermute | solution.py:21
  110.4 11.0 %collective-permute-start.19 = (bf16[96,2048]{1,0:T(8,128)(2,1)}, bf16[96,2048]{1,0:T(8,128)(2,1)S(1)}, u32[]{:S(2)}, u32[]{:S(2)}) collective-permute-start(bf16[96,2048]{1,0:T(8,128)(2,1)} %copy-done.14), channel_id=1, source_target_pairs={{0,4},{4,0},{8,12},{12,8},{16,20},{20,16},{24,28},{28,24},{1,5},{5... | collective-permute-start | bytes 1179656 | tf_op jit(solution)/shard_map/ppermute | solution.py:21
  119.3 35.8 %collective-permute-start.37 = (bf16[1024,256]{1,0:T(8,128)(2,1)}, bf16[1024,256]{1,0:T(8,128)(2,1)}, u32[]{:S(2)}, u32[]{:S(2)}) collective-permute-start(bf16[1024,256]{1,0:T(8,128)(2,1)} %get-tuple-element.52), channel_id=1, source_target_pairs={{0,2},{1,3},{2,0},{3,1},{4,6},{5,7},{6,4},{7,5},{8,10},{9,11},{10,... | collective-permute-start | bytes 1572872 | tf_op jit(solution)/shard_map/ppermute | solution.py:21
  122.2 40.5 %collective-permute-start.32 = (bf16[1024,256]{1,0:T(8,128)(2,1)}, bf16[1024,256]{1,0:T(8,128)(2,1)}, u32[]{:S(2)}, u32[]{:S(2)}) collective-permute-start(bf16[1024,256]{1,0:T(8,128)(2,1)} %get-tuple-element.51), channel_id=1, source_target_pairs={{0,1},{1,0},{2,3},{3,2},{4,5},{5,4},{6,7},{7,6},{8,9},{9,8},{10,11... | collective-permute-start | bytes 1572872 | tf_op jit(solution)/shard_map/ppermute | solution.py:21
  123.9 35.8 %collective-permute-start.43 = (bf16[1024,256]{1,0:T(8,128)(2,1)}, bf16[1024,256]{1,0:T(8,128)(2,1)}, u32[]{:S(2)}, u32[]{:S(2)}) collective-permute-start(bf16[1024,256]{1,0:T(8,128)(2,1)} %collective-permute-done.31.refs_4_), channel_id=1, source_target_pairs={{0,2},{1,3},{2,0},{3,1},{4,6},{5,7},{6,4},{7,5},{8,10},{9,11},{10,... | collective-permute-start | bytes 1572872 | tf_op jit(solution)/shard_map/ppermute | solution.py:21
  141.2 18.5 %collective-permute-start.44 = (bf16[1024,256]{1,0:T(8,128)(2,1)S(1)}, bf16[1024,256]{1,0:T(8,128)(2,1)}, u32[]{:S(2)}, u32[]{:S(2)}) collective-permute-start(bf16[1024,256]{1,0:T(8,128)(2,1)S(1)} %collective-permute-done.38.refs_5_), channel_id=1, source_target_pairs={{0,1},{1,0},{2,3},{3,2},{4,5},{5,4},{6,7},{7,6},{8,9},{9,8},{10,11... | collective-permute-start | bytes 1572872 | tf_op jit(solution)/shard_map/ppermute | solution.py:21
  170.7 11.5 %collective-permute-start.28 = (bf16[96,512]{1,0:T(8,128)(2,1)S(1)}, bf16[96,512]{1,0:T(8,128)(2,1)S(1)}, u32[]{:S(2)}, u32[]{:S(2)}) collective-permute-start(bf16[96,512]{1,0:T(8,128)(2,1)S(1)} %get-tuple-element.70), channel_id=1, source_target_pairs={{0,8},{4,12},{8,0},{12,4},{16,24},{20,28},{24,16},{28,20},{1,9},{5... | collective-permute-start | bytes 294920 | tf_op jit(solution)/shard_map/ppermute | solution.py:21
  172.9 16.9 %collective-permute-start.29 = (bf16[96,512]{1,0:T(8,128)(2,1)S(1)}, bf16[96,512]{1,0:T(8,128)(2,1)S(1)}, u32[]{:S(2)}, u32[]{:S(2)}) collective-permute-start(bf16[96,512]{1,0:T(8,128)(2,1)S(1)} %get-tuple-element.72), channel_id=1, source_target_pairs={{0,16},{4,20},{8,24},{12,28},{16,0},{20,4},{24,8},{28,12},{1,17},{... | collective-permute-start | bytes 294920 | tf_op jit(solution)/shard_map/ppermute | solution.py:21
  176.7 13.0 %collective-permute-start.30 = (bf16[96,512]{1,0:T(8,128)(2,1)S(1)}, bf16[96,512]{1,0:T(8,128)(2,1)S(1)}, u32[]{:S(2)}, u32[]{:S(2)}) collective-permute-start(bf16[96,512]{1,0:T(8,128)(2,1)S(1)} %get-tuple-element.71), channel_id=1, source_target_pairs={{0,24},{4,28},{8,16},{12,20},{16,8},{20,12},{24,0},{28,4},{1,25},{... | collective-permute-start | bytes 294920 | tf_op jit(solution)/shard_map/ppermute | solution.py:21
  178.7 19.1 %collective-permute-start.47 = (bf16[96,512]{1,0:T(8,128)(2,1)S(1)}, bf16[96,512]{1,0:T(8,128)(2,1)S(1)}, u32[]{:S(2)}, u32[]{:S(2)}) collective-permute-start(bf16[96,512]{1,0:T(8,128)(2,1)S(1)} %get-tuple-element.78), channel_id=1, source_target_pairs={{0,16},{4,20},{8,24},{12,28},{16,0},{20,4},{24,8},{28,12},{1,17},{... | collective-permute-start | bytes 294920 | tf_op jit(solution)/shard_map/ppermute | solution.py:21
  180.3 17.5 %collective-permute-start.48 = (bf16[96,512]{1,0:T(8,128)(2,1)S(1)}, bf16[96,512]{1,0:T(8,128)(2,1)S(1)}, u32[]{:S(2)}, u32[]{:S(2)}) collective-permute-start(bf16[96,512]{1,0:T(8,128)(2,1)S(1)} %get-tuple-element.77), channel_id=1, source_target_pairs={{0,24},{4,28},{8,16},{12,20},{16,8},{20,12},{24,0},{28,4},{1,25},{... | collective-permute-start | bytes 294920 | tf_op jit(solution)/shard_map/ppermute | solution.py:21
  182.2 15.6 %collective-permute-start.34 = (bf16[96,512]{1,0:T(8,128)(2,1)S(1)}, bf16[96,512]{1,0:T(8,128)(2,1)S(1)}, u32[]{:S(2)}, u32[]{:S(2)}) collective-permute-start(bf16[96,512]{1,0:T(8,128)(2,1)S(1)} %get-tuple-element.67), channel_id=1, source_target_pairs={{0,8},{4,12},{8,0},{12,4},{16,24},{20,28},{24,16},{28,20},{1,9},{5... | collective-permute-start | bytes 294920 | tf_op jit(solution)/shard_map/ppermute | solution.py:21
  189.8 12.2 %collective-permute-start.35 = (bf16[96,512]{1,0:T(8,128)(2,1)S(1)}, bf16[96,512]{1,0:T(8,128)(2,1)S(1)}, u32[]{:S(2)}, u32[]{:S(2)}) collective-permute-start(bf16[96,512]{1,0:T(8,128)(2,1)S(1)} %get-tuple-element.69), channel_id=1, source_target_pairs={{0,16},{4,20},{8,24},{12,28},{16,0},{20,4},{24,8},{28,12},{1,17},{... | collective-permute-start | bytes 294920 | tf_op jit(solution)/shard_map/ppermute | solution.py:21
  189.8 12.2 %collective-permute-start.36 = (bf16[96,512]{1,0:T(8,128)(2,1)S(1)}, bf16[96,512]{1,0:T(8,128)(2,1)S(1)}, u32[]{:S(2)}, u32[]{:S(2)}) collective-permute-start(bf16[96,512]{1,0:T(8,128)(2,1)S(1)} %get-tuple-element.68), channel_id=1, source_target_pairs={{0,24},{4,28},{8,16},{12,20},{16,8},{20,12},{24,0},{28,4},{1,25},{... | collective-permute-start | bytes 294920 | tf_op jit(solution)/shard_map/ppermute | solution.py:21
  (64 other events, 489.6 us)

commit v5 on v4

--- a/solution.py
+++ b/solution.py
@@ -187,13 +187,6 @@
     )(place, pool_in, doc_ids, start, sums, near, *far)
 
 
-def norm_rows(rows, features):
-    mean = sum(jnp.sum(r, axis=1, keepdims=True) for r in rows) / features
-    square = sum(jnp.sum(r * r, axis=1, keepdims=True) for r in rows) / features
-    scale = lax.rsqrt(square - mean * mean + EPS)
-    return [(r - mean) * scale for r in rows]
-
-
 def gather_rows_kernel(*refs):
     *parts, out_ref = refs
     rows = parts[0].shape[0]
@@ -319,13 +312,84 @@
         compiler_params=room(8),
         name="norm",
     )(place, *rows)
-    return tokens, [normed[k] for k in range(parts)], [scales[k] for k in range(parts)]
+    return tokens, normed, scales
+
+
+def share_kernel(place_ref, *refs):
+    *tables, out_ref = refs
+    count = tables[0].shape[-1]
+    mine = place_ref[0].astype(F32)
+    rows = []
+    for core in range(2):
+        for table in tables:
+            chosen = jnp.where(table[core, 0] == mine, table[core, 1], 0.0)
+            rows.append(jnp.sum(chosen, axis=0, keepdims=True))
+    rows = jnp.concatenate(rows)
+    row = lax.broadcasted_iota(jnp.int32, (count, count), 0)
+    col = lax.broadcasted_iota(jnp.int32, (count, count), 1)
+    columns = lax.dot_general(
+        jnp.where(row == col, 1.0, 0.0),
+        rows,
+        (((1,), (1,)), ((), ())),
+        precision=lax.Precision.HIGHEST,
+        preferred_element_type=F32,
+    )
+    for slot in range(rows.shape[0]):
+        out_ref[slot * count : (slot + 1) * count, :] = columns[:, slot : slot + 1]
+
+
+def token_shares(place, tables):
+    slots, count = 2 * len(tables), tables[0].shape[-1]
+    return pl.pallas_call(
+        share_kernel,
+        out_shape=jax.ShapeDtypeStruct((slots * count, 1), F32),
+        in_specs=[pl.BlockSpec(memory_space=pltpu.SMEM)] + in_vmem(len(tables)),
+        out_specs=in_vmem(1)[0],
+        compiler_params=room(4),
+        name="share",
+    )(place, *tables)
+
+
+def last_norm_kernel(parts, arrange, normed_ref, scale_ref, *refs):
+    outs, refs = refs[-parts:], refs[:-parts]
+    each = len(refs) // parts
+    sums = []
+    for k in range(parts):
+        own, *others = refs[k * each : (k + 1) * each]
+        total = own[...]
+        for other in others:
+            total = total + other[...].astype(F32)
+        sums.append(total)
+    rows = [
+        ALPHA * normed_ref[k].astype(F32) + part for k, part in enumerate(arrange(*sums))
+    ]
+    features = sum(r.shape[1] for r in rows)
+    mean = sum(jnp.sum(r, axis=1, keepdims=True) for r in rows) / features
+    square = sum(jnp.sum(r * r, axis=1, keepdims=True) for r in rows) / features
+    scale = lax.rsqrt(square - mean * mean + EPS)
+    for k, out_ref in enumerate(outs):
+        part = (rows[k] - mean) * scale * scale_ref[k, 2:3, :] + scale_ref[k, 3:4, :]
+        out_ref[...] = part.astype(BF16)
+
+
+def last_norm(arrange, normed, scales, groups):
+    parts, count, wide = normed.shape
+    flat = [r for group in groups for r in group]
+    return pl.pallas_call(
+        functools.partial(last_norm_kernel, parts, arrange),
+        out_shape=tuple(jax.ShapeDtypeStruct((count, wide), BF16) for _ in groups),
+        in_specs=in_vmem(2 + len(flat)),
+        out_specs=tuple(in_vmem(parts)),
+        compiler_params=room(12),
+        name="last",
+    )(normed, scales, *flat)
 
 
 def weight_parts(w_gate, w_up, w_down, tp):
     if tp != 4:
         gate, up, down = (exchange_all(w, "tp") for w in (w_gate, w_up, w_down))
-        return [list(pair) for pair in zip(gate, up)], [[w] for w in down]
+        pairs = [list(pair) for pair in zip(gate, up)]
+        return pairs, [[w] for w in down], lambda *parts: list(parts)
     gate1 = swap_with(w_gate, "tp", 1)
     up2 = swap_with(w_up, "tp", 2)
     up1 = swap_with(w_up, "tp", 1)
@@ -344,11 +408,17 @@
     first = [[w] for w in near] + [[gate3, up3]]
     down = [
         [w_down],
-        [down1_left, down1_right],
-        [down2_left, down2_right],
+        [down1_left, down2_right],
+        [down1_right, down2_left],
         [down3_left, down3_right],
     ]
-    return first, down
+
+    def by_distance(own, early, late, last):
+        one = jnp.concatenate([early[:, :wide], late[:, :wide]], axis=1)
+        two = jnp.concatenate([late[:, wide:], early[:, wide:]], axis=1)
+        return [own, one, two, last]
+
+    return first, down, by_distance
 
 
 def body(
@@ -372,8 +442,6 @@
     sp, tp = lax.axis_size("sp"), lax.axis_size("tp")
     i, j = lax.axis_index("sp"), lax.axis_index("tp")
     _, positions = pool_in.shape
-    width = residual.shape[1]
-    features = width * tp
     quarter = positions // tp
 
     place = jnp.stack([i, j])
@@ -384,9 +452,7 @@
     chosen = jnp.stack([my_routes.astype(F32).T, my_weights.T])
     chosen = jnp.stack([chosen, swap_with(chosen, "sp", 1)])
     chosen = [chosen] + [swap_with(chosen, "sp", 2 * k) for k in range(1, sp // 2)]
-    chosen = jnp.concatenate([c[core][None] for core in range(2) for c in chosen])
-    chosen = jnp.where(chosen[:, 0] == i.astype(F32), chosen[:, 1], 0.0)
-    share = jnp.sum(chosen, axis=1).reshape(-1, 1)
+    share = token_shares(place, chosen)
 
     gathered = jnp.concatenate(in_order(pooled_rel, j))
     group_count = gathered.shape[0] // GROUP_W
@@ -410,10 +476,10 @@
     )
     both = [jnp.concatenate([q, scales]) for q in quarters]
     both = [both[0]] + [swap_with(both[k], "tp", k) for k in range(1, tp)]
-    tokens, normed_rel, gains = first_norm(place, both, quarter)
+    tokens, normed, scales = first_norm(place, both, quarter)
 
     down_own, tokens = lax.optimization_barrier((w_down[0], tokens))
-    first_w, down_w = weight_parts(w_gate[0], w_up[0], down_own, tp)
+    first_w, down_w, by_distance = weight_parts(w_gate[0], w_up[0], down_own, tp)
 
     everyone = line_gather(tokens, "sp")
     inputs, first_hidden = hidden_units(everyone, first_w[0])
@@ -421,22 +487,19 @@
         hidden_units([inputs], first_w[k])[1] for k in range(1, tp)
     ]
 
-    final_rel = []
+    groups = []
     half_rows = (sp // 2) * quarter
     for k in range(tp):
         partial = weighted_outputs(place, share, hidden_rel, down_w[k])
         other = swap_with(partial[half_rows:], "sp", 1)
         joined = partial[:half_rows].astype(F32) + other.astype(F32)
-        moe = joined[:quarter]
         sent = joined.astype(BF16)
-        for d in range(1, sp // 2):
-            got = swap_with(sent[d * quarter : (d + 1) * quarter], "sp", 2 * d)
-            moe = moe + got.astype(F32)
-        final_rel.append(ALPHA * normed_rel[k].astype(F32) + moe)
-    out_rel = [
-        (r * gains[k][2] + gains[k][3]).astype(BF16)
-        for k, r in enumerate(norm_rows(final_rel, features))
-    ]
+        got = [
+            swap_with(sent[d * quarter : (d + 1) * quarter], "sp", 2 * d)
+            for d in range(1, sp // 2)
+        ]
+        groups.append([joined[:quarter]] + got)
+    out_rel = last_norm(by_distance, normed, scales, groups)
     home_rel = [out_rel[0]] + [swap_with(out_rel[k], "tp", k) for k in range(1, tp)]
     return jnp.concatenate(in_order(home_rel, j))
 

time: 212 us -> 225 us (1.061)
  waiting for transfers between devices: 109 us -> 129 us
  local copies, waits for them, and re-layouts: 18.5 us -> 6.54 us
  starting transfers between devices: 55.2 us -> 65.8 us
  Pallas kernels: 22.9 us -> 18.6 us
    ppermute x52, waiting for transfers between devices: 109 us -> 129 us  [swap_with(): return lax.ppermute(part, axis, [(i, i ^ bits) for i in range(size)])]
    ppermute x52, starting transfers between devices: 55.2 us -> 65.8 us  [swap_with(): return lax.ppermute(part, axis, [(i, i ^ bits) for i in range(size)])]
    unnamed x78 -> x28, local copies, waits for them, and re-layouts: 14.3 us -> 5.31 us
    pallas_call x1, Pallas kernels: 3.13 us -> 0.49 us  [staged(): pl.pallas_call(stage_kernel, out_shape=tuple((jax.ShapeDtypeStruct((g.sha...]
  transfers between devices with their start and end apart: 52 -> 52, of which waited for: 21 -> 24; matrix products, arithmetic and copies ran while one was open for 5% -> 1% of each run, Pallas kernels for 10% -> 7%
where the time goes in v5:
time: 225 us; the launch traced here: 224 us
  waiting for transfers between devices  129 us (57%)
  starting transfers between devices  65.8 us (29%)
  Pallas kernels  18.6 us (8%)
  local copies, waits for them, and re-layouts  6.54 us (3%)
  other arithmetic  3.23 us (1%)
    ppermute x52, waiting for transfers between devices, swap_with(): return lax.ppermute(part, axis, [(i, i ^ bits) for i in range(size)])  129 us
    ppermute x52, starting transfers between devices, swap_with(): return lax.ppermute(part, axis, [(i, i ^ bits) for i in range(size)])  65.8 us
    pallas_call x4, Pallas kernels, hidden_units(): pl.pallas_call(functools.partial(hidden_kernel, count), out_shape=outs, i...  7.19 us
    pallas_call x4, Pallas kernels, weighted_outputs(): pl.pallas_call(functools.partial(down_kernel, len(hidden)), out_shape=jax...  6.27 us
    unnamed x28, local copies, waits for them, and re-layouts  5.31 us
  transfers between devices with their start and end apart: 52, of which 24 were waited for; matrix products, arithmetic and copies ran while one was open for 1% of the time, Pallas kernels for 7%

profile of v5, /device:TPU:0, one launch (start us, length us, event | category | flops | bytes accessed | tf_op | source)
XLA Modules:
  0.0 224.2 jit_solution(16301060393461339162)
XLA Ops:
  3.2 2.9 %collective-permute-start.1 = (f32[2,24,128]{2,1,0:T(8,128)S(1)}, f32[2,24,128]{2,1,0:T(8,128)S(1)}, u32[]{:S(2)}, u32[]{:S(2)}) collective-permute-start(f32[2,24,128]{2,1,0:T(8,128)S(1)} %pad_maximum_fusion.8), channel_id=1, source_target_pairs={{0,8},{4,12},{8,0},{12,4},{16,24},{20,28},{24,16},{28,20},{1,9},{5... | collective-permute-start | bytes 73736 | tf_op jit(solution)/shard_map/ppermute | solution.py:21
  6.1 2.6 %collective-permute-start.2 = (f32[2,24,128]{2,1,0:T(8,128)S(1)}, f32[2,24,128]{2,1,0:T(8,128)S(1)}, u32[]{:S(2)}, u32[]{:S(2)}) collective-permute-start(f32[2,24,128]{2,1,0:T(8,128)S(1)} %pad_maximum_fusion.8), channel_id=1, source_target_pairs={{0,16},{4,20},{8,24},{12,28},{16,0},{20,4},{24,8},{28,12},{1,17},{... | collective-permute-start | bytes 73736 | tf_op jit(solution)/shard_map/ppermute | solution.py:21
  11.7 2.6 %collective-permute-done.3.rest_3_ = f32[2,24,128]{2,1,0:T(8,128)S(1)} collective-permute-done((f32[2,24,128]{2,1,0:T(8,128)S(1)}, f32[2,24,128]{2,1,0:T(8,128)S(1)}, u32[]{:S(2)}, u32[]{:S(2)}) %collective-permute-start.3) | collective-permute-done | bytes 24608 | tf_op jit(solution)/shard_map/ppermute | solution.py:21
  28.4 2.4 %collective-permute-start.9 = (f32[104,512]{1,0:T(8,128)S(1)}, f32[104,512]{1,0:T(8,128)S(1)}, u32[]{:S(2)}, u32[]{:S(2)}) collective-permute-start(f32[104,512]{1,0:T(8,128)S(1)} %get-tuple-element.71), channel_id=1, source_target_pairs={{0,3},{1,2},{2,1},{3,0},{4,7},{5,6},{6,5},{7,4},{8,11},{9,10},{10,... | collective-permute-start | bytes 638984 | tf_op jit(solution)/shard_map/ppermute | solution.py:21
  30.9 3.6 %collective-permute-done.7.refs_1_ = f32[104,512]{1,0:T(8,128)S(1)} collective-permute-done((f32[104,512]{1,0:T(8,128)S(1)}, f32[104,512]{1,0:T(8,128)S(1)}, u32[]{:S(2)}, u32[]{:S(2)}) %collective-permute-start.7) | collective-permute-done | bytes 213024 | tf_op jit(solution)/shard_map/ppermute | solution.py:21
  34.5 2.6 %collective-permute-done.8.refs_2_ = f32[104,512]{1,0:T(8,128)S(1)} collective-permute-done((f32[104,512]{1,0:T(8,128)S(1)}, f32[104,512]{1,0:T(8,128)S(1)}, u32[]{:S(2)}, u32[]{:S(2)}) %collective-permute-start.8) | collective-permute-done | bytes 213024 | tf_op jit(solution)/shard_map/ppermute | solution.py:21
  39.6 2.5 %collective-permute-start.15 = (bf16[96,2048]{1,0:T(8,128)(2,1)S(1)}, bf16[96,2048]{1,0:T(8,128)(2,1)S(1)}, u32[]{:S(2)}, u32[]{:S(2)}) collective-permute-start(bf16[96,2048]{1,0:T(8,128)(2,1)S(1)} %get-tuple-element.26.refs_0_), channel_id=1, source_target_pairs={{0,16},{4,20},{8,24},{12,28},{16,0},{20,4},{24,8},{28,12},{1,17},{... | collective-permute-start | bytes 1179656 | tf_op jit(solution)/shard_map/ppermute | solution.py:21
  42.1 1.8 collective-permute-start.16
  45.1 2.6 %collective-permute-start.12 = (f32[2,2,2,96]{3,2,1,0:T(2,128)S(1)}, f32[2,2,2,96]{3,2,1,0:T(2,128)S(1)}, u32[]{:S(2)}, u32[]{:S(2)}) collective-permute-start(f32[2,2,2,96]{3,2,1,0:T(2,128)S(1)} %pad_maximum_fusion.9.refs_0_), channel_id=1, source_target_pairs={{0,16},{4,20},{8,24},{12,28},{16,0},{20,4},{24,8},{28,12},{1,17},{... | collective-permute-start | bytes 9224 | tf_op jit(solution)/shard_map/ppermute | solution.py:21
  47.7 12.5 %collective-permute-done.11.refs_1_ = f32[2,2,2,96]{3,2,1,0:T(2,128)S(1)} collective-permute-done((f32[2,2,2,96]{3,2,1,0:T(2,128)S(1)}, f32[2,2,2,96]{3,2,1,0:T(2,128)S(1)}, u32[]{:S(2)}, u32[]{:S(2)}) %collective-permute-start.11) | collective-permute-done | bytes 3104 | tf_op jit(solution)/shard_map/ppermute | solution.py:21
  60.2 1.9 collective-permute-start.13
  62.0 11.4 %collective-permute-done.12.refs_2_ = f32[2,2,2,96]{3,2,1,0:T(2,128)S(1)} collective-permute-done((f32[2,2,2,96]{3,2,1,0:T(2,128)S(1)}, f32[2,2,2,96]{3,2,1,0:T(2,128)S(1)}, u32[]{:S(2)}, u32[]{:S(2)}) %collective-permute-start.12) | collective-permute-done | bytes 3104 | tf_op jit(solution)/shard_map/ppermute | solution.py:21
  78.7 31.9 %collective-permute-done.31.refs_4_ = bf16[1024,256]{1,0:T(8,128)(2,1)S(1)} collective-permute-done((bf16[1024,256]{1,0:T(8,128)(2,1)S(1)}, bf16[1024,256]{1,0:T(8,128)(2,1)S(1)}, u32[]{:S(2)}, u32[]{:S(2)}) %collective-permute-start.31) | collective-permute-done | bytes 524320 | tf_op jit(solution)/shard_map/ppermute | solution.py:21
  113.8 20.4 %collective-permute-done.32.refs_5_ = bf16[1024,256]{1,0:T(8,128)(2,1)S(1)} collective-permute-done((bf16[1024,256]{1,0:T(8,128)(2,1)S(1)}, bf16[1024,256]{1,0:T(8,128)(2,1)S(1)}, u32[]{:S(2)}, u32[]{:S(2)}) %collective-permute-start.32) | collective-permute-done | bytes 524320 | tf_op jit(solution)/shard_map/ppermute | solution.py:21
  139.3 17.5 %collective-permute-done.25.refs_1_ = bf16[2048,256]{1,0:T(8,128)(2,1)S(1)} collective-permute-done((bf16[2048,256]{1,0:T(8,128)(2,1)S(1)}, bf16[2048,256]{1,0:T(8,128)(2,1)S(1)}, u32[]{:S(2)}, u32[]{:S(2)}) %collective-permute-start.25) | collective-permute-done | bytes 1048608 | tf_op jit(solution)/shard_map/ppermute | solution.py:21
  159.4 1.8 hidden.4
  164.8 1.8 hidden.7.refs_3_
  171.1 2.6 %collective-permute-done.37.refs_4_ = bf16[1024,256]{1,0:T(8,128)(2,1)S(1)} collective-permute-done((bf16[1024,256]{1,0:T(8,128)(2,1)S(1)}, bf16[1024,256]{1,0:T(8,128)(2,1)S(1)}, u32[]{:S(2)}, u32[]{:S(2)}) %collective-permute-start.37) | collective-permute-done | bytes 524320 | tf_op jit(solution)/shard_map/ppermute | solution.py:21
  179.0 2.9 %collective-permute-start.47 = (bf16[96,512]{1,0:T(8,128)(2,1)S(1)}, bf16[96,512]{1,0:T(8,128)(2,1)S(1)}, u32[]{:S(2)}, u32[]{:S(2)}) collective-permute-start(bf16[96,512]{1,0:T(8,128)(2,1)S(1)} %get-tuple-element.56), channel_id=1, source_target_pairs={{0,16},{4,20},{8,24},{12,28},{16,0},{20,4},{24,8},{28,12},{1,17},{... | collective-permute-start | bytes 294920 | tf_op jit(solution)/shard_map/ppermute | solution.py:21
  183.5 3.3 %collective-permute-start.41 = (bf16[96,512]{1,0:T(8,128)(2,1)S(1)}, bf16[96,512]{1,0:T(8,128)(2,1)S(1)}, u32[]{:S(2)}, u32[]{:S(2)}) collective-permute-start(bf16[96,512]{1,0:T(8,128)(2,1)S(1)} %get-tuple-element.59), channel_id=1, source_target_pairs={{0,16},{4,20},{8,24},{12,28},{16,0},{20,4},{24,8},{28,12},{1,17},{... | collective-permute-start | bytes 294920 | tf_op jit(solution)/shard_map/ppermute | solution.py:21
  189.9 7.8 %collective-permute-start.35 = (bf16[96,512]{1,0:T(8,128)(2,1)S(1)}, bf16[96,512]{1,0:T(8,128)(2,1)S(1)}, u32[]{:S(2)}, u32[]{:S(2)}) collective-permute-start(bf16[96,512]{1,0:T(8,128)(2,1)S(1)} %get-tuple-element.62), channel_id=1, source_target_pairs={{0,16},{4,20},{8,24},{12,28},{16,0},{20,4},{24,8},{28,12},{1,17},{... | collective-permute-start | bytes 294920 | tf_op jit(solution)/shard_map/ppermute | solution.py:21
  199.4 6.7 %collective-permute-start.29 = (bf16[96,512]{1,0:T(8,128)(2,1)S(1)}, bf16[96,512]{1,0:T(8,128)(2,1)S(1)}, u32[]{:S(2)}, u32[]{:S(2)}) collective-permute-start(bf16[96,512]{1,0:T(8,128)(2,1)S(1)} %get-tuple-element.65), channel_id=1, source_target_pairs={{0,16},{4,20},{8,24},{12,28},{16,0},{20,4},{24,8},{28,12},{1,17},{... | collective-permute-start | bytes 294920 | tf_op jit(solution)/shard_map/ppermute | solution.py:21
  207.8 7.4 %collective-permute-done.29.refs_2_ = bf16[96,512]{1,0:T(8,128)(2,1)S(1)} collective-permute-done((bf16[96,512]{1,0:T(8,128)(2,1)S(1)}, bf16[96,512]{1,0:T(8,128)(2,1)S(1)}, u32[]{:S(2)}, u32[]{:S(2)}) %collective-permute-start.29) | collective-permute-done | bytes 98336 | tf_op jit(solution)/shard_map/ppermute | solution.py:21
  219.3 2.2 collective-permute-done.49
  (158 shorter events, 68.0 us)
Async XLA Ops:
  38.0 37.8 %collective-permute-start.14 = (bf16[96,2048]{1,0:T(8,128)(2,1)S(1)}, bf16[96,2048]{1,0:T(8,128)(2,1)S(1)}, u32[]{:S(2)}, u32[]{:S(2)}) collective-permute-start(bf16[96,2048]{1,0:T(8,128)(2,1)S(1)} %get-tuple-element.26.refs_0_), channel_id=1, source_target_pairs={{0,8},{4,12},{8,0},{12,4},{16,24},{20,28},{24,16},{28,20},{1,9},{5... | collective-permute-start | bytes 1179656 | tf_op jit(solution)/shard_map/ppermute | solution.py:21
  39.6 36.3 %collective-permute-start.15 = (bf16[96,2048]{1,0:T(8,128)(2,1)S(1)}, bf16[96,2048]{1,0:T(8,128)(2,1)S(1)}, u32[]{:S(2)}, u32[]{:S(2)}) collective-permute-start(bf16[96,2048]{1,0:T(8,128)(2,1)S(1)} %get-tuple-element.26.refs_0_), channel_id=1, source_target_pairs={{0,16},{4,20},{8,24},{12,28},{16,0},{20,4},{24,8},{28,12},{1,17},{... | collective-permute-start | bytes 1179656 | tf_op jit(solution)/shard_map/ppermute | solution.py:21
  42.1 34.9 %collective-permute-start.16 = (bf16[96,2048]{1,0:T(8,128)(2,1)S(1)}, bf16[96,2048]{1,0:T(8,128)(2,1)S(1)}, u32[]{:S(2)}, u32[]{:S(2)}) collective-permute-start(bf16[96,2048]{1,0:T(8,128)(2,1)S(1)} %get-tuple-element.26.refs_0_), channel_id=1, source_target_pairs={{0,24},{4,28},{8,16},{12,20},{16,8},{20,12},{24,0},{28,4},{1,25},{... | collective-permute-start | bytes 1179656 | tf_op jit(solution)/shard_map/ppermute | solution.py:21
  45.1 15.1 %collective-permute-start.11 = (f32[2,2,2,96]{3,2,1,0:T(2,128)S(1)}, f32[2,2,2,96]{3,2,1,0:T(2,128)S(1)}, u32[]{:S(2)}, u32[]{:S(2)}) collective-permute-start(f32[2,2,2,96]{3,2,1,0:T(2,128)S(1)} %pad_maximum_fusion.9.refs_0_), channel_id=1, source_target_pairs={{0,8},{4,12},{8,0},{12,4},{16,24},{20,28},{24,16},{28,20},{1,9},{5... | collective-permute-start | bytes 9224 | tf_op jit(solution)/shard_map/ppermute | solution.py:21
  45.1 28.3 %collective-permute-start.12 = (f32[2,2,2,96]{3,2,1,0:T(2,128)S(1)}, f32[2,2,2,96]{3,2,1,0:T(2,128)S(1)}, u32[]{:S(2)}, u32[]{:S(2)}) collective-permute-start(f32[2,2,2,96]{3,2,1,0:T(2,128)S(1)} %pad_maximum_fusion.9.refs_0_), channel_id=1, source_target_pairs={{0,16},{4,20},{8,24},{12,28},{16,0},{20,4},{24,8},{28,12},{1,17},{... | collective-permute-start | bytes 9224 | tf_op jit(solution)/shard_map/ppermute | solution.py:21
  60.2 14.4 %collective-permute-start.13 = (f32[2,2,2,96]{3,2,1,0:T(2,128)S(1)}, f32[2,2,2,96]{3,2,1,0:T(2,128)S(1)}, u32[]{:S(2)}, u32[]{:S(2)}) collective-permute-start(f32[2,2,2,96]{3,2,1,0:T(2,128)S(1)} %pad_maximum_fusion.9.refs_0_), channel_id=1, source_target_pairs={{0,24},{4,28},{8,16},{12,20},{16,8},{20,12},{24,0},{28,4},{1,25},{... | collective-permute-start | bytes 9224 | tf_op jit(solution)/shard_map/ppermute | solution.py:21
  73.4 38.7 %collective-permute-start.21 = (bf16[2048,256]{1,0:T(8,128)(2,1)S(1)}, bf16[2048,256]{1,0:T(8,128)(2,1)S(1)}, u32[]{:S(2)}, u32[]{:S(2)}) collective-permute-start(bf16[2048,256]{1,0:T(8,128)(2,1)S(1)} %bitcast.59), channel_id=1, source_target_pairs={{0,1},{1,0},{2,3},{3,2},{4,5},{5,4},{6,7},{7,6},{8,9},{9,8},{10,11... | collective-permute-start | bytes 3145736 | tf_op jit(solution)/shard_map/ppermute | solution.py:21
  74.5 38.2 %collective-permute-start.24 = (bf16[2048,256]{1,0:T(8,128)(2,1)S(1)}, bf16[2048,256]{1,0:T(8,128)(2,1)S(1)}, u32[]{:S(2)}, u32[]{:S(2)}) collective-permute-start(bf16[2048,256]{1,0:T(8,128)(2,1)S(1)} %bitcast.62), channel_id=1, source_target_pairs={{0,2},{1,3},{2,0},{3,1},{4,6},{5,7},{6,4},{7,5},{8,10},{9,11},{10,... | collective-permute-start | bytes 3145736 | tf_op jit(solution)/shard_map/ppermute | solution.py:21
  75.9 34.8 %collective-permute-start.31 = (bf16[1024,256]{1,0:T(8,128)(2,1)S(1)}, bf16[1024,256]{1,0:T(8,128)(2,1)S(1)}, u32[]{:S(2)}, u32[]{:S(2)}) collective-permute-start(bf16[1024,256]{1,0:T(8,128)(2,1)S(1)} %get-tuple-element.46), channel_id=1, source_target_pairs={{0,1},{1,0},{2,3},{3,2},{4,5},{5,4},{6,7},{7,6},{8,9},{9,8},{10,11... | collective-permute-start | bytes 1572872 | tf_op jit(solution)/shard_map/ppermute | solution.py:21
  77.0 57.2 %collective-permute-start.22 = (bf16[2048,256]{1,0:T(8,128)(2,1)S(1)}, bf16[2048,256]{1,0:T(8,128)(2,1)S(1)}, u32[]{:S(2)}, u32[]{:S(2)}) collective-permute-start(bf16[2048,256]{1,0:T(8,128)(2,1)S(1)} %bitcast.63), channel_id=1, source_target_pairs={{0,1},{1,0},{2,3},{3,2},{4,5},{5,4},{6,7},{7,6},{8,9},{9,8},{10,11... | collective-permute-start | bytes 3145736 | tf_op jit(solution)/shard_map/ppermute | solution.py:21
  78.0 56.8 %collective-permute-start.23 = (bf16[2048,256]{1,0:T(8,128)(2,1)S(1)}, bf16[2048,256]{1,0:T(8,128)(2,1)S(1)}, u32[]{:S(2)}, u32[]{:S(2)}) collective-permute-start(bf16[2048,256]{1,0:T(8,128)(2,1)S(1)} %bitcast.60), channel_id=1, source_target_pairs={{0,2},{1,3},{2,0},{3,1},{4,6},{5,7},{6,4},{7,5},{8,10},{9,11},{10,... | collective-permute-start | bytes 3145736 | tf_op jit(solution)/shard_map/ppermute | solution.py:21
  110.6 23.6 %collective-permute-start.32 = (bf16[1024,256]{1,0:T(8,128)(2,1)S(1)}, bf16[1024,256]{1,0:T(8,128)(2,1)S(1)}, u32[]{:S(2)}, u32[]{:S(2)}) collective-permute-start(bf16[1024,256]{1,0:T(8,128)(2,1)S(1)} %get-tuple-element.45), channel_id=1, source_target_pairs={{0,2},{1,3},{2,0},{3,1},{4,6},{5,7},{6,4},{7,5},{8,10},{9,11},{10,... | collective-permute-start | bytes 1572872 | tf_op jit(solution)/shard_map/ppermute | solution.py:21
  112.1 44.6 %collective-permute-start.25 = (bf16[2048,256]{1,0:T(8,128)(2,1)S(1)}, bf16[2048,256]{1,0:T(8,128)(2,1)S(1)}, u32[]{:S(2)}, u32[]{:S(2)}) collective-permute-start(bf16[2048,256]{1,0:T(8,128)(2,1)S(1)} %collective-permute-done.21.refs_2_), channel_id=1, source_target_pairs={{0,2},{1,3},{2,0},{3,1},{4,6},{5,7},{6,4},{7,5},{8,10},{9,11},{10,... | collective-permute-start | bytes 3145736 | tf_op jit(solution)/shard_map/ppermute | solution.py:21
  112.7 52.1 %collective-permute-start.26 = (bf16[2048,256]{1,0:T(8,128)(2,1)S(1)}, bf16[2048,256]{1,0:T(8,128)(2,1)S(1)}, u32[]{:S(2)}, u32[]{:S(2)}) collective-permute-start(bf16[2048,256]{1,0:T(8,128)(2,1)S(1)} %collective-permute-done.24.refs_5_), channel_id=1, source_target_pairs={{0,1},{1,0},{2,3},{3,2},{4,5},{5,4},{6,7},{7,6},{8,9},{9,8},{10,11... | collective-permute-start | bytes 3145736 | tf_op jit(solution)/shard_map/ppermute | solution.py:21
  136.0 32.0 %collective-permute-start.43 = (bf16[1024,256]{1,0:T(8,128)(2,1)S(1)}, bf16[1024,256]{1,0:T(8,128)(2,1)S(1)}, u32[]{:S(2)}, u32[]{:S(2)}) collective-permute-start(bf16[1024,256]{1,0:T(8,128)(2,1)S(1)} %collective-permute-done.31.refs_4_), channel_id=1, source_target_pairs={{0,2},{1,3},{2,0},{3,1},{4,6},{5,7},{6,4},{7,5},{8,10},{9,11},{10,... | collective-permute-start | bytes 1572872 | tf_op jit(solution)/shard_map/ppermute | solution.py:21
  137.2 30.7 %collective-permute-start.44 = (bf16[1024,256]{1,0:T(8,128)(2,1)S(1)}, bf16[1024,256]{1,0:T(8,128)(2,1)S(1)}, u32[]{:S(2)}, u32[]{:S(2)}) collective-permute-start(bf16[1024,256]{1,0:T(8,128)(2,1)S(1)} %collective-permute-done.32.refs_5_), channel_id=1, source_target_pairs={{0,1},{1,0},{2,3},{3,2},{4,5},{5,4},{6,7},{7,6},{8,9},{9,8},{10,11... | collective-permute-start | bytes 1572872 | tf_op jit(solution)/shard_map/ppermute | solution.py:21
  138.3 35.4 %collective-permute-start.37 = (bf16[1024,256]{1,0:T(8,128)(2,1)S(1)}, bf16[1024,256]{1,0:T(8,128)(2,1)S(1)}, u32[]{:S(2)}, u32[]{:S(2)}) collective-permute-start(bf16[1024,256]{1,0:T(8,128)(2,1)S(1)} %get-tuple-element.45), channel_id=1, source_target_pairs={{0,1},{1,0},{2,3},{3,2},{4,5},{5,4},{6,7},{7,6},{8,9},{9,8},{10,11... | collective-permute-start | bytes 1572872 | tf_op jit(solution)/shard_map/ppermute | solution.py:21
  156.7 17.6 %collective-permute-start.38 = (bf16[1024,256]{1,0:T(8,128)(2,1)S(1)}, bf16[1024,256]{1,0:T(8,128)(2,1)S(1)}, u32[]{:S(2)}, u32[]{:S(2)}) collective-permute-start(bf16[1024,256]{1,0:T(8,128)(2,1)S(1)} %get-tuple-element.46), channel_id=1, source_target_pairs={{0,2},{1,3},{2,0},{3,1},{4,6},{5,7},{6,4},{7,5},{8,10},{9,11},{10,... | collective-permute-start | bytes 1572872 | tf_op jit(solution)/shard_map/ppermute | solution.py:21
  183.2 14.5 %collective-permute-start.40 = (bf16[96,512]{1,0:T(8,128)(2,1)S(1)}, bf16[96,512]{1,0:T(8,128)(2,1)S(1)}, u32[]{:S(2)}, u32[]{:S(2)}) collective-permute-start(bf16[96,512]{1,0:T(8,128)(2,1)S(1)} %get-tuple-element.60), channel_id=1, source_target_pairs={{0,8},{4,12},{8,0},{12,4},{16,24},{20,28},{24,16},{28,20},{1,9},{5... | collective-permute-start | bytes 294920 | tf_op jit(solution)/shard_map/ppermute | solution.py:21
  183.5 16.0 %collective-permute-start.41 = (bf16[96,512]{1,0:T(8,128)(2,1)S(1)}, bf16[96,512]{1,0:T(8,128)(2,1)S(1)}, u32[]{:S(2)}, u32[]{:S(2)}) collective-permute-start(bf16[96,512]{1,0:T(8,128)(2,1)S(1)} %get-tuple-element.59), channel_id=1, source_target_pairs={{0,16},{4,20},{8,24},{12,28},{16,0},{20,4},{24,8},{28,12},{1,17},{... | collective-permute-start | bytes 294920 | tf_op jit(solution)/shard_map/ppermute | solution.py:21
  186.9 12.5 %collective-permute-start.42 = (bf16[96,512]{1,0:T(8,128)(2,1)S(1)}, bf16[96,512]{1,0:T(8,128)(2,1)S(1)}, u32[]{:S(2)}, u32[]{:S(2)}) collective-permute-start(bf16[96,512]{1,0:T(8,128)(2,1)S(1)} %get-tuple-element.58), channel_id=1, source_target_pairs={{0,24},{4,28},{8,16},{12,20},{16,8},{20,12},{24,0},{28,4},{1,25},{... | collective-permute-start | bytes 294920 | tf_op jit(solution)/shard_map/ppermute | solution.py:21
  189.9 16.3 %collective-permute-start.34 = (bf16[96,512]{1,0:T(8,128)(2,1)S(1)}, bf16[96,512]{1,0:T(8,128)(2,1)S(1)}, u32[]{:S(2)}, u32[]{:S(2)}) collective-permute-start(bf16[96,512]{1,0:T(8,128)(2,1)S(1)} %get-tuple-element.63), channel_id=1, source_target_pairs={{0,8},{4,12},{8,0},{12,4},{16,24},{20,28},{24,16},{28,20},{1,9},{5... | collective-permute-start | bytes 294920 | tf_op jit(solution)/shard_map/ppermute | solution.py:21
  189.9 17.9 %collective-permute-start.35 = (bf16[96,512]{1,0:T(8,128)(2,1)S(1)}, bf16[96,512]{1,0:T(8,128)(2,1)S(1)}, u32[]{:S(2)}, u32[]{:S(2)}) collective-permute-start(bf16[96,512]{1,0:T(8,128)(2,1)S(1)} %get-tuple-element.62), channel_id=1, source_target_pairs={{0,16},{4,20},{8,24},{12,28},{16,0},{20,4},{24,8},{28,12},{1,17},{... | collective-permute-start | bytes 294920 | tf_op jit(solution)/shard_map/ppermute | solution.py:21
  199.4 15.8 %collective-permute-start.29 = (bf16[96,512]{1,0:T(8,128)(2,1)S(1)}, bf16[96,512]{1,0:T(8,128)(2,1)S(1)}, u32[]{:S(2)}, u32[]{:S(2)}) collective-permute-start(bf16[96,512]{1,0:T(8,128)(2,1)S(1)} %get-tuple-element.65), channel_id=1, source_target_pairs={{0,16},{4,20},{8,24},{12,28},{16,0},{20,4},{24,8},{28,12},{1,17},{... | collective-permute-start | bytes 294920 | tf_op jit(solution)/shard_map/ppermute | solution.py:21
  (42 other events, 380.6 us)

commit v6 on v5

--- a/solution.py
+++ b/solution.py
@@ -152,17 +152,21 @@
     return pltpu.CompilerParams(vmem_limit_bytes=mebibytes << 20)
 
 
-def pooled_channels(pool_in, doc_ids, place):
-    channels, positions = pool_in.shape
-    scalars = pl.BlockSpec(memory_space=pltpu.SMEM)
-    table = pl.pallas_call(
+def table_call(pool_in, doc_ids):
+    return pl.pallas_call(
         table_kernel,
-        out_shape=jax.ShapeDtypeStruct((TABLE, channels), F32),
+        out_shape=jax.ShapeDtypeStruct((TABLE, pool_in.shape[0]), F32),
         in_specs=in_vmem(2),
         out_specs=in_vmem(1)[0],
         compiler_params=room(4),
         name="table",
     )(pool_in, doc_ids)
+
+
+def pooled_channels(pool_in, doc_ids, place):
+    channels, positions = pool_in.shape
+    scalars = pl.BlockSpec(memory_space=pltpu.SMEM)
+    table = table_call(pool_in, doc_ids)
     near = swap_with(table, "sp", 1)
     pair = jnp.stack([table, near])
     sums, start = pl.pallas_call(
@@ -229,20 +233,28 @@
     return (got[0], got[-1])
 
 
-def stage_kernel(*refs):
-    parts = len(refs) // 3
-    for k in range(parts):
-        half = refs[2 * k].shape[1]
-        refs[2 * parts + k][:, :half] = refs[2 * k][...]
-        refs[2 * parts + k][:, half:] = refs[2 * k + 1][...]
+def stage_kernel(pieces, *refs):
+    at = 0
+    outs = refs[sum(sum(p) for p in pieces) :]
+    for out, pair in zip(outs, pieces):
+        half = out.shape[1] // 2
+        for side, count in enumerate(pair):
+            row = 0
+            for ref in refs[at : at + count]:
+                depth = ref.shape[0]
+                out[row : row + depth, side * half : (side + 1) * half] = ref[...]
+                row += depth
+            at += count
 
 
 def staged(pairs):
-    flat = [w for pair in pairs for w in pair]
-    return pl.pallas_call(
-        stage_kernel,
+    flat = [w for pair in pairs for side in pair for w in side]
+    pieces = tuple(tuple(len(side) for side in pair) for pair in pairs)
+    depth = sum(w.shape[0] for w in pairs[0][0])
+    return pl.pallas_call(
+        functools.partial(stage_kernel, pieces),
         out_shape=tuple(
-            jax.ShapeDtypeStruct((g.shape[0], 2 * g.shape[1]), BF16) for g, _ in pairs
+            jax.ShapeDtypeStruct((depth, 2 * pair[0][0].shape[1]), BF16) for pair in pairs
         ),
         in_specs=in_vmem(len(flat)),
         out_specs=tuple(in_vmem(len(pairs))),
@@ -253,16 +265,14 @@
 
 def down_kernel(parts, place_ref, share_ref, *refs):
     hidden, weights, out_ref = refs[:parts], refs[parts:-1], refs[-1]
-    depth, at = hidden[0].shape[1], 0
-    for weight in weights:
-        total = None
-        for k in range(parts):
-            rows = pl.ds(pl.multiple_of((place_ref[1] ^ k) * depth, depth), depth)
-            piece = jnp.dot(hidden[k][...], weight[rows, :], preferred_element_type=F32)
-            total = piece if total is None else total + piece
-        wide = weight.shape[1]
-        out_ref[:, at : at + wide] = (total * share_ref[...]).astype(BF16)
-        at += wide
+    depth, total = hidden[0].shape[1], None
+    for k in range(parts):
+        rows = pl.ds(pl.multiple_of((place_ref[1] ^ k) * depth, depth), depth)
+        near = [weight[rows, :] for weight in weights]
+        near = near[0] if len(near) == 1 else jnp.concatenate(near, axis=1)
+        piece = jnp.dot(hidden[k][...], near, preferred_element_type=F32)
+        total = piece if total is None else total + piece
+    out_ref[...] = (total * share_ref[...]).astype(BF16)
 
 
 def weighted_outputs(place, share, hidden, weights):
@@ -278,41 +288,75 @@
     )(place, share, *hidden, *weights)
 
 
+LANES = 128
+
+
+def rows_kernel(place_ref, mixed_ref, *outs):
+    count, wide = outs[0].shape[0], mixed_ref.shape[1]
+    lane = lax.broadcasted_iota(jnp.int32, (count, LANES), 1)
+    for k, out_ref in enumerate(outs):
+        at = pl.multiple_of((place_ref[1] ^ k) * count, 8)
+        part = mixed_ref[pl.ds(at, count), :]
+        mean = jnp.sum(part, axis=1, keepdims=True) / wide
+        out_ref[:, :wide] = (part - mean).astype(BF16)
+        high = mean.astype(BF16).astype(F32)
+        middle = (mean - high).astype(BF16).astype(F32)
+        low = mean - high - middle
+        terms = jnp.where(lane == 0, high, jnp.where(lane == 1, middle, low))
+        out_ref[:, wide:] = terms.astype(BF16)
+
+
+def rows_to_send(place, mixed, parts):
+    count, wide = mixed.shape[0] // parts, mixed.shape[1]
+    return pl.pallas_call(
+        rows_kernel,
+        out_shape=tuple(
+            jax.ShapeDtypeStruct((count, wide + LANES), BF16) for _ in range(parts)
+        ),
+        in_specs=[pl.BlockSpec(memory_space=pltpu.SMEM)] + in_vmem(1),
+        out_specs=tuple(in_vmem(parts)),
+        compiler_params=room(4),
+        name="rows",
+    )(place, mixed)
+
+
 def first_norm_kernel(parts, place_ref, *refs):
-    rows, (tokens_ref, normed_ref, scale_ref) = refs[:parts], refs[parts:]
-    count, wide = normed_ref.shape[1:]
-    total = square = 0.0
+    rows, gains, outs = refs[:parts], refs[parts : 2 * parts], refs[2 * parts :]
+    tokens_ref, normed_ref, scale_ref = outs
+    wide = normed_ref.shape[2]
+    values = []
     for ref in rows:
-        part = ref[:count, :]
-        total = total + jnp.sum(part, axis=1, keepdims=True)
-        square = square + jnp.sum(part * part, axis=1, keepdims=True)
-    mean = total / (parts * wide)
-    scale = lax.rsqrt(square / (parts * wide) - mean * mean + EPS)
-    for k, ref in enumerate(rows):
-        gains = ref[count:, :]
-        scale_ref[k] = gains
-        part = (ref[:count, :] - mean) * scale * gains[:1] + gains[1:2]
+        mean = ref[:, wide : wide + 3].astype(F32)
+        mean = mean[:, :1] + mean[:, 1:2] + mean[:, 2:3]
+        values.append(ref[:, :wide].astype(F32) + mean)
+    features = parts * wide
+    mean = sum(jnp.sum(v, axis=1, keepdims=True) for v in values) / features
+    square = sum(jnp.sum(v * v, axis=1, keepdims=True) for v in values) / features
+    scale = lax.rsqrt(square - mean * mean + EPS)
+    for k, value in enumerate(values):
+        scale_ref[k] = gains[k][...]
+        part = (value - mean) * scale * gains[k][:1, :] + gains[k][1:2, :]
         part = part.astype(BF16)
         normed_ref[k] = part
         at = pl.multiple_of((place_ref[1] ^ k) * wide, wide)
         tokens_ref[:, pl.ds(at, wide)] = part
 
 
-def first_norm(place, rows, count):
-    parts, wide = len(rows), rows[0].shape[1]
-    tokens, normed, scales = pl.pallas_call(
+def first_norm(place, rows, gains):
+    parts, count = len(rows), rows[0].shape[0]
+    wide = gains[0].shape[1]
+    return pl.pallas_call(
         functools.partial(first_norm_kernel, parts),
         out_shape=(
             jax.ShapeDtypeStruct((count, parts * wide), BF16),
             jax.ShapeDtypeStruct((parts, count, wide), BF16),
-            jax.ShapeDtypeStruct((parts, rows[0].shape[0] - count, wide), F32),
+            jax.ShapeDtypeStruct((parts,) + gains[0].shape, F32),
         ),
-        in_specs=[pl.BlockSpec(memory_space=pltpu.SMEM)] + in_vmem(parts),
+        in_specs=[pl.BlockSpec(memory_space=pltpu.SMEM)] + in_vmem(2 * parts),
         out_specs=tuple(in_vmem(3)),
         compiler_params=room(8),
         name="norm",
-    )(place, *rows)
-    return tokens, normed, scales
+    )(place, *rows, *gains)
 
 
 def share_kernel(place_ref, *refs):
@@ -350,11 +394,11 @@
     )(place, *tables)
 
 
-def last_norm_kernel(parts, arrange, normed_ref, scale_ref, *refs):
+def last_norm_kernel(parts, groups, arrange, normed_ref, scale_ref, *refs):
     outs, refs = refs[-parts:], refs[:-parts]
-    each = len(refs) // parts
+    each = len(refs) // groups
     sums = []
-    for k in range(parts):
+    for k in range(groups):
         own, *others = refs[k * each : (k + 1) * each]
         total = own[...]
         for other in others:
@@ -376,8 +420,8 @@
     parts, count, wide = normed.shape
     flat = [r for group in groups for r in group]
     return pl.pallas_call(
-        functools.partial(last_norm_kernel, parts, arrange),
-        out_shape=tuple(jax.ShapeDtypeStruct((count, wide), BF16) for _ in groups),
+        functools.partial(last_norm_kernel, parts, len(groups), arrange),
+        out_shape=tuple(jax.ShapeDtypeStruct((count, wide), BF16) for _ in range(parts)),
         in_specs=in_vmem(2 + len(flat)),
         out_specs=tuple(in_vmem(parts)),
         compiler_params=room(12),
@@ -385,33 +429,35 @@
     )(normed, scales, *flat)
 
 
-def weight_parts(w_gate, w_up, w_down, tp):
+def weight_parts(w_gate, w_up, w_down, tp, later_of):
     if tp != 4:
         gate, up, down = (exchange_all(w, "tp") for w in (w_gate, w_up, w_down))
         pairs = [list(pair) for pair in zip(gate, up)]
         return pairs, [[w] for w in down], lambda *parts: list(parts)
     gate1 = swap_with(w_gate, "tp", 1)
     up2 = swap_with(w_up, "tp", 2)
-    up1 = swap_with(w_up, "tp", 1)
-    gate2 = swap_with(w_gate, "tp", 2)
+    top = w_gate.shape[0] // 4
+    later_gate, later_up = later_of(w_gate), later_of(w_up)
+    up1_top = swap_with(later_up[:top], "tp", 1)
+    gate2_top = swap_with(later_gate[:top], "tp", 2)
+    up1_low = swap_with(later_up[top:], "tp", 1)
+    gate2_low = swap_with(later_gate[top:], "tp", 2)
     up3 = swap_with(up2, "tp", 1)
     gate3 = swap_with(gate1, "tp", 2)
     wide = w_down.shape[1] // 2
-    left, right = w_down[:, :wide], w_down[:, wide:]
-    down1_left = swap_with(left, "tp", 1)
-    down2_right = swap_with(right, "tp", 2)
-    down1_right = swap_with(right, "tp", 1)
-    down2_left = swap_with(left, "tp", 2)
-    down3_right = swap_with(down2_right, "tp", 1)
-    down3_left = swap_with(down1_left, "tp", 2)
-    near = staged([(w_gate, w_up), (gate1, up1), (gate2, up2)])
+    w_late = later_of(w_down)
+    left, right = w_late[:, :wide], w_late[:, wide:]
+    down1_l = swap_with(left, "tp", 1)
+    down2_r = swap_with(right, "tp", 2)
+    down1_r = swap_with(right, "tp", 1)
+    down2_l = swap_with(left, "tp", 2)
+    down3_r = swap_with(down2_r, "tp", 1)
+    down3_l = swap_with(down1_l, "tp", 2)
+    near = staged(
+        [([w_gate], [w_up]), ([gate1], [up1_top, up1_low]), ([gate2_top, gate2_low], [up2])]
+    )
     first = [[w] for w in near] + [[gate3, up3]]
-    down = [
-        [w_down],
-        [down1_left, down2_right],
-        [down1_right, down2_left],
-        [down3_left, down3_right],
-    ]
+    down = [[w_down], [down1_l, down2_r], [down1_r, down2_l], [down3_l, down3_r]]
 
     def by_distance(own, early, late, last):
         one = jnp.concatenate([early[:, :wide], late[:, :wide]], axis=1)
@@ -445,7 +491,18 @@
     quarter = positions // tp
 
     place = jnp.stack([i, j])
+    gains = jnp.pad(
+        jnp.stack([first_gain, first_bias, second_gain, second_bias]), ((0, 4), (0, 0))
+    )
+    gains = exchange_all(gains, "tp")
     pooled = pooled_channels(pool_in, doc_ids, place)
+
+    def later_of(weight):
+        return lax.optimization_barrier((weight, pooled))[0]
+
+    first_w, down_w, by_distance = weight_parts(
+        w_gate[0], w_up[0], w_down[0], tp, later_of
+    )
     pooled_rel = exchange_all(pooled, "tp")
     my_routes = lax.dynamic_slice_in_dim(routes, j * quarter, quarter, 0)
     my_weights = lax.dynamic_slice_in_dim(route_weight, j * quarter, quarter, 0)
@@ -468,18 +525,9 @@
     )
     mixed = ALPHA * residual.astype(F32) + mixer_out
 
-    quarters = [
-        lax.dynamic_slice_in_dim(mixed, (j ^ k) * quarter, quarter, 0) for k in range(tp)
-    ]
-    scales = jnp.pad(
-        jnp.stack([first_gain, first_bias, second_gain, second_bias]), ((0, 4), (0, 0))
-    )
-    both = [jnp.concatenate([q, scales]) for q in quarters]
-    both = [both[0]] + [swap_with(both[k], "tp", k) for k in range(1, tp)]
-    tokens, normed, scales = first_norm(place, both, quarter)
-
-    down_own, tokens = lax.optimization_barrier((w_down[0], tokens))
-    first_w, down_w, by_distance = weight_parts(w_gate[0], w_up[0], down_own, tp)
+    sent = rows_to_send(place, mixed, tp)
+    both = [sent[0]] + [swap_with(sent[k], "tp", k) for k in range(1, tp)]
+    tokens, normed, scales = first_norm(place, both, gains)
 
     everyone = line_gather(tokens, "sp")
     inputs, first_hidden = hidden_units(everyone, first_w[0])
@@ -489,7 +537,7 @@
 
     groups = []
     half_rows = (sp // 2) * quarter
-    for k in range(tp):
+    for k in range(len(down_w)):
         partial = weighted_outputs(place, share, hidden_rel, down_w[k])
         other = swap_with(partial[half_rows:], "sp", 1)
         joined = partial[:half_rows].astype(F32) + other.astype(F32)

time: 225 us -> 192 us (0.85)
  waiting for transfers between devices: 129 us -> 87.6 us
  starting transfers between devices: 65.8 us -> 71.5 us
    ppermute x52 -> x57, waiting for transfers between devices: 129 us -> 87.6 us  [swap_with(): return lax.ppermute(part, axis, [(i, i ^ bits) for i in range(size)])]
    ppermute x52 -> x57, starting transfers between devices: 65.8 us -> 71.5 us  [swap_with(): return lax.ppermute(part, axis, [(i, i ^ bits) for i in range(size)])]
  transfers between devices with their start and end apart: 52 -> 57, of which waited for: 24 -> 21; matrix products, arithmetic and copies ran while one was open for 1% -> 3% of each run, Pallas kernels for 7% -> 10%
where the time goes in v6:
time: 192 us; the launch traced here: 191 us
  waiting for transfers between devices  87.6 us (46%)
  starting transfers between devices  71.5 us (37%)
  Pallas kernels  19.6 us (10%)
  local copies, waits for them, and re-layouts  8.03 us (4%)
  other arithmetic  3.18 us (2%)
    ppermute x57, waiting for transfers between devices, swap_with(): return lax.ppermute(part, axis, [(i, i ^ bits) for i in range(size)])  87.6 us
    ppermute x57, starting transfers between devices, swap_with(): return lax.ppermute(part, axis, [(i, i ^ bits) for i in range(size)])  71.5 us
    pallas_call x4, Pallas kernels, hidden_units(): pl.pallas_call(functools.partial(hidden_kernel, count), out_shape=outs, i...  7.19 us
    pallas_call x4, Pallas kernels, weighted_outputs(): pl.pallas_call(functools.partial(down_kernel, len(hidden)), out_shape=jax...  6.26 us
    unnamed x28, local copies, waits for them, and re-layouts  4.82 us
  transfers between devices with their start and end apart: 57, of which 21 were waited for; matrix products, arithmetic and copies ran while one was open for 3% of the time, Pallas kernels for 10%

profile of v6, /device:TPU:0, one launch (start us, length us, event | category | flops | bytes accessed | tf_op | source)
XLA Modules:
  0.0 191.2 jit_solution(14049052681917111087)
XLA Ops:
  3.1 2.5 %collective-permute-start.10 = (f32[8,512]{1,0:T(8,128)S(1)}, f32[8,512]{1,0:T(8,128)S(1)}, u32[]{:S(2)}, u32[]{:S(2)}) collective-permute-start(f32[8,512]{1,0:T(8,128)S(1)} %select_maximum_fusion.refs_4_), channel_id=1, source_target_pairs={{0,1},{1,0},{2,3},{3,2},{4,5},{5,4},{6,7},{7,6},{8,9},{9,8},{10,11... | collective-permute-start | bytes 49160 | tf_op jit(solution)/shard_map/ppermute | solution.py:21
  9.0 2.6 %collective-permute-start.2 = (f32[2,24,128]{2,1,0:T(8,128)S(1)}, f32[2,24,128]{2,1,0:T(8,128)S(1)}, u32[]{:S(2)}, u32[]{:S(2)}) collective-permute-start(f32[2,24,128]{2,1,0:T(8,128)S(1)} %pad_maximum_fusion.4), channel_id=1, source_target_pairs={{0,16},{4,20},{8,24},{12,28},{16,0},{20,4},{24,8},{28,12},{1,17},{... | collective-permute-start | bytes 73736 | tf_op jit(solution)/shard_map/ppermute | solution.py:21
  33.5 2.5 %collective-permute-start.25 = (bf16[512,256]{1,0:T(8,128)(2,1)S(1)}, bf16[512,256]{1,0:T(8,128)(2,1)S(1)}, u32[]{:S(2)}, u32[]{:S(2)}) collective-permute-start(bf16[512,256]{1,0:T(8,128)(2,1)S(1)} %slice.90), channel_id=1, source_target_pairs={{0,1},{1,0},{2,3},{3,2},{4,5},{5,4},{6,7},{7,6},{8,9},{9,8},{10,11... | collective-permute-start | bytes 786440 | tf_op jit(solution)/shard_map/ppermute | solution.py:21
  40.5 4.9 %collective-permute-done.7.refs_1_ = bf16[96,640]{1,0:T(8,128)(2,1)S(1)} collective-permute-done((bf16[96,640]{1,0:T(8,128)(2,1)S(1)}, bf16[96,640]{1,0:T(8,128)(2,1)S(1)}, u32[]{:S(2)}, u32[]{:S(2)}) %collective-permute-start.7) | collective-permute-done | bytes 122912 | tf_op jit(solution)/shard_map/ppermute | solution.py:21
  45.3 1.8 collective-permute-start.36
  52.1 8.0 %collective-permute-done.36.refs_4_ = bf16[1024,256]{1,0:T(8,128)(2,1)S(1)} collective-permute-done((bf16[1024,256]{1,0:T(8,128)(2,1)S(1)}, bf16[1024,256]{1,0:T(8,128)(2,1)S(1)}, u32[]{:S(2)}, u32[]{:S(2)}) %collective-permute-start.36) | collective-permute-done | bytes 524320 | tf_op jit(solution)/shard_map/ppermute | solution.py:21
  60.7 3.0 %collective-permute-done.37.refs_5_ = bf16[1024,256]{1,0:T(8,128)(2,1)S(1)} collective-permute-done((bf16[1024,256]{1,0:T(8,128)(2,1)S(1)}, bf16[1024,256]{1,0:T(8,128)(2,1)S(1)}, u32[]{:S(2)}, u32[]{:S(2)}) %collective-permute-start.37) | collective-permute-done | bytes 524320 | tf_op jit(solution)/shard_map/ppermute | solution.py:21
  65.3 2.1 %collective-permute-done.17.refs_1_ = bf16[96,2048]{1,0:T(8,128)(2,1)S(1)} collective-permute-done((bf16[96,2048]{1,0:T(8,128)(2,1)S(1)}, bf16[96,2048]{1,0:T(8,128)(2,1)S(1)}, u32[]{:S(2)}, u32[]{:S(2)}) %collective-permute-start.17) | collective-permute-done | bytes 393248 | tf_op jit(solution)/shard_map/ppermute | solution.py:21
  67.4 2.2 %collective-permute-start.26 = (bf16[1536,256]{1,0:T(8,128)(2,1)S(1)}, bf16[1536,256]{1,0:T(8,128)(2,1)S(1)}, u32[]{:S(2)}, u32[]{:S(2)}) collective-permute-start(bf16[1536,256]{1,0:T(8,128)(2,1)S(1)} %slice.91), channel_id=1, source_target_pairs={{0,1},{1,0},{2,3},{3,2},{4,5},{5,4},{6,7},{7,6},{8,9},{9,8},{10,11... | collective-permute-start | bytes 2359304 | tf_op jit(solution)/shard_map/ppermute | solution.py:21
  69.7 13.6 %collective-permute-done.18.refs_2_ = bf16[96,2048]{1,0:T(8,128)(2,1)S(1)} collective-permute-done((bf16[96,2048]{1,0:T(8,128)(2,1)S(1)}, bf16[96,2048]{1,0:T(8,128)(2,1)S(1)}, u32[]{:S(2)}, u32[]{:S(2)}) %collective-permute-start.18) | collective-permute-done | bytes 393248 | tf_op jit(solution)/shard_map/ppermute | solution.py:21
  86.3 13.1 %collective-permute-done.26.refs_4_ = bf16[1536,256]{1,0:T(8,128)(2,1)S(1)} collective-permute-done((bf16[1536,256]{1,0:T(8,128)(2,1)S(1)}, bf16[1536,256]{1,0:T(8,128)(2,1)S(1)}, u32[]{:S(2)}, u32[]{:S(2)}) %collective-permute-start.26) | collective-permute-done | bytes 786464 | tf_op jit(solution)/shard_map/ppermute | solution.py:21
  99.5 4.2 %collective-permute-done.28.refs_6_ = bf16[1536,256]{1,0:T(8,128)(2,1)S(1)} collective-permute-done((bf16[1536,256]{1,0:T(8,128)(2,1)S(1)}, bf16[1536,256]{1,0:T(8,128)(2,1)S(1)}, u32[]{:S(2)}, u32[]{:S(2)}) %collective-permute-start.28) | collective-permute-done | bytes 786464 | tf_op jit(solution)/shard_map/ppermute | solution.py:21
  106.9 19.2 %collective-permute-done.30.refs_1_ = bf16[2048,256]{1,0:T(8,128)(2,1)S(1)} collective-permute-done((bf16[2048,256]{1,0:T(8,128)(2,1)S(1)}, bf16[2048,256]{1,0:T(8,128)(2,1)S(1)}, u32[]{:S(2)}, u32[]{:S(2)}) %collective-permute-start.30) | collective-permute-done | bytes 1048608 | tf_op jit(solution)/shard_map/ppermute | solution.py:21
  128.7 1.8 hidden.4
  145.5 2.4 %collective-permute-start.52 = (bf16[96,512]{1,0:T(8,128)(2,1)S(1)}, bf16[96,512]{1,0:T(8,128)(2,1)S(1)}, u32[]{:S(2)}, u32[]{:S(2)}) collective-permute-start(bf16[96,512]{1,0:T(8,128)(2,1)S(1)} %get-tuple-element.62), channel_id=1, source_target_pairs={{0,16},{4,20},{8,24},{12,28},{16,0},{20,4},{24,8},{28,12},{1,17},{... | collective-permute-start | bytes 294920 | tf_op jit(solution)/shard_map/ppermute | solution.py:21
  147.9 1.9 %collective-permute-start.53 = (bf16[96,512]{1,0:T(8,128)(2,1)S(1)}, bf16[96,512]{1,0:T(8,128)(2,1)S(1)}, u32[]{:S(2)}, u32[]{:S(2)}) collective-permute-start(bf16[96,512]{1,0:T(8,128)(2,1)S(1)} %get-tuple-element.61), channel_id=1, source_target_pairs={{0,24},{4,28},{8,16},{12,20},{16,8},{20,12},{24,0},{28,4},{1,25},{... | collective-permute-start | bytes 294920 | tf_op jit(solution)/shard_map/ppermute | solution.py:21
  150.2 2.5 %collective-permute-start.46 = (bf16[96,512]{1,0:T(8,128)(2,1)S(1)}, bf16[96,512]{1,0:T(8,128)(2,1)S(1)}, u32[]{:S(2)}, u32[]{:S(2)}) collective-permute-start(bf16[96,512]{1,0:T(8,128)(2,1)S(1)} %get-tuple-element.65), channel_id=1, source_target_pairs={{0,16},{4,20},{8,24},{12,28},{16,0},{20,4},{24,8},{28,12},{1,17},{... | collective-permute-start | bytes 294920 | tf_op jit(solution)/shard_map/ppermute | solution.py:21
  152.9 2.0 %collective-permute-start.47 = (bf16[96,512]{1,0:T(8,128)(2,1)S(1)}, bf16[96,512]{1,0:T(8,128)(2,1)S(1)}, u32[]{:S(2)}, u32[]{:S(2)}) collective-permute-start(bf16[96,512]{1,0:T(8,128)(2,1)S(1)} %get-tuple-element.64), channel_id=1, source_target_pairs={{0,24},{4,28},{8,16},{12,20},{16,8},{20,12},{24,0},{28,4},{1,25},{... | collective-permute-start | bytes 294920 | tf_op jit(solution)/shard_map/ppermute | solution.py:21
  156.4 7.3 %collective-permute-start.40 = (bf16[96,512]{1,0:T(8,128)(2,1)S(1)}, bf16[96,512]{1,0:T(8,128)(2,1)S(1)}, u32[]{:S(2)}, u32[]{:S(2)}) collective-permute-start(bf16[96,512]{1,0:T(8,128)(2,1)S(1)} %get-tuple-element.68), channel_id=1, source_target_pairs={{0,16},{4,20},{8,24},{12,28},{16,0},{20,4},{24,8},{28,12},{1,17},{... | collective-permute-start | bytes 294920 | tf_op jit(solution)/shard_map/ppermute | solution.py:21
  163.7 1.9 %collective-permute-start.41 = (bf16[96,512]{1,0:T(8,128)(2,1)S(1)}, bf16[96,512]{1,0:T(8,128)(2,1)S(1)}, u32[]{:S(2)}, u32[]{:S(2)}) collective-permute-start(bf16[96,512]{1,0:T(8,128)(2,1)S(1)} %get-tuple-element.67), channel_id=1, source_target_pairs={{0,24},{4,28},{8,16},{12,20},{16,8},{20,12},{24,0},{28,4},{1,25},{... | collective-permute-start | bytes 294920 | tf_op jit(solution)/shard_map/ppermute | solution.py:21
  165.7 6.5 %collective-permute-start.34 = (bf16[96,512]{1,0:T(8,128)(2,1)S(1)}, bf16[96,512]{1,0:T(8,128)(2,1)S(1)}, u32[]{:S(2)}, u32[]{:S(2)}) collective-permute-start(bf16[96,512]{1,0:T(8,128)(2,1)S(1)} %get-tuple-element.71), channel_id=1, source_target_pairs={{0,16},{4,20},{8,24},{12,28},{16,0},{20,4},{24,8},{28,12},{1,17},{... | collective-permute-start | bytes 294920 | tf_op jit(solution)/shard_map/ppermute | solution.py:21
  172.1 1.9 %collective-permute-start.35 = (bf16[96,512]{1,0:T(8,128)(2,1)S(1)}, bf16[96,512]{1,0:T(8,128)(2,1)S(1)}, u32[]{:S(2)}, u32[]{:S(2)}) collective-permute-start(bf16[96,512]{1,0:T(8,128)(2,1)S(1)} %get-tuple-element.70), channel_id=1, source_target_pairs={{0,24},{4,28},{8,16},{12,20},{16,8},{20,12},{24,0},{28,4},{1,25},{... | collective-permute-start | bytes 294920 | tf_op jit(solution)/shard_map/ppermute | solution.py:21
  175.4 6.3 %collective-permute-done.34.refs_2_ = bf16[96,512]{1,0:T(8,128)(2,1)S(1)} collective-permute-done((bf16[96,512]{1,0:T(8,128)(2,1)S(1)}, bf16[96,512]{1,0:T(8,128)(2,1)S(1)}, u32[]{:S(2)}, u32[]{:S(2)}) %collective-permute-start.34) | collective-permute-done | bytes 98336 | tf_op jit(solution)/shard_map/ppermute | solution.py:21
  187.3 2.0 %collective-permute-done.55 = bf16[96,512]{1,0:T(8,128)(2,1)S(1)} collective-permute-done((bf16[96,512]{1,0:T(8,128)(2,1)S(1)}, bf16[96,512]{1,0:T(8,128)(2,1)S(1)}, u32[]{:S(2)}, u32[]{:S(2)}) %collective-permute-start.55) | collective-permute-done | bytes 98336 | tf_op jit(solution)/shard_map/ppermute | solution.py:21
  (171 shorter events, 74.3 us)
Async XLA Ops:
  3.1 33.8 %collective-permute-start.10 = (f32[8,512]{1,0:T(8,128)S(1)}, f32[8,512]{1,0:T(8,128)S(1)}, u32[]{:S(2)}, u32[]{:S(2)}) collective-permute-start(f32[8,512]{1,0:T(8,128)S(1)} %select_maximum_fusion.refs_4_), channel_id=1, source_target_pairs={{0,1},{1,0},{2,3},{3,2},{4,5},{5,4},{6,7},{7,6},{8,9},{9,8},{10,11... | collective-permute-start | bytes 49160 | tf_op jit(solution)/shard_map/ppermute | solution.py:21
  14.8 23.6 %collective-permute-start.11 = (f32[8,512]{1,0:T(8,128)S(1)}, f32[8,512]{1,0:T(8,128)S(1)}, u32[]{:S(2)}, u32[]{:S(2)}) collective-permute-start(f32[8,512]{1,0:T(8,128)S(1)} %select_maximum_fusion.refs_4_), channel_id=1, source_target_pairs={{0,2},{1,3},{2,0},{3,1},{4,6},{5,7},{6,4},{7,5},{8,10},{9,11},{10,... | collective-permute-start | bytes 49160 | tf_op jit(solution)/shard_map/ppermute | solution.py:21
  33.5 17.0 %collective-permute-start.25 = (bf16[512,256]{1,0:T(8,128)(2,1)S(1)}, bf16[512,256]{1,0:T(8,128)(2,1)S(1)}, u32[]{:S(2)}, u32[]{:S(2)}) collective-permute-start(bf16[512,256]{1,0:T(8,128)(2,1)S(1)} %slice.90), channel_id=1, source_target_pairs={{0,1},{1,0},{2,3},{3,2},{4,5},{5,4},{6,7},{7,6},{8,9},{9,8},{10,11... | collective-permute-start | bytes 786440 | tf_op jit(solution)/shard_map/ppermute | solution.py:21
  36.0 16.1 %collective-permute-start.27 = (bf16[512,256]{1,0:T(8,128)(2,1)S(1)}, bf16[512,256]{1,0:T(8,128)(2,1)S(1)}, u32[]{:S(2)}, u32[]{:S(2)}) collective-permute-start(bf16[512,256]{1,0:T(8,128)(2,1)S(1)} %slice.92), channel_id=1, source_target_pairs={{0,2},{1,3},{2,0},{3,1},{4,6},{5,7},{6,4},{7,5},{8,10},{9,11},{10,... | collective-permute-start | bytes 786440 | tf_op jit(solution)/shard_map/ppermute | solution.py:21
  45.3 14.8 %collective-permute-start.36 = (bf16[1024,256]{1,0:T(8,128)(2,1)S(1)}, bf16[1024,256]{1,0:T(8,128)(2,1)S(1)}, u32[]{:S(2)}, u32[]{:S(2)}) collective-permute-start(bf16[1024,256]{1,0:T(8,128)(2,1)S(1)} %get-tuple-element.56), channel_id=1, source_target_pairs={{0,1},{1,0},{2,3},{3,2},{4,5},{5,4},{6,7},{7,6},{8,9},{9,8},{10,11... | collective-permute-start | bytes 1572872 | tf_op jit(solution)/shard_map/ppermute | solution.py:21
  47.2 37.3 %collective-permute-start.24 = (bf16[2048,256]{1,0:T(8,128)(2,1)S(1)}, bf16[2048,256]{1,0:T(8,128)(2,1)S(1)}, u32[]{:S(2)}, u32[]{:S(2)}) collective-permute-start(bf16[2048,256]{1,0:T(8,128)(2,1)S(1)} %bitcast.58), channel_id=1, source_target_pairs={{0,1},{1,0},{2,3},{3,2},{4,5},{5,4},{6,7},{7,6},{8,9},{9,8},{10,11... | collective-permute-start | bytes 3145736 | tf_op jit(solution)/shard_map/ppermute | solution.py:21
  48.9 14.8 %collective-permute-start.37 = (bf16[1024,256]{1,0:T(8,128)(2,1)S(1)}, bf16[1024,256]{1,0:T(8,128)(2,1)S(1)}, u32[]{:S(2)}, u32[]{:S(2)}) collective-permute-start(bf16[1024,256]{1,0:T(8,128)(2,1)S(1)} %get-tuple-element.55), channel_id=1, source_target_pairs={{0,2},{1,3},{2,0},{3,1},{4,6},{5,7},{6,4},{7,5},{8,10},{9,11},{10,... | collective-permute-start | bytes 1572872 | tf_op jit(solution)/shard_map/ppermute | solution.py:21
  50.6 34.8 %collective-permute-start.29 = (bf16[2048,256]{1,0:T(8,128)(2,1)S(1)}, bf16[2048,256]{1,0:T(8,128)(2,1)S(1)}, u32[]{:S(2)}, u32[]{:S(2)}) collective-permute-start(bf16[2048,256]{1,0:T(8,128)(2,1)S(1)} %bitcast.62), channel_id=1, source_target_pairs={{0,2},{1,3},{2,0},{3,1},{4,6},{5,7},{6,4},{7,5},{8,10},{9,11},{10,... | collective-permute-start | bytes 3145736 | tf_op jit(solution)/shard_map/ppermute | solution.py:21
  52.1 15.3 %collective-permute-start.17 = (bf16[96,2048]{1,0:T(8,128)(2,1)S(1)}, bf16[96,2048]{1,0:T(8,128)(2,1)S(1)}, u32[]{:S(2)}, u32[]{:S(2)}) collective-permute-start(bf16[96,2048]{1,0:T(8,128)(2,1)S(1)} %get-tuple-element.34.refs_0_), channel_id=1, source_target_pairs={{0,8},{4,12},{8,0},{12,4},{16,24},{20,28},{24,16},{28,20},{1,9},{5... | collective-permute-start | bytes 1179656 | tf_op jit(solution)/shard_map/ppermute | solution.py:21
  60.1 23.1 %collective-permute-start.18 = (bf16[96,2048]{1,0:T(8,128)(2,1)S(1)}, bf16[96,2048]{1,0:T(8,128)(2,1)S(1)}, u32[]{:S(2)}, u32[]{:S(2)}) collective-permute-start(bf16[96,2048]{1,0:T(8,128)(2,1)S(1)} %get-tuple-element.34.refs_0_), channel_id=1, source_target_pairs={{0,16},{4,20},{8,24},{12,28},{16,0},{20,4},{24,8},{28,12},{1,17},{... | collective-permute-start | bytes 1179656 | tf_op jit(solution)/shard_map/ppermute | solution.py:21
  63.7 20.8 %collective-permute-start.19 = (bf16[96,2048]{1,0:T(8,128)(2,1)S(1)}, bf16[96,2048]{1,0:T(8,128)(2,1)S(1)}, u32[]{:S(2)}, u32[]{:S(2)}) collective-permute-start(bf16[96,2048]{1,0:T(8,128)(2,1)S(1)} %get-tuple-element.34.refs_0_), channel_id=1, source_target_pairs={{0,24},{4,28},{8,16},{12,20},{16,8},{20,12},{24,0},{28,4},{1,25},{... | collective-permute-start | bytes 1179656 | tf_op jit(solution)/shard_map/ppermute | solution.py:21
  67.4 32.1 %collective-permute-start.26 = (bf16[1536,256]{1,0:T(8,128)(2,1)S(1)}, bf16[1536,256]{1,0:T(8,128)(2,1)S(1)}, u32[]{:S(2)}, u32[]{:S(2)}) collective-permute-start(bf16[1536,256]{1,0:T(8,128)(2,1)S(1)} %slice.91), channel_id=1, source_target_pairs={{0,1},{1,0},{2,3},{3,2},{4,5},{5,4},{6,7},{7,6},{8,9},{9,8},{10,11... | collective-permute-start | bytes 2359304 | tf_op jit(solution)/shard_map/ppermute | solution.py:21
  83.3 20.4 %collective-permute-start.28 = (bf16[1536,256]{1,0:T(8,128)(2,1)S(1)}, bf16[1536,256]{1,0:T(8,128)(2,1)S(1)}, u32[]{:S(2)}, u32[]{:S(2)}) collective-permute-start(bf16[1536,256]{1,0:T(8,128)(2,1)S(1)} %slice.93), channel_id=1, source_target_pairs={{0,2},{1,3},{2,0},{3,1},{4,6},{5,7},{6,4},{7,5},{8,10},{9,11},{10,... | collective-permute-start | bytes 2359304 | tf_op jit(solution)/shard_map/ppermute | solution.py:21
  84.5 41.7 %collective-permute-start.30 = (bf16[2048,256]{1,0:T(8,128)(2,1)S(1)}, bf16[2048,256]{1,0:T(8,128)(2,1)S(1)}, u32[]{:S(2)}, u32[]{:S(2)}) collective-permute-start(bf16[2048,256]{1,0:T(8,128)(2,1)S(1)} %collective-permute-done.24.refs_2_), channel_id=1, source_target_pairs={{0,2},{1,3},{2,0},{3,1},{4,6},{5,7},{6,4},{7,5},{8,10},{9,11},{10,... | collective-permute-start | bytes 3145736 | tf_op jit(solution)/shard_map/ppermute | solution.py:21
  85.4 48.8 %collective-permute-start.31 = (bf16[2048,256]{1,0:T(8,128)(2,1)S(1)}, bf16[2048,256]{1,0:T(8,128)(2,1)S(1)}, u32[]{:S(2)}, u32[]{:S(2)}) collective-permute-start(bf16[2048,256]{1,0:T(8,128)(2,1)S(1)} %collective-permute-done.29.refs_7_), channel_id=1, source_target_pairs={{0,1},{1,0},{2,3},{3,2},{4,5},{5,4},{6,7},{7,6},{8,9},{9,8},{10,11... | collective-permute-start | bytes 3145736 | tf_op jit(solution)/shard_map/ppermute | solution.py:21
  86.2 17.5 %collective-permute-start.21 = (bf16[96,2048]{1,0:T(8,128)(2,1)S(1)}, bf16[96,2048]{1,0:T(8,128)(2,1)S(1)}, u32[]{:S(2)}, u32[]{:S(2)}) collective-permute-start(bf16[96,2048]{1,0:T(8,128)(2,1)S(1)} %collective-permute-done.17.refs_1_), channel_id=1, source_target_pairs={{0,4},{4,0},{8,12},{12,8},{16,20},{20,16},{24,28},{28,24},{1,5},{5... | collective-permute-start | bytes 1179656 | tf_op jit(solution)/shard_map/ppermute | solution.py:21
  103.7 32.3 %collective-permute-start.48 = (bf16[1024,256]{1,0:T(8,128)(2,1)S(1)}, bf16[1024,256]{1,0:T(8,128)(2,1)S(1)}, u32[]{:S(2)}, u32[]{:S(2)}) collective-permute-start(bf16[1024,256]{1,0:T(8,128)(2,1)S(1)} %collective-permute-done.36.refs_4_), channel_id=1, source_target_pairs={{0,2},{1,3},{2,0},{3,1},{4,6},{5,7},{6,4},{7,5},{8,10},{9,11},{10,... | collective-permute-start | bytes 1572872 | tf_op jit(solution)/shard_map/ppermute | solution.py:21
  104.9 31.1 %collective-permute-start.49 = (bf16[1024,256]{1,0:T(8,128)(2,1)S(1)}, bf16[1024,256]{1,0:T(8,128)(2,1)S(1)}, u32[]{:S(2)}, u32[]{:S(2)}) collective-permute-start(bf16[1024,256]{1,0:T(8,128)(2,1)S(1)} %collective-permute-done.37.refs_5_), channel_id=1, source_target_pairs={{0,1},{1,0},{2,3},{3,2},{4,5},{5,4},{6,7},{7,6},{8,9},{9,8},{10,11... | collective-permute-start | bytes 1572872 | tf_op jit(solution)/shard_map/ppermute | solution.py:21
  106.3 33.5 %collective-permute-start.42 = (bf16[1024,256]{1,0:T(8,128)(2,1)S(1)}, bf16[1024,256]{1,0:T(8,128)(2,1)S(1)}, u32[]{:S(2)}, u32[]{:S(2)}) collective-permute-start(bf16[1024,256]{1,0:T(8,128)(2,1)S(1)} %get-tuple-element.55), channel_id=1, source_target_pairs={{0,1},{1,0},{2,3},{3,2},{4,5},{5,4},{6,7},{7,6},{8,9},{9,8},{10,11... | collective-permute-start | bytes 1572872 | tf_op jit(solution)/shard_map/ppermute | solution.py:21
  126.1 15.0 %collective-permute-start.43 = (bf16[1024,256]{1,0:T(8,128)(2,1)S(1)}, bf16[1024,256]{1,0:T(8,128)(2,1)S(1)}, u32[]{:S(2)}, u32[]{:S(2)}) collective-permute-start(bf16[1024,256]{1,0:T(8,128)(2,1)S(1)} %get-tuple-element.56), channel_id=1, source_target_pairs={{0,2},{1,3},{2,0},{3,1},{4,6},{5,7},{6,4},{7,5},{8,10},{9,11},{10,... | collective-permute-start | bytes 1572872 | tf_op jit(solution)/shard_map/ppermute | solution.py:21
  150.2 15.4 %collective-permute-start.46 = (bf16[96,512]{1,0:T(8,128)(2,1)S(1)}, bf16[96,512]{1,0:T(8,128)(2,1)S(1)}, u32[]{:S(2)}, u32[]{:S(2)}) collective-permute-start(bf16[96,512]{1,0:T(8,128)(2,1)S(1)} %get-tuple-element.65), channel_id=1, source_target_pairs={{0,16},{4,20},{8,24},{12,28},{16,0},{20,4},{24,8},{28,12},{1,17},{... | collective-permute-start | bytes 294920 | tf_op jit(solution)/shard_map/ppermute | solution.py:21
  156.4 15.7 %collective-permute-start.39 = (bf16[96,512]{1,0:T(8,128)(2,1)S(1)}, bf16[96,512]{1,0:T(8,128)(2,1)S(1)}, u32[]{:S(2)}, u32[]{:S(2)}) collective-permute-start(bf16[96,512]{1,0:T(8,128)(2,1)S(1)} %get-tuple-element.69), channel_id=1, source_target_pairs={{0,8},{4,12},{8,0},{12,4},{16,24},{20,28},{24,16},{28,20},{1,9},{5... | collective-permute-start | bytes 294920 | tf_op jit(solution)/shard_map/ppermute | solution.py:21
  156.4 18.9 %collective-permute-start.40 = (bf16[96,512]{1,0:T(8,128)(2,1)S(1)}, bf16[96,512]{1,0:T(8,128)(2,1)S(1)}, u32[]{:S(2)}, u32[]{:S(2)}) collective-permute-start(bf16[96,512]{1,0:T(8,128)(2,1)S(1)} %get-tuple-element.68), channel_id=1, source_target_pairs={{0,16},{4,20},{8,24},{12,28},{16,0},{20,4},{24,8},{28,12},{1,17},{... | collective-permute-start | bytes 294920 | tf_op jit(solution)/shard_map/ppermute | solution.py:21
  165.7 16.0 %collective-permute-start.34 = (bf16[96,512]{1,0:T(8,128)(2,1)S(1)}, bf16[96,512]{1,0:T(8,128)(2,1)S(1)}, u32[]{:S(2)}, u32[]{:S(2)}) collective-permute-start(bf16[96,512]{1,0:T(8,128)(2,1)S(1)} %get-tuple-element.71), channel_id=1, source_target_pairs={{0,16},{4,20},{8,24},{12,28},{16,0},{20,4},{24,8},{28,12},{1,17},{... | collective-permute-start | bytes 294920 | tf_op jit(solution)/shard_map/ppermute | solution.py:21
  (47 other events, 365.9 us)

commit v7 on v6

--- a/solution.py
+++ b/solution.py
@@ -29,15 +29,20 @@
     ]
 
 
+def exchange(parts, axis, unit):
+    got = {0: parts[0]}
+    for k in range(len(parts) - 1, 0, -1):
+        got[k] = swap_with(parts[k], axis, unit * k)
+    return [got[k] for k in range(len(parts))]
+
+
 def exchange_all(part, axis):
-    return [part] + [swap_with(part, axis, k) for k in range(1, lax.axis_size(axis))]
+    return exchange([part] * lax.axis_size(axis), axis, 1)
 
 
 def line_gather(part, axis):
     size = lax.axis_size(axis)
-    mine = [part]
-    for k in range(1, size // 2):
-        mine.append(swap_with(part, axis, 2 * k))
+    mine = exchange([part] * (size // 2), axis, 2)
     return mine + [swap_with(m, axis, 1) for m in mine]
 
 
@@ -263,23 +268,24 @@
     )(*flat)
 
 
-def down_kernel(parts, place_ref, share_ref, *refs):
+def down_kernel(parts, first, place_ref, share_ref, *refs):
     hidden, weights, out_ref = refs[:parts], refs[parts:-1], refs[-1]
     depth, total = hidden[0].shape[1], None
+    kept = slice(first, first + out_ref.shape[0])
     for k in range(parts):
         rows = pl.ds(pl.multiple_of((place_ref[1] ^ k) * depth, depth), depth)
         near = [weight[rows, :] for weight in weights]
         near = near[0] if len(near) == 1 else jnp.concatenate(near, axis=1)
-        piece = jnp.dot(hidden[k][...], near, preferred_element_type=F32)
+        piece = jnp.dot(hidden[k][kept, :], near, preferred_element_type=F32)
         total = piece if total is None else total + piece
-    out_ref[...] = (total * share_ref[...]).astype(BF16)
-
-
-def weighted_outputs(place, share, hidden, weights):
+    out_ref[...] = (total * share_ref[kept, :]).astype(out_ref.dtype)
+
+
+def weighted_outputs(place, share, hidden, weights, first, rows, dtype):
     wide = sum(w.shape[1] for w in weights)
     return pl.pallas_call(
-        functools.partial(down_kernel, len(hidden)),
-        out_shape=jax.ShapeDtypeStruct((hidden[0].shape[0], wide), BF16),
+        functools.partial(down_kernel, len(hidden), first),
+        out_shape=jax.ShapeDtypeStruct((rows, wide), dtype),
         in_specs=[pl.BlockSpec(memory_space=pltpu.SMEM)]
         + in_vmem(1 + len(hidden) + len(weights)),
         out_specs=in_vmem(1)[0],
@@ -436,7 +442,7 @@
         return pairs, [[w] for w in down], lambda *parts: list(parts)
     gate1 = swap_with(w_gate, "tp", 1)
     up2 = swap_with(w_up, "tp", 2)
-    top = w_gate.shape[0] // 4
+    top = w_gate.shape[0] * 5 // 16
     later_gate, later_up = later_of(w_gate), later_of(w_up)
     up1_top = swap_with(later_up[:top], "tp", 1)
     gate2_top = swap_with(later_gate[:top], "tp", 2)
@@ -526,7 +532,7 @@
     mixed = ALPHA * residual.astype(F32) + mixer_out
 
     sent = rows_to_send(place, mixed, tp)
-    both = [sent[0]] + [swap_with(sent[k], "tp", k) for k in range(1, tp)]
+    both = exchange(sent, "tp", 1)
     tokens, normed, scales = first_norm(place, both, gains)
 
     everyone = line_gather(tokens, "sp")
@@ -538,17 +544,18 @@
     groups = []
     half_rows = (sp // 2) * quarter
     for k in range(len(down_w)):
-        partial = weighted_outputs(place, share, hidden_rel, down_w[k])
-        other = swap_with(partial[half_rows:], "sp", 1)
-        joined = partial[:half_rows].astype(F32) + other.astype(F32)
+        common = (place, share, hidden_rel, down_w[k])
+        other = weighted_outputs(*common, half_rows, half_rows, BF16)
+        other = swap_with(other, "sp", 1)
+        own = weighted_outputs(*common, 0, half_rows, F32)
+        joined = own + other.astype(F32)
         sent = joined.astype(BF16)
-        got = [
-            swap_with(sent[d * quarter : (d + 1) * quarter], "sp", 2 * d)
-            for d in range(1, sp // 2)
-        ]
-        groups.append([joined[:quarter]] + got)
+        got = exchange(
+            [sent[d * quarter : (d + 1) * quarter] for d in range(sp // 2)], "sp", 2
+        )
+        groups.append([joined[:quarter]] + got[1:])
     out_rel = last_norm(by_distance, normed, scales, groups)
-    home_rel = [out_rel[0]] + [swap_with(out_rel[k], "tp", k) for k in range(1, tp)]
+    home_rel = exchange(out_rel, "tp", 1)
     return jnp.concatenate(in_order(home_rel, j))
 
 

time: 192 us -> 228 us (1.19)
  waiting for transfers between devices: 87.6 us -> 113 us
  starting transfers between devices: 71.5 us -> 79.7 us
  Pallas kernels: 19.6 us -> 22.4 us
    ppermute x57, waiting for transfers between devices: 87.6 us -> 113 us  [swap_with(): return lax.ppermute(part, axis, [(i, i ^ bits) for i in range(size)])]
    ppermute x57, starting transfers between devices: 71.5 us -> 79.7 us  [swap_with(): return lax.ppermute(part, axis, [(i, i ^ bits) for i in range(size)])]
    pallas_call x4 -> x8, Pallas kernels: 6.26 us -> 9.11 us  [weighted_outputs(): pl.pallas_call(functools.partial(down_kernel, len(hidden), first), out_sh...]
  transfers between devices with their start and end apart: 57 -> 57, of which waited for: 21 -> 18; matrix products, arithmetic and copies ran while one was open for 3% -> 3% of each run, Pallas kernels for 10% -> 10%
where the time goes in v7:
time: 228 us; the launch traced here: 227 us
  waiting for transfers between devices  113 us (50%)
  starting transfers between devices  79.7 us (35%)
  Pallas kernels  22.4 us (10%)
  local copies, waits for them, and re-layouts  7.97 us (3%)
  other arithmetic  3.18 us (1%)
    ppermute x57, waiting for transfers between devices, swap_with(): return lax.ppermute(part, axis, [(i, i ^ bits) for i in range(size)])  113 us
    ppermute x57, starting transfers between devices, swap_with(): return lax.ppermute(part, axis, [(i, i ^ bits) for i in range(size)])  79.7 us
    pallas_call x8, Pallas kernels, weighted_outputs(): pl.pallas_call(functools.partial(down_kernel, len(hidden), first), out_sh...  9.11 us
    pallas_call x4, Pallas kernels, hidden_units(): pl.pallas_call(functools.partial(hidden_kernel, count), out_shape=outs, i...  7.19 us
    unnamed x28, local copies, waits for them, and re-layouts  4.82 us
  transfers between devices with their start and end apart: 57, of which 18 were waited for; matrix products, arithmetic and copies ran while one was open for 3% of the time, Pallas kernels for 10%

profile of v7, /device:TPU:0, one launch (start us, length us, event | category | flops | bytes accessed | tf_op | source)
XLA Modules:
  0.0 227.3 jit_solution(15709288884316054166)
XLA Ops:
  3.1 2.5 %collective-permute-start.10 = (f32[8,512]{1,0:T(8,128)S(1)}, f32[8,512]{1,0:T(8,128)S(1)}, u32[]{:S(2)}, u32[]{:S(2)}) collective-permute-start(f32[8,512]{1,0:T(8,128)S(1)} %select_maximum_fusion.refs_4_), channel_id=1, source_target_pairs={{0,1},{1,0},{2,3},{3,2},{4,5},{5,4},{6,7},{7,6},{8,9},{9,8},{10,11... | collective-permute-start | bytes 49160 | tf_op jit(solution)/shard_map/ppermute | solution.py:21
  8.9 2.6 %collective-permute-start.2 = (f32[2,24,128]{2,1,0:T(8,128)S(1)}, f32[2,24,128]{2,1,0:T(8,128)S(1)}, u32[]{:S(2)}, u32[]{:S(2)}) collective-permute-start(f32[2,24,128]{2,1,0:T(8,128)S(1)} %pad_maximum_fusion.4), channel_id=1, source_target_pairs={{0,16},{4,20},{8,24},{12,28},{16,0},{20,4},{24,8},{28,12},{1,17},{... | collective-permute-start | bytes 73736 | tf_op jit(solution)/shard_map/ppermute | solution.py:21
  33.5 2.4 %collective-permute-start.25 = (bf16[640,256]{1,0:T(8,128)(2,1)S(1)}, bf16[640,256]{1,0:T(8,128)(2,1)S(1)}, u32[]{:S(2)}, u32[]{:S(2)}) collective-permute-start(bf16[640,256]{1,0:T(8,128)(2,1)S(1)} %slice.66), channel_id=1, source_target_pairs={{0,1},{1,0},{2,3},{3,2},{4,5},{5,4},{6,7},{7,6},{8,9},{9,8},{10,11... | collective-permute-start | bytes 983048 | tf_op jit(solution)/shard_map/ppermute | solution.py:21
  40.5 6.6 %collective-permute-done.7.refs_1_ = bf16[96,640]{1,0:T(8,128)(2,1)S(1)} collective-permute-done((bf16[96,640]{1,0:T(8,128)(2,1)S(1)}, bf16[96,640]{1,0:T(8,128)(2,1)S(1)}, u32[]{:S(2)}, u32[]{:S(2)}) %collective-permute-start.7) | collective-permute-done | bytes 122912 | tf_op jit(solution)/shard_map/ppermute | solution.py:21
  47.1 2.1 collective-permute-start.24
  53.5 25.9 %collective-permute-done.36.refs_4_ = bf16[1024,256]{1,0:T(8,128)(2,1)S(1)} collective-permute-done((bf16[1024,256]{1,0:T(8,128)(2,1)S(1)}, bf16[1024,256]{1,0:T(8,128)(2,1)S(1)}, u32[]{:S(2)}, u32[]{:S(2)}) %collective-permute-start.36) | collective-permute-done | bytes 524320 | tf_op jit(solution)/shard_map/ppermute | solution.py:21
  79.5 2.0 collective-permute-start.19
  81.5 2.3 %collective-permute-start.26 = (bf16[1408,256]{1,0:T(8,128)(2,1)S(1)}, bf16[1408,256]{1,0:T(8,128)(2,1)S(1)}, u32[]{:S(2)}, u32[]{:S(2)}) collective-permute-start(bf16[1408,256]{1,0:T(8,128)(2,1)S(1)} %slice.67), channel_id=1, source_target_pairs={{0,1},{1,0},{2,3},{3,2},{4,5},{5,4},{6,7},{7,6},{8,9},{9,8},{10,11... | collective-permute-start | bytes 2162696 | tf_op jit(solution)/shard_map/ppermute | solution.py:21
  83.9 18.2 %collective-permute-done.18.refs_2_ = bf16[96,2048]{1,0:T(8,128)(2,1)S(1)} collective-permute-done((bf16[96,2048]{1,0:T(8,128)(2,1)S(1)}, bf16[96,2048]{1,0:T(8,128)(2,1)S(1)}, u32[]{:S(2)}, u32[]{:S(2)}) %collective-permute-start.18) | collective-permute-done | bytes 393248 | tf_op jit(solution)/shard_map/ppermute | solution.py:21
  102.1 2.1 collective-permute-start.28
  106.4 14.9 %collective-permute-done.28.refs_6_ = bf16[1408,256]{1,0:T(8,128)(2,1)S(1)} collective-permute-done((bf16[1408,256]{1,0:T(8,128)(2,1)S(1)}, bf16[1408,256]{1,0:T(8,128)(2,1)S(1)}, u32[]{:S(2)}, u32[]{:S(2)}) %collective-permute-start.28) | collective-permute-done | bytes 720928 | tf_op jit(solution)/shard_map/ppermute | solution.py:21
  121.3 2.0 collective-permute-start.48
  125.3 18.4 %collective-permute-done.30.refs_1_ = bf16[2048,256]{1,0:T(8,128)(2,1)S(1)} collective-permute-done((bf16[2048,256]{1,0:T(8,128)(2,1)S(1)}, bf16[2048,256]{1,0:T(8,128)(2,1)S(1)}, u32[]{:S(2)}, u32[]{:S(2)}) %collective-permute-start.30) | collective-permute-done | bytes 1048608 | tf_op jit(solution)/shard_map/ppermute | solution.py:21
  143.8 2.0 collective-permute-start.43
  158.4 7.6 %collective-permute-done.43.refs_5_ = bf16[1024,256]{1,0:T(8,128)(2,1)S(1)} collective-permute-done((bf16[1024,256]{1,0:T(8,128)(2,1)S(1)}, bf16[1024,256]{1,0:T(8,128)(2,1)S(1)}, u32[]{:S(2)}, u32[]{:S(2)}) %collective-permute-start.43) | collective-permute-done | bytes 524320 | tf_op jit(solution)/shard_map/ppermute | solution.py:21
  172.7 8.3 %collective-permute-start.51 = (bf16[96,512]{1,0:T(8,128)(2,1)S(1)}, bf16[96,512]{1,0:T(8,128)(2,1)S(1)}, u32[]{:S(2)}, u32[]{:S(2)}) collective-permute-start(bf16[96,512]{1,0:T(8,128)(2,1)S(1)} %get-tuple-element.63), channel_id=1, source_target_pairs={{0,8},{4,12},{8,0},{12,4},{16,24},{20,28},{24,16},{28,20},{1,9},{5... | collective-permute-start | bytes 294920 | tf_op jit(solution)/shard_map/ppermute | solution.py:21
  181.6 1.9 collective-permute-start.53
  186.7 2.0 collective-permute-start.47
  188.6 3.3 %collective-permute-done.52.refs_14_ = bf16[96,512]{1,0:T(8,128)(2,1)S(1)} collective-permute-done((bf16[96,512]{1,0:T(8,128)(2,1)S(1)}, bf16[96,512]{1,0:T(8,128)(2,1)S(1)}, u32[]{:S(2)}, u32[]{:S(2)}) %collective-permute-start.52) | collective-permute-done | bytes 98336 | tf_op jit(solution)/shard_map/ppermute | solution.py:21
  191.9 7.3 %collective-permute-start.40 = (bf16[96,512]{1,0:T(8,128)(2,1)S(1)}, bf16[96,512]{1,0:T(8,128)(2,1)S(1)}, u32[]{:S(2)}, u32[]{:S(2)}) collective-permute-start(bf16[96,512]{1,0:T(8,128)(2,1)S(1)} %get-tuple-element.68), channel_id=1, source_target_pairs={{0,16},{4,20},{8,24},{12,28},{16,0},{20,4},{24,8},{28,12},{1,17},{... | collective-permute-start | bytes 294920 | tf_op jit(solution)/shard_map/ppermute | solution.py:21
  199.3 1.9 collective-permute-start.41
  202.5 5.2 %collective-permute-start.34 = (bf16[96,512]{1,0:T(8,128)(2,1)S(1)}, bf16[96,512]{1,0:T(8,128)(2,1)S(1)}, u32[]{:S(2)}, u32[]{:S(2)}) collective-permute-start(bf16[96,512]{1,0:T(8,128)(2,1)S(1)} %get-tuple-element.71), channel_id=1, source_target_pairs={{0,16},{4,20},{8,24},{12,28},{16,0},{20,4},{24,8},{28,12},{1,17},{... | collective-permute-start | bytes 294920 | tf_op jit(solution)/shard_map/ppermute | solution.py:21
  210.9 6.3 %collective-permute-done.34.refs_2_ = bf16[96,512]{1,0:T(8,128)(2,1)S(1)} collective-permute-done((bf16[96,512]{1,0:T(8,128)(2,1)S(1)}, bf16[96,512]{1,0:T(8,128)(2,1)S(1)}, u32[]{:S(2)}, u32[]{:S(2)}) %collective-permute-start.34) | collective-permute-done | bytes 98336 | tf_op jit(solution)/shard_map/ppermute | solution.py:21
  221.2 2.1 collective-permute-done.54
  (171 shorter events, 76.6 us)
Async XLA Ops:
  3.1 33.9 %collective-permute-start.10 = (f32[8,512]{1,0:T(8,128)S(1)}, f32[8,512]{1,0:T(8,128)S(1)}, u32[]{:S(2)}, u32[]{:S(2)}) collective-permute-start(f32[8,512]{1,0:T(8,128)S(1)} %select_maximum_fusion.refs_4_), channel_id=1, source_target_pairs={{0,1},{1,0},{2,3},{3,2},{4,5},{5,4},{6,7},{7,6},{8,9},{9,8},{10,11... | collective-permute-start | bytes 49160 | tf_op jit(solution)/shard_map/ppermute | solution.py:21
  14.7 23.7 %collective-permute-start.11 = (f32[8,512]{1,0:T(8,128)S(1)}, f32[8,512]{1,0:T(8,128)S(1)}, u32[]{:S(2)}, u32[]{:S(2)}) collective-permute-start(f32[8,512]{1,0:T(8,128)S(1)} %select_maximum_fusion.refs_4_), channel_id=1, source_target_pairs={{0,2},{1,3},{2,0},{3,1},{4,6},{5,7},{6,4},{7,5},{8,10},{9,11},{10,... | collective-permute-start | bytes 49160 | tf_op jit(solution)/shard_map/ppermute | solution.py:21
  33.5 17.7 %collective-permute-start.25 = (bf16[640,256]{1,0:T(8,128)(2,1)S(1)}, bf16[640,256]{1,0:T(8,128)(2,1)S(1)}, u32[]{:S(2)}, u32[]{:S(2)}) collective-permute-start(bf16[640,256]{1,0:T(8,128)(2,1)S(1)} %slice.66), channel_id=1, source_target_pairs={{0,1},{1,0},{2,3},{3,2},{4,5},{5,4},{6,7},{7,6},{8,9},{9,8},{10,11... | collective-permute-start | bytes 983048 | tf_op jit(solution)/shard_map/ppermute | solution.py:21
  36.0 17.5 %collective-permute-start.27 = (bf16[640,256]{1,0:T(8,128)(2,1)S(1)}, bf16[640,256]{1,0:T(8,128)(2,1)S(1)}, u32[]{:S(2)}, u32[]{:S(2)}) collective-permute-start(bf16[640,256]{1,0:T(8,128)(2,1)S(1)} %slice.68), channel_id=1, source_target_pairs={{0,2},{1,3},{2,0},{3,1},{4,6},{5,7},{6,4},{7,5},{8,10},{9,11},{10,... | collective-permute-start | bytes 983048 | tf_op jit(solution)/shard_map/ppermute | solution.py:21
  47.1 57.2 %collective-permute-start.24 = (bf16[2048,256]{1,0:T(8,128)(2,1)S(1)}, bf16[2048,256]{1,0:T(8,128)(2,1)S(1)}, u32[]{:S(2)}, u32[]{:S(2)}) collective-permute-start(bf16[2048,256]{1,0:T(8,128)(2,1)S(1)} %bitcast.61), channel_id=1, source_target_pairs={{0,1},{1,0},{2,3},{3,2},{4,5},{5,4},{6,7},{7,6},{8,9},{9,8},{10,11... | collective-permute-start | bytes 3145736 | tf_op jit(solution)/shard_map/ppermute | solution.py:21
  49.2 30.3 %collective-permute-start.36 = (bf16[1024,256]{1,0:T(8,128)(2,1)S(1)}, bf16[1024,256]{1,0:T(8,128)(2,1)S(1)}, u32[]{:S(2)}, u32[]{:S(2)}) collective-permute-start(bf16[1024,256]{1,0:T(8,128)(2,1)S(1)} %get-tuple-element.56), channel_id=1, source_target_pairs={{0,1},{1,0},{2,3},{3,2},{4,5},{5,4},{6,7},{7,6},{8,9},{9,8},{10,11... | collective-permute-start | bytes 1572872 | tf_op jit(solution)/shard_map/ppermute | solution.py:21
  50.3 29.2 %collective-permute-start.37 = (bf16[1024,256]{1,0:T(8,128)(2,1)S(1)}, bf16[1024,256]{1,0:T(8,128)(2,1)S(1)}, u32[]{:S(2)}, u32[]{:S(2)}) collective-permute-start(bf16[1024,256]{1,0:T(8,128)(2,1)S(1)} %get-tuple-element.55), channel_id=1, source_target_pairs={{0,2},{1,3},{2,0},{3,1},{4,6},{5,7},{6,4},{7,5},{8,10},{9,11},{10,... | collective-permute-start | bytes 1572872 | tf_op jit(solution)/shard_map/ppermute | solution.py:21
  51.2 53.2 %collective-permute-start.29 = (bf16[2048,256]{1,0:T(8,128)(2,1)S(1)}, bf16[2048,256]{1,0:T(8,128)(2,1)S(1)}, u32[]{:S(2)}, u32[]{:S(2)}) collective-permute-start(bf16[2048,256]{1,0:T(8,128)(2,1)S(1)} %bitcast.65), channel_id=1, source_target_pairs={{0,2},{1,3},{2,0},{3,1},{4,6},{5,7},{6,4},{7,5},{8,10},{9,11},{10,... | collective-permute-start | bytes 3145736 | tf_op jit(solution)/shard_map/ppermute | solution.py:21
  53.5 28.1 %collective-permute-start.17 = (bf16[96,2048]{1,0:T(8,128)(2,1)S(1)}, bf16[96,2048]{1,0:T(8,128)(2,1)S(1)}, u32[]{:S(2)}, u32[]{:S(2)}) collective-permute-start(bf16[96,2048]{1,0:T(8,128)(2,1)S(1)} %get-tuple-element.34.refs_0_), channel_id=1, source_target_pairs={{0,8},{4,12},{8,0},{12,4},{16,24},{20,28},{24,16},{28,20},{1,9},{5... | collective-permute-start | bytes 1179656 | tf_op jit(solution)/shard_map/ppermute | solution.py:21
  79.5 22.6 %collective-permute-start.18 = (bf16[96,2048]{1,0:T(8,128)(2,1)S(1)}, bf16[96,2048]{1,0:T(8,128)(2,1)S(1)}, u32[]{:S(2)}, u32[]{:S(2)}) collective-permute-start(bf16[96,2048]{1,0:T(8,128)(2,1)S(1)} %get-tuple-element.34.refs_0_), channel_id=1, source_target_pairs={{0,16},{4,20},{8,24},{12,28},{16,0},{20,4},{24,8},{28,12},{1,17},{... | collective-permute-start | bytes 1179656 | tf_op jit(solution)/shard_map/ppermute | solution.py:21
  79.5 22.6 %collective-permute-start.19 = (bf16[96,2048]{1,0:T(8,128)(2,1)S(1)}, bf16[96,2048]{1,0:T(8,128)(2,1)S(1)}, u32[]{:S(2)}, u32[]{:S(2)}) collective-permute-start(bf16[96,2048]{1,0:T(8,128)(2,1)S(1)} %get-tuple-element.34.refs_0_), channel_id=1, source_target_pairs={{0,24},{4,28},{8,16},{12,20},{16,8},{20,12},{24,0},{28,4},{1,25},{... | collective-permute-start | bytes 1179656 | tf_op jit(solution)/shard_map/ppermute | solution.py:21
  81.5 24.4 %collective-permute-start.26 = (bf16[1408,256]{1,0:T(8,128)(2,1)S(1)}, bf16[1408,256]{1,0:T(8,128)(2,1)S(1)}, u32[]{:S(2)}, u32[]{:S(2)}) collective-permute-start(bf16[1408,256]{1,0:T(8,128)(2,1)S(1)} %slice.67), channel_id=1, source_target_pairs={{0,1},{1,0},{2,3},{3,2},{4,5},{5,4},{6,7},{7,6},{8,9},{9,8},{10,11... | collective-permute-start | bytes 2162696 | tf_op jit(solution)/shard_map/ppermute | solution.py:21
  102.1 19.1 %collective-permute-start.28 = (bf16[1408,256]{1,0:T(8,128)(2,1)S(1)}, bf16[1408,256]{1,0:T(8,128)(2,1)S(1)}, u32[]{:S(2)}, u32[]{:S(2)}) collective-permute-start(bf16[1408,256]{1,0:T(8,128)(2,1)S(1)} %slice.69), channel_id=1, source_target_pairs={{0,2},{1,3},{2,0},{3,1},{4,6},{5,7},{6,4},{7,5},{8,10},{9,11},{10,... | collective-permute-start | bytes 2162696 | tf_op jit(solution)/shard_map/ppermute | solution.py:21
  104.3 39.5 %collective-permute-start.30 = (bf16[2048,256]{1,0:T(8,128)(2,1)S(1)}, bf16[2048,256]{1,0:T(8,128)(2,1)S(1)}, u32[]{:S(2)}, u32[]{:S(2)}) collective-permute-start(bf16[2048,256]{1,0:T(8,128)(2,1)S(1)} %collective-permute-done.24.refs_2_), channel_id=1, source_target_pairs={{0,2},{1,3},{2,0},{3,1},{4,6},{5,7},{6,4},{7,5},{8,10},{9,11},{10,... | collective-permute-start | bytes 3145736 | tf_op jit(solution)/shard_map/ppermute | solution.py:21
  104.4 48.2 %collective-permute-start.31 = (bf16[2048,256]{1,0:T(8,128)(2,1)S(1)}, bf16[2048,256]{1,0:T(8,128)(2,1)S(1)}, u32[]{:S(2)}, u32[]{:S(2)}) collective-permute-start(bf16[2048,256]{1,0:T(8,128)(2,1)S(1)} %collective-permute-done.29.refs_7_), channel_id=1, source_target_pairs={{0,1},{1,0},{2,3},{3,2},{4,5},{5,4},{6,7},{7,6},{8,9},{9,8},{10,11... | collective-permute-start | bytes 3145736 | tf_op jit(solution)/shard_map/ppermute | solution.py:21
  105.9 17.4 %collective-permute-start.22 = (bf16[96,2048]{1,0:T(8,128)(2,1)S(1)}, bf16[96,2048]{1,0:T(8,128)(2,1)S(1)}, u32[]{:S(2)}, u32[]{:S(2)}) collective-permute-start(bf16[96,2048]{1,0:T(8,128)(2,1)S(1)} %collective-permute-done.18.refs_2_), channel_id=1, source_target_pairs={{0,4},{4,0},{8,12},{12,8},{16,20},{20,16},{24,28},{28,24},{1,5},{5... | collective-permute-start | bytes 1179656 | tf_op jit(solution)/shard_map/ppermute | solution.py:21
  121.3 33.7 %collective-permute-start.48 = (bf16[1024,256]{1,0:T(8,128)(2,1)S(1)}, bf16[1024,256]{1,0:T(8,128)(2,1)S(1)}, u32[]{:S(2)}, u32[]{:S(2)}) collective-permute-start(bf16[1024,256]{1,0:T(8,128)(2,1)S(1)} %collective-permute-done.36.refs_4_), channel_id=1, source_target_pairs={{0,2},{1,3},{2,0},{3,1},{4,6},{5,7},{6,4},{7,5},{8,10},{9,11},{10,... | collective-permute-start | bytes 1572872 | tf_op jit(solution)/shard_map/ppermute | solution.py:21
  123.3 31.7 %collective-permute-start.49 = (bf16[1024,256]{1,0:T(8,128)(2,1)S(1)}, bf16[1024,256]{1,0:T(8,128)(2,1)S(1)}, u32[]{:S(2)}, u32[]{:S(2)}) collective-permute-start(bf16[1024,256]{1,0:T(8,128)(2,1)S(1)} %collective-permute-done.37.refs_5_), channel_id=1, source_target_pairs={{0,1},{1,0},{2,3},{3,2},{4,5},{5,4},{6,7},{7,6},{8,9},{9,8},{10,11... | collective-permute-start | bytes 1572872 | tf_op jit(solution)/shard_map/ppermute | solution.py:21
  124.8 33.6 %collective-permute-start.42 = (bf16[1024,256]{1,0:T(8,128)(2,1)S(1)}, bf16[1024,256]{1,0:T(8,128)(2,1)S(1)}, u32[]{:S(2)}, u32[]{:S(2)}) collective-permute-start(bf16[1024,256]{1,0:T(8,128)(2,1)S(1)} %get-tuple-element.55), channel_id=1, source_target_pairs={{0,1},{1,0},{2,3},{3,2},{4,5},{5,4},{6,7},{7,6},{8,9},{9,8},{10,11... | collective-permute-start | bytes 1572872 | tf_op jit(solution)/shard_map/ppermute | solution.py:21
  143.8 22.3 %collective-permute-start.43 = (bf16[1024,256]{1,0:T(8,128)(2,1)S(1)}, bf16[1024,256]{1,0:T(8,128)(2,1)S(1)}, u32[]{:S(2)}, u32[]{:S(2)}) collective-permute-start(bf16[1024,256]{1,0:T(8,128)(2,1)S(1)} %get-tuple-element.56), channel_id=1, source_target_pairs={{0,2},{1,3},{2,0},{3,1},{4,6},{5,7},{6,4},{7,5},{8,10},{9,11},{10,... | collective-permute-start | bytes 1572872 | tf_op jit(solution)/shard_map/ppermute | solution.py:21
  156.1 16.4 %collective-permute-start.50 = (bf16[384,512]{1,0:T(8,128)(2,1)S(1)}, bf16[384,512]{1,0:T(8,128)(2,1)S(1)}, u32[]{:S(2)}, u32[]{:S(2)}) collective-permute-start(bf16[384,512]{1,0:T(8,128)(2,1)S(1)} %down.15), channel_id=1, source_target_pairs={{0,4},{4,0},{8,12},{12,8},{16,20},{20,16},{24,28},{28,24},{1,5},{5... | collective-permute-start | bytes 1179656 | tf_op jit(solution)/shard_map/ppermute | solution.py:21
  169.1 15.9 %collective-permute-start.32 = (bf16[384,512]{1,0:T(8,128)(2,1)S(1)}, bf16[384,512]{1,0:T(8,128)(2,1)S(1)}, u32[]{:S(2)}, u32[]{:S(2)}) collective-permute-start(bf16[384,512]{1,0:T(8,128)(2,1)S(1)} %down.9), channel_id=1, source_target_pairs={{0,4},{4,0},{8,12},{12,8},{16,20},{20,16},{24,28},{28,24},{1,5},{5... | collective-permute-start | bytes 1179656 | tf_op jit(solution)/shard_map/ppermute | solution.py:21
  185.0 17.5 %collective-permute-start.46 = (bf16[96,512]{1,0:T(8,128)(2,1)S(1)}, bf16[96,512]{1,0:T(8,128)(2,1)S(1)}, u32[]{:S(2)}, u32[]{:S(2)}) collective-permute-start(bf16[96,512]{1,0:T(8,128)(2,1)S(1)} %get-tuple-element.65), channel_id=1, source_target_pairs={{0,16},{4,20},{8,24},{12,28},{16,0},{20,4},{24,8},{28,12},{1,17},{... | collective-permute-start | bytes 294920 | tf_op jit(solution)/shard_map/ppermute | solution.py:21
  191.9 18.9 %collective-permute-start.40 = (bf16[96,512]{1,0:T(8,128)(2,1)S(1)}, bf16[96,512]{1,0:T(8,128)(2,1)S(1)}, u32[]{:S(2)}, u32[]{:S(2)}) collective-permute-start(bf16[96,512]{1,0:T(8,128)(2,1)S(1)} %get-tuple-element.68), channel_id=1, source_target_pairs={{0,16},{4,20},{8,24},{12,28},{16,0},{20,4},{24,8},{28,12},{1,17},{... | collective-permute-start | bytes 294920 | tf_op jit(solution)/shard_map/ppermute | solution.py:21
  (47 other events, 417.5 us)

commit v8 on v7

--- a/solution.py
+++ b/solution.py
@@ -442,7 +442,7 @@
         return pairs, [[w] for w in down], lambda *parts: list(parts)
     gate1 = swap_with(w_gate, "tp", 1)
     up2 = swap_with(w_up, "tp", 2)
-    top = w_gate.shape[0] * 5 // 16
+    top = w_gate.shape[0] * 9 // 32
     later_gate, later_up = later_of(w_gate), later_of(w_up)
     up1_top = swap_with(later_up[:top], "tp", 1)
     gate2_top = swap_with(later_gate[:top], "tp", 2)
@@ -497,9 +497,7 @@
     quarter = positions // tp
 
     place = jnp.stack([i, j])
-    gains = jnp.pad(
-        jnp.stack([first_gain, first_bias, second_gain, second_bias]), ((0, 4), (0, 0))
-    )
+    gains = jnp.stack([first_gain, first_bias, second_gain, second_bias])
     gains = exchange_all(gains, "tp")
     pooled = pooled_channels(pool_in, doc_ids, place)
 

time: 228 us -> 228 us (level)
  transfers between devices with their start and end apart: 57 -> 57, of which waited for: 18 -> 19; matrix products, arithmetic and copies ran while one was open for 3% -> 3% of each run, Pallas kernels for 10% -> 10%
where the time goes in v8:
time: 228 us; the launch traced here: 227 us
  waiting for transfers between devices  113 us (50%)
  starting transfers between devices  79.5 us (35%)
  Pallas kernels  22.4 us (10%)
  local copies, waits for them, and re-layouts  7.95 us (3%)
  other arithmetic  3.18 us (1%)
    ppermute x57, waiting for transfers between devices, swap_with(): return lax.ppermute(part, axis, [(i, i ^ bits) for i in range(size)])  113 us
    ppermute x57, starting transfers between devices, swap_with(): return lax.ppermute(part, axis, [(i, i ^ bits) for i in range(size)])  79.5 us
    pallas_call x8, Pallas kernels, weighted_outputs(): pl.pallas_call(functools.partial(down_kernel, len(hidden), first), out_sh...  9.11 us
    pallas_call x4, Pallas kernels, hidden_units(): pl.pallas_call(functools.partial(hidden_kernel, count), out_shape=outs, i...  7.19 us
    unnamed x28, local copies, waits for them, and re-layouts  4.82 us
  transfers between devices with their start and end apart: 57, of which 19 were waited for; matrix products, arithmetic and copies ran while one was open for 3% of the time, Pallas kernels for 10%

profile of v8, /device:TPU:0, one launch (start us, length us, event | category | flops | bytes accessed | tf_op | source)
XLA Modules:
  0.0 227.3 jit_solution(16038636241119772400)
XLA Ops:
  3.1 2.5 %collective-permute-start.10 = (f32[4,512]{1,0:T(4,128)S(1)}, f32[4,512]{1,0:T(4,128)S(1)}, u32[]{:S(2)}, u32[]{:S(2)}) collective-permute-start(f32[4,512]{1,0:T(4,128)S(1)} %pad_maximum_fusion.5.refs_4_), channel_id=1, source_target_pairs={{0,1},{1,0},{2,3},{3,2},{4,5},{5,4},{6,7},{7,6},{8,9},{9,8},{10,11... | collective-permute-start | bytes 24584 | tf_op jit(solution)/shard_map/ppermute | solution.py:21
  8.9 2.6 %collective-permute-start.2 = (f32[2,24,128]{2,1,0:T(8,128)S(1)}, f32[2,24,128]{2,1,0:T(8,128)S(1)}, u32[]{:S(2)}, u32[]{:S(2)}) collective-permute-start(f32[2,24,128]{2,1,0:T(8,128)S(1)} %pad_maximum_fusion.4), channel_id=1, source_target_pairs={{0,16},{4,20},{8,24},{12,28},{16,0},{20,4},{24,8},{28,12},{1,17},{... | collective-permute-start | bytes 73736 | tf_op jit(solution)/shard_map/ppermute | solution.py:21
  33.5 2.4 %collective-permute-start.25 = (bf16[576,256]{1,0:T(8,128)(2,1)S(1)}, bf16[576,256]{1,0:T(8,128)(2,1)S(1)}, u32[]{:S(2)}, u32[]{:S(2)}) collective-permute-start(bf16[576,256]{1,0:T(8,128)(2,1)S(1)} %slice.66), channel_id=1, source_target_pairs={{0,1},{1,0},{2,3},{3,2},{4,5},{5,4},{6,7},{7,6},{8,9},{9,8},{10,11... | collective-permute-start | bytes 884744 | tf_op jit(solution)/shard_map/ppermute | solution.py:21
  40.5 5.3 %collective-permute-done.7.refs_1_ = bf16[96,640]{1,0:T(8,128)(2,1)S(1)} collective-permute-done((bf16[96,640]{1,0:T(8,128)(2,1)S(1)}, bf16[96,640]{1,0:T(8,128)(2,1)S(1)}, u32[]{:S(2)}, u32[]{:S(2)}) %collective-permute-start.7) | collective-permute-done | bytes 122912 | tf_op jit(solution)/shard_map/ppermute | solution.py:21
  45.8 2.4 %collective-permute-start.24 = (bf16[2048,256]{1,0:T(8,128)(2,1)S(1)}, bf16[2048,256]{1,0:T(8,128)(2,1)S(1)}, u32[]{:S(2)}, u32[]{:S(2)}) collective-permute-start(bf16[2048,256]{1,0:T(8,128)(2,1)S(1)} %bitcast.61), channel_id=1, source_target_pairs={{0,1},{1,0},{2,3},{3,2},{4,5},{5,4},{6,7},{7,6},{8,9},{9,8},{10,11... | collective-permute-start | bytes 3145736 | tf_op jit(solution)/shard_map/ppermute | solution.py:21
  52.8 25.9 %collective-permute-done.36.refs_4_ = bf16[1024,256]{1,0:T(8,128)(2,1)S(1)} collective-permute-done((bf16[1024,256]{1,0:T(8,128)(2,1)S(1)}, bf16[1024,256]{1,0:T(8,128)(2,1)S(1)}, u32[]{:S(2)}, u32[]{:S(2)}) %collective-permute-start.36) | collective-permute-done | bytes 524320 | tf_op jit(solution)/shard_map/ppermute | solution.py:21
  80.6 2.3 %collective-permute-start.26 = (bf16[1472,256]{1,0:T(8,128)(2,1)S(1)}, bf16[1472,256]{1,0:T(8,128)(2,1)S(1)}, u32[]{:S(2)}, u32[]{:S(2)}) collective-permute-start(bf16[1472,256]{1,0:T(8,128)(2,1)S(1)} %slice.67), channel_id=1, source_target_pairs={{0,1},{1,0},{2,3},{3,2},{4,5},{5,4},{6,7},{7,6},{8,9},{9,8},{10,11... | collective-permute-start | bytes 2261000 | tf_op jit(solution)/shard_map/ppermute | solution.py:21
  82.9 18.6 %collective-permute-done.18.refs_2_ = bf16[96,2048]{1,0:T(8,128)(2,1)S(1)} collective-permute-done((bf16[96,2048]{1,0:T(8,128)(2,1)S(1)}, bf16[96,2048]{1,0:T(8,128)(2,1)S(1)}, u32[]{:S(2)}, u32[]{:S(2)}) %collective-permute-start.18) | collective-permute-done | bytes 393248 | tf_op jit(solution)/shard_map/ppermute | solution.py:21
  101.6 2.0 collective-permute-start.28
  105.8 15.6 %collective-permute-done.28.refs_6_ = bf16[1472,256]{1,0:T(8,128)(2,1)S(1)} collective-permute-done((bf16[1472,256]{1,0:T(8,128)(2,1)S(1)}, bf16[1472,256]{1,0:T(8,128)(2,1)S(1)}, u32[]{:S(2)}, u32[]{:S(2)}) %collective-permute-start.28) | collective-permute-done | bytes 753696 | tf_op jit(solution)/shard_map/ppermute | solution.py:21
  121.4 1.9 collective-permute-start.48
  125.4 18.5 %collective-permute-done.30.refs_1_ = bf16[2048,256]{1,0:T(8,128)(2,1)S(1)} collective-permute-done((bf16[2048,256]{1,0:T(8,128)(2,1)S(1)}, bf16[2048,256]{1,0:T(8,128)(2,1)S(1)}, u32[]{:S(2)}, u32[]{:S(2)}) %collective-permute-start.30) | collective-permute-done | bytes 1048608 | tf_op jit(solution)/shard_map/ppermute | solution.py:21
  143.8 1.9 collective-permute-start.43
  158.5 7.5 %collective-permute-done.43.refs_5_ = bf16[1024,256]{1,0:T(8,128)(2,1)S(1)} collective-permute-done((bf16[1024,256]{1,0:T(8,128)(2,1)S(1)}, bf16[1024,256]{1,0:T(8,128)(2,1)S(1)}, u32[]{:S(2)}, u32[]{:S(2)}) %collective-permute-start.43) | collective-permute-done | bytes 524320 | tf_op jit(solution)/shard_map/ppermute | solution.py:21
  172.8 8.3 %collective-permute-start.51 = (bf16[96,512]{1,0:T(8,128)(2,1)S(1)}, bf16[96,512]{1,0:T(8,128)(2,1)S(1)}, u32[]{:S(2)}, u32[]{:S(2)}) collective-permute-start(bf16[96,512]{1,0:T(8,128)(2,1)S(1)} %get-tuple-element.63), channel_id=1, source_target_pairs={{0,8},{4,12},{8,0},{12,4},{16,24},{20,28},{24,16},{28,20},{1,9},{5... | collective-permute-start | bytes 294920 | tf_op jit(solution)/shard_map/ppermute | solution.py:21
  181.7 1.9 collective-permute-start.53
  186.7 1.9 collective-permute-start.47
  188.6 3.3 %collective-permute-done.52.refs_14_ = bf16[96,512]{1,0:T(8,128)(2,1)S(1)} collective-permute-done((bf16[96,512]{1,0:T(8,128)(2,1)S(1)}, bf16[96,512]{1,0:T(8,128)(2,1)S(1)}, u32[]{:S(2)}, u32[]{:S(2)}) %collective-permute-start.52) | collective-permute-done | bytes 98336 | tf_op jit(solution)/shard_map/ppermute | solution.py:21
  192.0 7.3 %collective-permute-start.40 = (bf16[96,512]{1,0:T(8,128)(2,1)S(1)}, bf16[96,512]{1,0:T(8,128)(2,1)S(1)}, u32[]{:S(2)}, u32[]{:S(2)}) collective-permute-start(bf16[96,512]{1,0:T(8,128)(2,1)S(1)} %get-tuple-element.68), channel_id=1, source_target_pairs={{0,16},{4,20},{8,24},{12,28},{16,0},{20,4},{24,8},{28,12},{1,17},{... | collective-permute-start | bytes 294920 | tf_op jit(solution)/shard_map/ppermute | solution.py:21
  199.3 1.9 collective-permute-start.41
  202.5 5.2 %collective-permute-start.34 = (bf16[96,512]{1,0:T(8,128)(2,1)S(1)}, bf16[96,512]{1,0:T(8,128)(2,1)S(1)}, u32[]{:S(2)}, u32[]{:S(2)}) collective-permute-start(bf16[96,512]{1,0:T(8,128)(2,1)S(1)} %get-tuple-element.71), channel_id=1, source_target_pairs={{0,16},{4,20},{8,24},{12,28},{16,0},{20,4},{24,8},{28,12},{1,17},{... | collective-permute-start | bytes 294920 | tf_op jit(solution)/shard_map/ppermute | solution.py:21
  207.7 1.9 collective-permute-start.35
  210.9 6.3 %collective-permute-done.34.refs_2_ = bf16[96,512]{1,0:T(8,128)(2,1)S(1)} collective-permute-done((bf16[96,512]{1,0:T(8,128)(2,1)S(1)}, bf16[96,512]{1,0:T(8,128)(2,1)S(1)}, u32[]{:S(2)}, u32[]{:S(2)}) %collective-permute-start.34) | collective-permute-done | bytes 98336 | tf_op jit(solution)/shard_map/ppermute | solution.py:21
  221.3 2.1 collective-permute-done.54
  (171 shorter events, 76.9 us)
Async XLA Ops:
  3.1 33.8 %collective-permute-start.10 = (f32[4,512]{1,0:T(4,128)S(1)}, f32[4,512]{1,0:T(4,128)S(1)}, u32[]{:S(2)}, u32[]{:S(2)}) collective-permute-start(f32[4,512]{1,0:T(4,128)S(1)} %pad_maximum_fusion.5.refs_4_), channel_id=1, source_target_pairs={{0,1},{1,0},{2,3},{3,2},{4,5},{5,4},{6,7},{7,6},{8,9},{9,8},{10,11... | collective-permute-start | bytes 24584 | tf_op jit(solution)/shard_map/ppermute | solution.py:21
  14.7 23.7 %collective-permute-start.11 = (f32[4,512]{1,0:T(4,128)S(1)}, f32[4,512]{1,0:T(4,128)S(1)}, u32[]{:S(2)}, u32[]{:S(2)}) collective-permute-start(f32[4,512]{1,0:T(4,128)S(1)} %pad_maximum_fusion.5.refs_4_), channel_id=1, source_target_pairs={{0,2},{1,3},{2,0},{3,1},{4,6},{5,7},{6,4},{7,5},{8,10},{9,11},{10,... | collective-permute-start | bytes 24584 | tf_op jit(solution)/shard_map/ppermute | solution.py:21
  33.5 16.4 %collective-permute-start.25 = (bf16[576,256]{1,0:T(8,128)(2,1)S(1)}, bf16[576,256]{1,0:T(8,128)(2,1)S(1)}, u32[]{:S(2)}, u32[]{:S(2)}) collective-permute-start(bf16[576,256]{1,0:T(8,128)(2,1)S(1)} %slice.66), channel_id=1, source_target_pairs={{0,1},{1,0},{2,3},{3,2},{4,5},{5,4},{6,7},{7,6},{8,9},{9,8},{10,11... | collective-permute-start | bytes 884744 | tf_op jit(solution)/shard_map/ppermute | solution.py:21
  36.0 16.7 %collective-permute-start.27 = (bf16[576,256]{1,0:T(8,128)(2,1)S(1)}, bf16[576,256]{1,0:T(8,128)(2,1)S(1)}, u32[]{:S(2)}, u32[]{:S(2)}) collective-permute-start(bf16[576,256]{1,0:T(8,128)(2,1)S(1)} %slice.68), channel_id=1, source_target_pairs={{0,2},{1,3},{2,0},{3,1},{4,6},{5,7},{6,4},{7,5},{8,10},{9,11},{10,... | collective-permute-start | bytes 884744 | tf_op jit(solution)/shard_map/ppermute | solution.py:21
  45.8 57.8 %collective-permute-start.24 = (bf16[2048,256]{1,0:T(8,128)(2,1)S(1)}, bf16[2048,256]{1,0:T(8,128)(2,1)S(1)}, u32[]{:S(2)}, u32[]{:S(2)}) collective-permute-start(bf16[2048,256]{1,0:T(8,128)(2,1)S(1)} %bitcast.61), channel_id=1, source_target_pairs={{0,1},{1,0},{2,3},{3,2},{4,5},{5,4},{6,7},{7,6},{8,9},{9,8},{10,11... | collective-permute-start | bytes 3145736 | tf_op jit(solution)/shard_map/ppermute | solution.py:21
  48.2 30.5 %collective-permute-start.36 = (bf16[1024,256]{1,0:T(8,128)(2,1)S(1)}, bf16[1024,256]{1,0:T(8,128)(2,1)S(1)}, u32[]{:S(2)}, u32[]{:S(2)}) collective-permute-start(bf16[1024,256]{1,0:T(8,128)(2,1)S(1)} %get-tuple-element.56), channel_id=1, source_target_pairs={{0,1},{1,0},{2,3},{3,2},{4,5},{5,4},{6,7},{7,6},{8,9},{9,8},{10,11... | collective-permute-start | bytes 1572872 | tf_op jit(solution)/shard_map/ppermute | solution.py:21
  49.6 29.2 %collective-permute-start.37 = (bf16[1024,256]{1,0:T(8,128)(2,1)S(1)}, bf16[1024,256]{1,0:T(8,128)(2,1)S(1)}, u32[]{:S(2)}, u32[]{:S(2)}) collective-permute-start(bf16[1024,256]{1,0:T(8,128)(2,1)S(1)} %get-tuple-element.55), channel_id=1, source_target_pairs={{0,2},{1,3},{2,0},{3,1},{4,6},{5,7},{6,4},{7,5},{8,10},{9,11},{10,... | collective-permute-start | bytes 1572872 | tf_op jit(solution)/shard_map/ppermute | solution.py:21
  49.9 53.8 %collective-permute-start.29 = (bf16[2048,256]{1,0:T(8,128)(2,1)S(1)}, bf16[2048,256]{1,0:T(8,128)(2,1)S(1)}, u32[]{:S(2)}, u32[]{:S(2)}) collective-permute-start(bf16[2048,256]{1,0:T(8,128)(2,1)S(1)} %bitcast.65), channel_id=1, source_target_pairs={{0,2},{1,3},{2,0},{3,1},{4,6},{5,7},{6,4},{7,5},{8,10},{9,11},{10,... | collective-permute-start | bytes 3145736 | tf_op jit(solution)/shard_map/ppermute | solution.py:21
  52.7 27.9 %collective-permute-start.17 = (bf16[96,2048]{1,0:T(8,128)(2,1)S(1)}, bf16[96,2048]{1,0:T(8,128)(2,1)S(1)}, u32[]{:S(2)}, u32[]{:S(2)}) collective-permute-start(bf16[96,2048]{1,0:T(8,128)(2,1)S(1)} %get-tuple-element.34.refs_0_), channel_id=1, source_target_pairs={{0,8},{4,12},{8,0},{12,4},{16,24},{20,28},{24,16},{28,20},{1,9},{5... | collective-permute-start | bytes 1179656 | tf_op jit(solution)/shard_map/ppermute | solution.py:21
  78.7 22.8 %collective-permute-start.18 = (bf16[96,2048]{1,0:T(8,128)(2,1)S(1)}, bf16[96,2048]{1,0:T(8,128)(2,1)S(1)}, u32[]{:S(2)}, u32[]{:S(2)}) collective-permute-start(bf16[96,2048]{1,0:T(8,128)(2,1)S(1)} %get-tuple-element.34.refs_0_), channel_id=1, source_target_pairs={{0,16},{4,20},{8,24},{12,28},{16,0},{20,4},{24,8},{28,12},{1,17},{... | collective-permute-start | bytes 1179656 | tf_op jit(solution)/shard_map/ppermute | solution.py:21
  78.7 22.8 %collective-permute-start.19 = (bf16[96,2048]{1,0:T(8,128)(2,1)S(1)}, bf16[96,2048]{1,0:T(8,128)(2,1)S(1)}, u32[]{:S(2)}, u32[]{:S(2)}) collective-permute-start(bf16[96,2048]{1,0:T(8,128)(2,1)S(1)} %get-tuple-element.34.refs_0_), channel_id=1, source_target_pairs={{0,24},{4,28},{8,16},{12,20},{16,8},{20,12},{24,0},{28,4},{1,25},{... | collective-permute-start | bytes 1179656 | tf_op jit(solution)/shard_map/ppermute | solution.py:21
  80.6 24.7 %collective-permute-start.26 = (bf16[1472,256]{1,0:T(8,128)(2,1)S(1)}, bf16[1472,256]{1,0:T(8,128)(2,1)S(1)}, u32[]{:S(2)}, u32[]{:S(2)}) collective-permute-start(bf16[1472,256]{1,0:T(8,128)(2,1)S(1)} %slice.67), channel_id=1, source_target_pairs={{0,1},{1,0},{2,3},{3,2},{4,5},{5,4},{6,7},{7,6},{8,9},{9,8},{10,11... | collective-permute-start | bytes 2261000 | tf_op jit(solution)/shard_map/ppermute | solution.py:21
  101.6 19.8 %collective-permute-start.28 = (bf16[1472,256]{1,0:T(8,128)(2,1)S(1)}, bf16[1472,256]{1,0:T(8,128)(2,1)S(1)}, u32[]{:S(2)}, u32[]{:S(2)}) collective-permute-start(bf16[1472,256]{1,0:T(8,128)(2,1)S(1)} %slice.69), channel_id=1, source_target_pairs={{0,2},{1,3},{2,0},{3,1},{4,6},{5,7},{6,4},{7,5},{8,10},{9,11},{10,... | collective-permute-start | bytes 2261000 | tf_op jit(solution)/shard_map/ppermute | solution.py:21
  103.6 40.2 %collective-permute-start.30 = (bf16[2048,256]{1,0:T(8,128)(2,1)S(1)}, bf16[2048,256]{1,0:T(8,128)(2,1)S(1)}, u32[]{:S(2)}, u32[]{:S(2)}) collective-permute-start(bf16[2048,256]{1,0:T(8,128)(2,1)S(1)} %collective-permute-done.24.refs_2_), channel_id=1, source_target_pairs={{0,2},{1,3},{2,0},{3,1},{4,6},{5,7},{6,4},{7,5},{8,10},{9,11},{10,... | collective-permute-start | bytes 3145736 | tf_op jit(solution)/shard_map/ppermute | solution.py:21
  103.7 48.9 %collective-permute-start.31 = (bf16[2048,256]{1,0:T(8,128)(2,1)S(1)}, bf16[2048,256]{1,0:T(8,128)(2,1)S(1)}, u32[]{:S(2)}, u32[]{:S(2)}) collective-permute-start(bf16[2048,256]{1,0:T(8,128)(2,1)S(1)} %collective-permute-done.29.refs_7_), channel_id=1, source_target_pairs={{0,1},{1,0},{2,3},{3,2},{4,5},{5,4},{6,7},{7,6},{8,9},{9,8},{10,11... | collective-permute-start | bytes 3145736 | tf_op jit(solution)/shard_map/ppermute | solution.py:21
  105.3 16.1 %collective-permute-start.21 = (bf16[96,2048]{1,0:T(8,128)(2,1)S(1)}, bf16[96,2048]{1,0:T(8,128)(2,1)S(1)}, u32[]{:S(2)}, u32[]{:S(2)}) collective-permute-start(bf16[96,2048]{1,0:T(8,128)(2,1)S(1)} %collective-permute-done.17.refs_1_), channel_id=1, source_target_pairs={{0,4},{4,0},{8,12},{12,8},{16,20},{20,16},{24,28},{28,24},{1,5},{5... | collective-permute-start | bytes 1179656 | tf_op jit(solution)/shard_map/ppermute | solution.py:21
  105.3 18.1 %collective-permute-start.22 = (bf16[96,2048]{1,0:T(8,128)(2,1)S(1)}, bf16[96,2048]{1,0:T(8,128)(2,1)S(1)}, u32[]{:S(2)}, u32[]{:S(2)}) collective-permute-start(bf16[96,2048]{1,0:T(8,128)(2,1)S(1)} %collective-permute-done.18.refs_2_), channel_id=1, source_target_pairs={{0,4},{4,0},{8,12},{12,8},{16,20},{20,16},{24,28},{28,24},{1,5},{5... | collective-permute-start | bytes 1179656 | tf_op jit(solution)/shard_map/ppermute | solution.py:21
  121.4 33.7 %collective-permute-start.48 = (bf16[1024,256]{1,0:T(8,128)(2,1)S(1)}, bf16[1024,256]{1,0:T(8,128)(2,1)S(1)}, u32[]{:S(2)}, u32[]{:S(2)}) collective-permute-start(bf16[1024,256]{1,0:T(8,128)(2,1)S(1)} %collective-permute-done.36.refs_4_), channel_id=1, source_target_pairs={{0,2},{1,3},{2,0},{3,1},{4,6},{5,7},{6,4},{7,5},{8,10},{9,11},{10,... | collective-permute-start | bytes 1572872 | tf_op jit(solution)/shard_map/ppermute | solution.py:21
  123.3 31.7 %collective-permute-start.49 = (bf16[1024,256]{1,0:T(8,128)(2,1)S(1)}, bf16[1024,256]{1,0:T(8,128)(2,1)S(1)}, u32[]{:S(2)}, u32[]{:S(2)}) collective-permute-start(bf16[1024,256]{1,0:T(8,128)(2,1)S(1)} %collective-permute-done.37.refs_5_), channel_id=1, source_target_pairs={{0,1},{1,0},{2,3},{3,2},{4,5},{5,4},{6,7},{7,6},{8,9},{9,8},{10,11... | collective-permute-start | bytes 1572872 | tf_op jit(solution)/shard_map/ppermute | solution.py:21
  124.8 33.7 %collective-permute-start.42 = (bf16[1024,256]{1,0:T(8,128)(2,1)S(1)}, bf16[1024,256]{1,0:T(8,128)(2,1)S(1)}, u32[]{:S(2)}, u32[]{:S(2)}) collective-permute-start(bf16[1024,256]{1,0:T(8,128)(2,1)S(1)} %get-tuple-element.55), channel_id=1, source_target_pairs={{0,1},{1,0},{2,3},{3,2},{4,5},{5,4},{6,7},{7,6},{8,9},{9,8},{10,11... | collective-permute-start | bytes 1572872 | tf_op jit(solution)/shard_map/ppermute | solution.py:21
  143.8 22.2 %collective-permute-start.43 = (bf16[1024,256]{1,0:T(8,128)(2,1)S(1)}, bf16[1024,256]{1,0:T(8,128)(2,1)S(1)}, u32[]{:S(2)}, u32[]{:S(2)}) collective-permute-start(bf16[1024,256]{1,0:T(8,128)(2,1)S(1)} %get-tuple-element.56), channel_id=1, source_target_pairs={{0,2},{1,3},{2,0},{3,1},{4,6},{5,7},{6,4},{7,5},{8,10},{9,11},{10,... | collective-permute-start | bytes 1572872 | tf_op jit(solution)/shard_map/ppermute | solution.py:21
  156.2 16.4 %collective-permute-start.50 = (bf16[384,512]{1,0:T(8,128)(2,1)S(1)}, bf16[384,512]{1,0:T(8,128)(2,1)S(1)}, u32[]{:S(2)}, u32[]{:S(2)}) collective-permute-start(bf16[384,512]{1,0:T(8,128)(2,1)S(1)} %down.15), channel_id=1, source_target_pairs={{0,4},{4,0},{8,12},{12,8},{16,20},{20,16},{24,28},{28,24},{1,5},{5... | collective-permute-start | bytes 1179656 | tf_op jit(solution)/shard_map/ppermute | solution.py:21
  185.0 17.5 %collective-permute-start.46 = (bf16[96,512]{1,0:T(8,128)(2,1)S(1)}, bf16[96,512]{1,0:T(8,128)(2,1)S(1)}, u32[]{:S(2)}, u32[]{:S(2)}) collective-permute-start(bf16[96,512]{1,0:T(8,128)(2,1)S(1)} %get-tuple-element.65), channel_id=1, source_target_pairs={{0,16},{4,20},{8,24},{12,28},{16,0},{20,4},{24,8},{28,12},{1,17},{... | collective-permute-start | bytes 294920 | tf_op jit(solution)/shard_map/ppermute | solution.py:21
  192.0 18.9 %collective-permute-start.40 = (bf16[96,512]{1,0:T(8,128)(2,1)S(1)}, bf16[96,512]{1,0:T(8,128)(2,1)S(1)}, u32[]{:S(2)}, u32[]{:S(2)}) collective-permute-start(bf16[96,512]{1,0:T(8,128)(2,1)S(1)} %get-tuple-element.68), channel_id=1, source_target_pairs={{0,16},{4,20},{8,24},{12,28},{16,0},{20,4},{24,8},{28,12},{1,17},{... | collective-permute-start | bytes 294920 | tf_op jit(solution)/shard_map/ppermute | solution.py:21
  (47 other events, 412.2 us)
